TPU v7x, 32 devices: a whole 2x2x4 slice. The times are simulated.
32 devices in a mesh: sp: 8 (over z, y), dp: 4 (over x, core).
Axes of the slice: x: 2, y: 2, z: 4, core: 2. Of those that a mesh axis runs over, the one named last changes fastest.
Arguments:
- queries: bfloat16 [4, 2048, 1280], P('dp', None, 'sp'), may hold values from -6 to 6
- keys: bfloat16 [4, 1024, 1280], P('dp', None, 'sp'), may hold values from -6 to 6
- values: bfloat16 [4, 1024, 1280], P('dp', None, 'sp'), may hold values from -48 to 48
- q_gain: float32 [64], replicated, may hold values from 0.5 to 10
- k_gain: float32 [64], replicated, may hold values from 0.5 to 10
- w_out: bfloat16 [2048, 2048], P(None, 'dp'), may hold values from -0.125 to 0.125
Outputs:
- mixed: bfloat16 [4, 1280, 2048], P('dp', 'sp')
All inputs are finite; a program needn't handle non-finite values.
Results may differ from a plain program's by a relative error of at most 0.0038.
The roundings to bfloat16 on the way count: a program that leaves them out, or rounds other values in their place, can miss the bound.
Values may be sent and summed in bfloat16 or wider, within the bound.
No kernel may reach another device: no remote copies, remote signals or barrier semaphores. Data moves between devices by JAX's collectives and lax.ppermute only.
A program may use at most 64 MiB of HBM per device.

v0:
```python
import functools

import jax
import jax.numpy as jnp
from jax import lax
from jax.experimental import pallas as pl
from jax.experimental.pallas import tpu as pltpu
from jax.sharding import PartitionSpec as P


HD = 64
QH = 32
KV = 16
GRID_W = 64
GROUP = QH // KV

epsilon = 1e-06
rotary_base = 10000.0
block_count = 8


def swapped(block, axis, apart):
    count = lax.axis_size(axis)
    route = []
    for low in range(count):
        high = low | 1 << apart
        if high != low and high < count:
            route += [(low, high), (high, low)]
    return lax.ppermute(block, axis, route)


def rotary_tables(first_row, row_count):
    position = first_row + lax.iota(jnp.int32, row_count)
    grid_row = (position // GRID_W).astype(jnp.float32)
    grid_col = (position % GRID_W).astype(jnp.float32)
    quarter = HD // 4
    inv_freq = rotary_base ** (-(2.0 * lax.iota(jnp.float32, quarter)) / (HD // 2))
    row_angle = inv_freq[:, None] * grid_row[None, :]
    col_angle = inv_freq[:, None] * grid_col[None, :]
    cos_table = jnp.concatenate(
        [jnp.cos(row_angle), jnp.cos(row_angle), jnp.cos(col_angle), jnp.cos(col_angle)], axis=0
    )
    sin_table = jnp.concatenate(
        [jnp.sin(row_angle), jnp.sin(row_angle), jnp.sin(col_angle), jnp.sin(col_angle)], axis=0
    )
    return (cos_table, sin_table)


def normalize_turn(field, gain, cos_table, sin_table):
    head_count = field.shape[0] // HD
    values_f = field.astype(jnp.float32).reshape(head_count, HD, field.shape[1])
    normed = (
        values_f
        * lax.rsqrt(jnp.mean(values_f * values_f, axis=1, keepdims=True) + epsilon)
        * gain[None, :, None]
    )
    quarter = HD // 4
    quarters_of = normed.reshape(head_count, 4, quarter, field.shape[1])
    turned = jnp.concatenate(
        [-quarters_of[:, 1], quarters_of[:, 0], -quarters_of[:, 3], quarters_of[:, 2]], axis=1
    )
    return (normed * cos_table[None] + turned * sin_table[None]).astype(jnp.bfloat16)


def attention_heads(query_heads, key_heads, value_heads, seq_len):
    kv_local = key_heads.shape[0]
    group_local = query_heads.shape[0] // kv_local
    query_split = query_heads.reshape(kv_local, group_local, HD, seq_len)
    score_scale = HD ** (-0.5)
    block_rows = seq_len // block_count

    def one_block(block_index, result):
        row_start = block_index * block_rows
        query_block = lax.dynamic_slice_in_dim(query_split, row_start, block_rows, 3)
        scores = (
            jnp.einsum("hgdq,hdk->hgqk", query_block, key_heads, preferred_element_type=jnp.float32)
            * score_scale
        )
        row_max = jnp.max(scores, axis=-1, keepdims=True)
        weights = jnp.exp(scores - row_max)
        weights = (weights / jnp.sum(weights, axis=-1, keepdims=True)).astype(jnp.bfloat16)
        attended = jnp.einsum(
            "hgqk,hdk->hgdq", weights, value_heads, preferred_element_type=jnp.float32
        )
        return lax.dynamic_update_slice_in_dim(result, attended.astype(jnp.bfloat16), row_start, 3)

    result = jnp.zeros(query_split.shape, jnp.bfloat16)
    result = lax.fori_loop(0, block_count, one_block, result)
    return result.reshape(query_heads.shape)


def plain_form(queries, keys, values, q_gain, k_gain, w_out):
    sp_count = lax.axis_size("sp")
    tok_rows = queries.shape[2]
    seq_len = tok_rows * sp_count
    cos_table, sin_table = rotary_tables(lax.axis_index("sp") * tok_rows, tok_rows)
    query_rot = normalize_turn(queries[0], q_gain, cos_table, sin_table)
    key_rot = normalize_turn(keys[0], k_gain, cos_table, sin_table)
    value_rows = values[0].reshape(KV, HD, tok_rows)
    query_heads = lax.all_to_all(query_rot, "sp", split_axis=0, concat_axis=2, tiled=True)
    share_count = max(sp_count // KV, 1)
    part_rows = tok_rows // share_count
    key_cut = (
        key_rot.reshape(KV, HD, share_count, part_rows)
        .transpose(0, 2, 1, 3)
        .reshape(KV * share_count, HD, part_rows)
    )
    value_cut = (
        value_rows.reshape(KV, HD, share_count, part_rows)
        .transpose(0, 2, 1, 3)
        .reshape(KV * share_count, HD, part_rows)
    )
    key_got, value_got = (
        lax.all_to_all(key_cut, "sp", split_axis=0, concat_axis=2, tiled=True),
        lax.all_to_all(value_cut, "sp", split_axis=0, concat_axis=2, tiled=True),
    )
    kv_local = key_got.shape[0]
    key_got = key_got.reshape(kv_local, HD, sp_count, part_rows)
    value_got = value_got.reshape(kv_local, HD, sp_count, part_rows)
    for bit_index in range(share_count.bit_length() - 1):
        key_other, value_other = swapped((key_got, value_got), "sp", bit_index)
        key_got = jnp.concatenate([key_got, key_other], axis=3)
        value_got = jnp.concatenate([value_got, value_other], axis=3)
    key_heads = key_got.reshape(kv_local, HD, seq_len)
    value_heads = value_got.reshape(kv_local, HD, seq_len)
    attended = attention_heads(query_heads, key_heads, value_heads, seq_len)
    token_heads = lax.all_to_all(attended, "sp", split_axis=2, concat_axis=0, tiled=True)
    token_rows = token_heads.reshape(QH * HD, tok_rows)
    product = lax.dot_general(
        token_rows,
        lax.all_gather(w_out, "dp", axis=1, tiled=True),
        (((0,), (0,)), ((), ())),
        preferred_element_type=jnp.float32,
    )
    mixed_rows = product.astype(jnp.bfloat16)
    return mixed_rows[None]


TILE = 128


def rotary_lanes(first_row, row_count):
    position = first_row + lax.broadcasted_iota(jnp.int32, (row_count, TILE), 0)
    lane = lax.broadcasted_iota(jnp.int32, (row_count, TILE), 1) % HD
    quarter = HD // 4
    inv_freq = rotary_base ** (-(2.0 * (lane % quarter).astype(jnp.float32)) / (HD // 2))
    place = jnp.where(lane < HD // 2, position // GRID_W, position % GRID_W).astype(jnp.float32)
    angle = inv_freq * place
    sine = jnp.sin(angle)
    return jnp.cos(angle), jnp.where((lane // quarter) % 2 == 0, -sine, sine)


def turn_kernel(groups, chunks, *refs):
    sources, (cos_ref, sin_ref), out_refs = refs[:5], refs[5:7], refs[7:-6]
    held, sems = refs[-6:-1], refs[-1]
    copies = [pltpu.make_async_copy(src, dst, sems.at[i]) for i, (src, dst) in enumerate(zip(sources, held))]
    for copy in copies:
        copy.start()
    for copy in copies:
        copy.wait()
    q_ref, k_ref, v_ref, qg_ref, kg_ref = held
    home = lax.axis_index("sp") % groups
    cos_table, sin_table = cos_ref[...], sin_ref[...]
    q_gain = jnp.concatenate([qg_ref[...]] * 2, axis=1)
    k_gain = jnp.concatenate([kg_ref[...]] * 2, axis=1)
    quarter = HD // 4
    lane = lax.broadcasted_iota(jnp.int32, cos_table.shape, 1)
    even = (lane // quarter) % 2 == 0
    row_head = (lax.broadcasted_iota(jnp.int32, (2 * TILE, TILE), 0) % TILE) // HD
    col_head = lax.broadcasted_iota(jnp.int32, (2 * TILE, TILE), 1) // HD
    average = jnp.where(row_head == col_head, 1.0 / HD, 0.0).astype(jnp.bfloat16)

    def turned(tile, gain):
        field = tile.astype(jnp.float32)
        square = field * field
        coarse = square.astype(jnp.bfloat16)
        fine = (square - coarse.astype(jnp.float32)).astype(jnp.bfloat16)
        mean = jnp.dot(
            jnp.concatenate([coarse, fine], axis=1), average, preferred_element_type=jnp.float32
        )
        normed = field * lax.rsqrt(mean + epsilon) * gain
        partner = jnp.where(even, pltpu.roll(normed, TILE - quarter, 1), pltpu.roll(normed, quarter, 1))
        return (normed * cos_table + partner * sin_table).astype(jnp.bfloat16)

    both_refs, kv_refs = out_refs[: groups * chunks], out_refs[groups * chunks :]
    for c in range(chunks):
        for j in range(groups):
            place = (home ^ j) * chunks + c
            both, kv = both_refs[c * groups + j], kv_refs[c * groups + j]
            for p in range(2):
                lanes = pl.ds(pl.multiple_of((place * 2 + p) * TILE, TILE), TILE)
                both[:, p * TILE : (p + 1) * TILE] = turned(q_ref[:, lanes], q_gain)
            lanes = pl.ds(pl.multiple_of(place * TILE, TILE), TILE)
            key, value = turned(k_ref[:, lanes], k_gain), v_ref[:, lanes]
            both[:, 2 * TILE : 3 * TILE] = key
            both[:, 3 * TILE :] = value
            kv[:, :TILE] = key
            kv[:, TILE:] = value


def in_vmem(count):
    return [pl.BlockSpec(memory_space=pltpu.VMEM)] * count


def params(mib):
    return pltpu.CompilerParams(vmem_limit_bytes=mib << 20)


def turn_and_pack(queries, keys, values, q_gain, k_gain, cos_table, sin_table, groups, chunks):
    tok = queries.shape[0]
    made = groups * chunks
    out = pl.pallas_call(
        functools.partial(turn_kernel, groups, chunks),
        in_specs=[pl.BlockSpec(memory_space=pltpu.HBM)] * 5 + in_vmem(2),
        out_specs=in_vmem(2 * made),
        out_shape=[jax.ShapeDtypeStruct((tok, 4 * TILE), jnp.bfloat16)] * made
        + [jax.ShapeDtypeStruct((tok, 2 * TILE), jnp.bfloat16)] * made,
        scratch_shapes=[pltpu.VMEM(x.shape, x.dtype) for x in (queries, keys, values)]
        + [pltpu.VMEM((1, HD), jnp.float32)] * 2
        + [pltpu.SemaphoreType.DMA((5,))],
        compiler_params=params(16),
        cost_estimate=pl.CostEstimate(flops=40 * 3072 * tok, bytes_accessed=6 * 4096 * tok, transcendentals=0),
        name="turn",
    )(queries, keys, values, q_gain[None], k_gain[None], cos_table, sin_table)
    both = [out[c * groups : (c + 1) * groups] for c in range(chunks)]
    kv = [out[made + c * groups : made + (c + 1) * groups] for c in range(chunks)]
    return both, kv


SOFT_ROWS = 16


def attend_kernel(groups, *refs):
    both_refs, far_refs, out_refs = refs[:groups], refs[groups : 2 * groups], refs[2 * groups : 3 * groups]
    keys_scr, vals_scr, s_scr, w_scr = refs[3 * groups :]
    rows = both_refs[0].shape[0]
    seq = 2 * groups * rows
    pair = pl.program_id(0)
    first = pair == 0
    low = lax.broadcasted_iota(jnp.int32, (rows, TILE), 1) < HD

    def spread(tile, scr, i):
        tile = tile.astype(jnp.float32)
        other = pltpu.roll(tile, HD, 1)
        here, there = jnp.where(first, tile, other), jnp.where(first, other, tile)
        scr[i * rows : (i + 1) * rows, :] = jnp.where(low, here, 0.0).astype(jnp.bfloat16)
        scr[seq + i * rows : seq + (i + 1) * rows, :] = jnp.where(low, 0.0, there).astype(jnp.bfloat16)

    for i in range(groups):
        spread(both_refs[i][:, 2 * TILE : 3 * TILE], keys_scr, i)
        spread(both_refs[i][:, 3 * TILE :], vals_scr, i)
        spread(far_refs[i][:, :TILE], keys_scr, groups + i)
        spread(far_refs[i][:, TILE:], vals_scr, groups + i)

    factor = HD ** (-0.5) * 1.4426950408889634
    lanes = pl.ds(pl.multiple_of(pair * TILE, TILE), TILE)
    for j in range(groups):
        slot = j % 2
        s_scr[slot] = lax.dot_general(
            both_refs[j][:, lanes], keys_scr[...], (((1,), (1,)), ((), ())), preferred_element_type=jnp.float32
        )
        for g in range(GROUP):
            for r in range(0, rows, SOFT_ROWS):
                s = s_scr[slot, r : r + SOFT_ROWS, g * seq : (g + 1) * seq]
                e = jnp.exp2((s - jnp.max(s, axis=-1, keepdims=True)) * factor)
                w = e * (1.0 / jnp.sum(e, axis=-1, keepdims=True))
                w_scr[slot, r : r + SOFT_ROWS, g * seq : (g + 1) * seq] = w.astype(jnp.bfloat16)
        out_refs[j][:, lanes] = jnp.dot(
            w_scr[slot], vals_scr[...], preferred_element_type=jnp.float32
        ).astype(jnp.bfloat16)


def attend(both, far):
    groups = len(both)
    rows = both[0].shape[0]
    seq = 2 * groups * rows
    return pl.pallas_call(
        functools.partial(attend_kernel, groups),
        grid=(2,),
        in_specs=in_vmem(2 * groups),
        out_specs=in_vmem(groups),
        out_shape=[jax.ShapeDtypeStruct((rows, 2 * TILE), jnp.bfloat16)] * groups,
        scratch_shapes=[
            pltpu.VMEM((GROUP * seq, TILE), jnp.bfloat16),
            pltpu.VMEM((GROUP * seq, TILE), jnp.bfloat16),
            pltpu.VMEM((2, rows, GROUP * seq), jnp.float32),
            pltpu.VMEM((2, rows, GROUP * seq), jnp.bfloat16),
        ],
        compiler_params=params(24),
        cost_estimate=pl.CostEstimate(
            flops=16 * groups * rows * seq * HD, bytes_accessed=12 * seq * TILE, transcendentals=0
        ),
        name="attend",
    )(*both, *far)


def project_kernel(groups, chunks, early, late, *refs):
    att_refs, refs = refs[: groups * chunks], refs[groups * chunks :]
    home = lax.axis_index("sp") % groups

    def product(w_ref):
        total = None
        for c in range(chunks):
            for j in range(groups):
                row = pl.ds(pl.multiple_of(((home ^ j) * chunks + c) * 2 * TILE, 2 * TILE), 2 * TILE)
                term = jnp.dot(att_refs[c * groups + j][...], w_ref[row, :], preferred_element_type=jnp.float32)
                total = term if total is None else total + term
        return total.astype(jnp.bfloat16)

    if late is None:
        for i, w_ref, out_ref in zip(early, refs[: len(early)], refs[len(early) :]):
            out_ref[...] = product(w_ref)
        return
    me = lax.axis_index("dp")
    w_refs, early_refs, out_ref = refs[: len(late)], refs[len(late) : -1], refs[-1]
    width = w_refs[0].shape[1]
    column = lambda i: pl.ds(pl.multiple_of((me ^ i) * width, width), width)
    for i, early_ref in zip(early, early_refs):
        out_ref[:, column(i)] = early_ref[...]
    for i, w_ref in zip(late, w_refs):
        out_ref[:, column(i)] = product(w_ref)


def project(attended, blocks, early, late=None, made=()):
    chunks, groups = len(attended), len(attended[0])
    tok = attended[0][0].shape[0]
    depth, width = blocks[0].shape
    flat = [piece for chunk in attended for piece in chunk]
    which = early if late is None else late
    if late is None:
        out_shape = [jax.ShapeDtypeStruct((tok, width), jnp.bfloat16)] * len(early)
        out_specs = in_vmem(len(early))
    else:
        out_shape = jax.ShapeDtypeStruct((tok, len(blocks) * width), jnp.bfloat16)
        out_specs = pl.BlockSpec(memory_space=pltpu.VMEM)
    return pl.pallas_call(
        functools.partial(project_kernel, groups, chunks, early, late),
        in_specs=in_vmem(len(flat) + len(which) + len(made)),
        out_specs=out_specs,
        out_shape=out_shape,
        compiler_params=params(16),
        cost_estimate=pl.CostEstimate(
            flops=2 * tok * depth * width * len(which), bytes_accessed=2 * depth * width * len(which),
            transcendentals=0,
        ),
        name="project",
    )(*flat, *[blocks[i] for i in which], *made)


def exchanged(block, axis, flip):
    count = lax.axis_size(axis)
    return lax.ppermute(block, axis, [(i, i ^ flip) for i in range(count)])


def group_form(queries, keys, values, q_gain, k_gain, w_out):
    sp_count, dp_count = lax.axis_size("sp"), lax.axis_size("dp")
    tok = queries.shape[2]
    groups = sp_count // 2
    chunks = KV // groups // 2
    bits = dp_count.bit_length() - 1
    top = 1 << (bits - 1)
    blocks = {0: w_out, top: exchanged(w_out, "dp", top)}
    early, late = [0], [top]
    for bit in reversed(range(bits - 1)):
        for listed in (early, late):
            for key in list(listed):
                blocks[key | 1 << bit] = exchanged(blocks[key], "dp", 1 << bit)
                listed.append(key | 1 << bit)
    cos_table, sin_table = rotary_lanes(lax.axis_index("sp") * tok, tok)
    both, kv = turn_and_pack(queries[0].T, keys[0].T, values[0].T, q_gain, k_gain, cos_table, sin_table, groups, chunks)
    near, far = [], []
    for c in range(chunks):
        near.append([both[c][0]] + [exchanged(both[c][j], "sp", j) for j in range(1, groups)])
        far.append([exchanged(kv[c][j], "sp", groups + j) for j in range(groups)])
    back = []
    for c in range(chunks):
        done = attend(near[c], far[c])
        back.append([done[0]] + [exchanged(done[j], "sp", j) for j in range(1, groups)])
    listed = [blocks[i] for i in range(dp_count)]
    made = project(back, listed, early)
    mixed = project(back, listed, early, late, made)
    return mixed[None]


def grouped(sp_count, dp_count):
    powers = sp_count & (sp_count - 1) == 0 and dp_count & (dp_count - 1) == 0
    return powers and sp_count > 2 and dp_count > 1 and KV % sp_count == 0


def on_device(*args):
    if grouped(lax.axis_size("sp"), lax.axis_size("dp")):
        return group_form(*args)
    return plain_form(*args)


def solution(mesh):
    placed = (
        P("dp", None, "sp"),
        P("dp", None, "sp"),
        P("dp", None, "sp"),
        P(),
        P(),
        P(None, "dp"),
    )
    return jax.shard_map(
        on_device, mesh=mesh, in_specs=placed, out_specs=P("dp", "sp", None), check_vma=False
    )
```

profile of v0, /device:TPU:0, one launch (start us, length us, event | category | flops | bytes accessed | tf_op | source)
XLA Modules:
  0.0 127.4 jit_solution(1124418323862072182)
XLA Ops:
  0.0 3.0 %collective-permute-start.20 = (bf16[2048,512]{1,0:T(8,128)(2,1)}, bf16[2048,512]{1,0:T(8,128)(2,1)}, u32[]{:S(2)}, u32[]{:S(2)}) collective-permute-start(bf16[2048,512]{1,0:T(8,128)(2,1)} %refs_8_.1), channel_id=1, source_target_pairs={{0,2},{1,3},{2,0},{3,1},{4,6},{5,7},{6,4},{7,5},{8,10},{9,11},{10,... | collective-permute-start | bytes 6291464 | tf_op jit(solution)/shard_map/ppermute | solution.py:352
  3.0 45.9 %collective-permute-done.20.refs_8_ = bf16[2048,512]{1,0:T(8,128)(2,1)} collective-permute-done((bf16[2048,512]{1,0:T(8,128)(2,1)}, bf16[2048,512]{1,0:T(8,128)(2,1)}, u32[]{:S(2)}, u32[]{:S(2)}) %collective-permute-start.20) | collective-permute-done | bytes 2097184 | tf_op jit(solution)/shard_map/ppermute | solution.py:352
  48.9 0.0 collective-permute-start.21
  49.0 0.4 negate_select_fusion
  49.4 0.0 copy-start.1
  49.4 1.1 copy-done.1
  50.5 1.0 copy-done.2
  51.5 1.0 copy-done.3
  52.4 0.7 copy-done.4
  53.1 0.7 copy-done.5
  53.7 2.1 %turn.1 = (bf16[160,512]{1,0:T(8,128)(2,1)S(1)}, bf16[160,512]{1,0:T(8,128)(2,1)S(1)}, bf16[160,512]{1,0:T(8,128)(2,1)S(1)}, bf16[160,512]{1,0:T(8,128)(2,1)S(1)...) custom-call(bf16[160,2048]{1,0:T(8,128)(2,1)S(1)} %bitcast.12, ...), custom_call_target="tpu_custom_call" | custom-call | flops 19660800 | bytes 3932160 | tf_op jit(solution)/shard_map/turn/pallas_call | solution.py:212
  55.9 2.9 %collective-permute-start.13 = (bf16[160,256]{1,0:T(8,128)(2,1)S(1)}, bf16[160,256]{1,0:T(8,128)(2,1)S(1)}, u32[]{:S(2)}, u32[]{:S(2)}) collective-permute-start(bf16[160,256]{1,0:T(8,128)(2,1)S(1)} %get-tuple-element.47), channel_id=1, source_target_pairs={{0,16},{4,20},{8,24},{12,28},{16,0},{20,4},{24,8},{28,12},{1,17},{... | collective-permute-start | bytes 245768 | tf_op jit(solution)/shard_map/ppermute | solution.py:352
  58.8 1.3 %collective-permute-start.14 = (bf16[160,256]{1,0:T(8,128)(2,1)S(1)}, bf16[160,256]{1,0:T(8,128)(2,1)S(1)}, u32[]{:S(2)}, u32[]{:S(2)}) collective-permute-start(bf16[160,256]{1,0:T(8,128)(2,1)S(1)} %get-tuple-element.48), channel_id=1, source_target_pairs={{0,20},{4,16},{8,28},{12,24},{16,4},{20,0},{24,12},{28,8},{1,21},{... | collective-permute-start | bytes 245768 | tf_op jit(solution)/shard_map/ppermute | solution.py:352
  60.1 3.6 %collective-permute-start.15 = (bf16[160,256]{1,0:T(8,128)(2,1)S(1)}, bf16[160,256]{1,0:T(8,128)(2,1)S(1)}, u32[]{:S(2)}, u32[]{:S(2)}) collective-permute-start(bf16[160,256]{1,0:T(8,128)(2,1)S(1)} %get-tuple-element.49), channel_id=1, source_target_pairs={{0,24},{4,28},{8,16},{12,20},{16,8},{20,12},{24,0},{28,4},{1,25},{... | collective-permute-start | bytes 245768 | tf_op jit(solution)/shard_map/ppermute | solution.py:352
  63.7 0.2 collective-permute-done.13.refs_4_
  63.8 7.9 %collective-permute-start.16 = (bf16[160,256]{1,0:T(8,128)(2,1)S(1)}, bf16[160,256]{1,0:T(8,128)(2,1)S(1)}, u32[]{:S(2)}, u32[]{:S(2)}) collective-permute-start(bf16[160,256]{1,0:T(8,128)(2,1)S(1)} %get-tuple-element.50), channel_id=1, source_target_pairs={{0,28},{4,24},{8,20},{12,16},{16,12},{20,8},{24,4},{28,0},{1,29},{... | collective-permute-start | bytes 245768 | tf_op jit(solution)/shard_map/ppermute | solution.py:352
  71.7 2.9 %collective-permute-start.4 = (bf16[160,256]{1,0:T(8,128)(2,1)S(1)}, bf16[160,256]{1,0:T(8,128)(2,1)S(1)}, u32[]{:S(2)}, u32[]{:S(2)}) collective-permute-start(bf16[160,256]{1,0:T(8,128)(2,1)S(1)} %get-tuple-element.36), channel_id=1, source_target_pairs={{0,20},{4,16},{8,28},{12,24},{16,4},{20,0},{24,12},{28,8},{1,21},{... | collective-permute-start | bytes 245768 | tf_op jit(solution)/shard_map/ppermute | solution.py:352
  74.6 4.2 %collective-permute-start.5 = (bf16[160,256]{1,0:T(8,128)(2,1)S(1)}, bf16[160,256]{1,0:T(8,128)(2,1)S(1)}, u32[]{:S(2)}, u32[]{:S(2)}) collective-permute-start(bf16[160,256]{1,0:T(8,128)(2,1)S(1)} %get-tuple-element.37), channel_id=1, source_target_pairs={{0,24},{4,28},{8,16},{12,20},{16,8},{20,12},{24,0},{28,4},{1,25},{... | collective-permute-start | bytes 245768 | tf_op jit(solution)/shard_map/ppermute | solution.py:352
  78.8 3.2 %collective-permute-done.3.refs_4_ = bf16[160,256]{1,0:T(8,128)(2,1)S(1)} collective-permute-done((bf16[160,256]{1,0:T(8,128)(2,1)S(1)}, bf16[160,256]{1,0:T(8,128)(2,1)S(1)}, u32[]{:S(2)}, u32[]{:S(2)}) %collective-permute-start.3) | collective-permute-done | bytes 81952 | tf_op jit(solution)/shard_map/ppermute | solution.py:352
  82.0 2.9 %collective-permute-start.6 = (bf16[160,256]{1,0:T(8,128)(2,1)S(1)}, bf16[160,256]{1,0:T(8,128)(2,1)S(1)}, u32[]{:S(2)}, u32[]{:S(2)}) collective-permute-start(bf16[160,256]{1,0:T(8,128)(2,1)S(1)} %get-tuple-element.38), channel_id=1, source_target_pairs={{0,28},{4,24},{8,20},{12,16},{16,12},{20,8},{24,4},{28,0},{1,29},{... | collective-permute-start | bytes 245768 | tf_op jit(solution)/shard_map/ppermute | solution.py:352
  84.9 0.0 collective-permute-done.4.refs_5_
  84.9 0.7 collective-permute-start.10
  85.6 0.0 collective-permute-done.5.refs_6_
  85.6 1.4 %collective-permute-start.11 = (bf16[160,512]{1,0:T(8,128)(2,1)S(1)}, bf16[160,512]{1,0:T(8,128)(2,1)S(1)}, u32[]{:S(2)}, u32[]{:S(2)}) collective-permute-start(bf16[160,512]{1,0:T(8,128)(2,1)S(1)} %get-tuple-element.45), channel_id=1, source_target_pairs={{0,8},{4,12},{8,0},{12,4},{16,24},{20,28},{24,16},{28,20},{1,9},{5... | collective-permute-start | bytes 491528 | tf_op jit(solution)/shard_map/ppermute | solution.py:352
  86.9 2.3 %collective-permute-done.6.refs_7_ = bf16[160,256]{1,0:T(8,128)(2,1)S(1)} collective-permute-done((bf16[160,256]{1,0:T(8,128)(2,1)S(1)}, bf16[160,256]{1,0:T(8,128)(2,1)S(1)}, u32[]{:S(2)}, u32[]{:S(2)}) %collective-permute-start.6) | collective-permute-done | bytes 81952 | tf_op jit(solution)/shard_map/ppermute | solution.py:352
  89.2 1.3 %collective-permute-start.12 = (bf16[160,512]{1,0:T(8,128)(2,1)S(1)}, bf16[160,512]{1,0:T(8,128)(2,1)S(1)}, u32[]{:S(2)}, u32[]{:S(2)}) collective-permute-start(bf16[160,512]{1,0:T(8,128)(2,1)S(1)} %get-tuple-element.46), channel_id=1, source_target_pairs={{0,12},{4,8},{8,4},{12,0},{16,28},{20,24},{24,20},{28,16},{1,13},{... | collective-permute-start | bytes 491528 | tf_op jit(solution)/shard_map/ppermute | solution.py:352
  90.5 2.6 %collective-permute-done.10.refs_1_ = bf16[160,512]{1,0:T(8,128)(2,1)S(1)} collective-permute-done((bf16[160,512]{1,0:T(8,128)(2,1)S(1)}, bf16[160,512]{1,0:T(8,128)(2,1)S(1)}, u32[]{:S(2)}, u32[]{:S(2)}) %collective-permute-start.10) | collective-permute-done | bytes 163872 | tf_op jit(solution)/shard_map/ppermute | solution.py:352
  93.1 3.2 %collective-permute-done.12.refs_3_ = bf16[160,512]{1,0:T(8,128)(2,1)S(1)} collective-permute-done((bf16[160,512]{1,0:T(8,128)(2,1)S(1)}, bf16[160,512]{1,0:T(8,128)(2,1)S(1)}, u32[]{:S(2)}, u32[]{:S(2)}) %collective-permute-start.12) | collective-permute-done | bytes 163872 | tf_op jit(solution)/shard_map/ppermute | solution.py:352
  96.2 2.1 %collective-permute-start.2 = (bf16[160,512]{1,0:T(8,128)(2,1)S(1)}, bf16[160,512]{1,0:T(8,128)(2,1)S(1)}, u32[]{:S(2)}, u32[]{:S(2)}) collective-permute-start(bf16[160,512]{1,0:T(8,128)(2,1)S(1)} %get-tuple-element.34), channel_id=1, source_target_pairs={{0,12},{4,8},{8,4},{12,0},{16,28},{20,24},{24,20},{28,16},{1,13},{... | collective-permute-start | bytes 491528 | tf_op jit(solution)/shard_map/ppermute | solution.py:352
  98.3 6.9 %attend.3 = (bf16[160,256]{1,0:T(8,128)(2,1)S(1)}, bf16[160,256]{1,0:T(8,128)(2,1)S(1)}, bf16[160,256]{1,0:T(8,128)(2,1)S(1)}, bf16[160,256]{1,0:T(8,128)(2,1)S(1)}) custom-call(bf16[160,512]{1,0:T(8,128)(2,1)S(1)} %get-tuple-element.43.refs_0_, bf16[160,512]{1,0:T(8,128)(2,1)S(1)} %collective-permute-done.10.refs_1_, ...), custom_call_target="tpu_custom_call" | custom-call | flops 838860800 | bytes 1966080 | tf_op jit(solution)/shard_map/attend/pallas_call | solution.py:277
  105.3 0.0 copy-start
  105.3 0.0 collective-permute-done.refs_1_
  105.3 0.1 collective-permute-start.17
  105.4 1.4 %collective-permute-start.18 = (bf16[160,256]{1,0:T(8,128)(2,1)S(1)}, bf16[160,256]{1,0:T(8,128)(2,1)S(1)}, u32[]{:S(2)}, u32[]{:S(2)}) collective-permute-start(bf16[160,256]{1,0:T(8,128)(2,1)S(1)} %get-tuple-element.53), channel_id=1, source_target_pairs={{0,8},{4,12},{8,0},{12,4},{16,24},{20,28},{24,16},{28,20},{1,9},{5... | collective-permute-start | bytes 245768 | tf_op jit(solution)/shard_map/ppermute | solution.py:352
  106.8 0.0 collective-permute-done.2.refs_3_
  106.8 2.1 %collective-permute-start.19 = (bf16[160,256]{1,0:T(8,128)(2,1)S(1)}, bf16[160,256]{1,0:T(8,128)(2,1)S(1)}, u32[]{:S(2)}, u32[]{:S(2)}) collective-permute-start(bf16[160,256]{1,0:T(8,128)(2,1)S(1)} %get-tuple-element.54), channel_id=1, source_target_pairs={{0,12},{4,8},{8,4},{12,0},{16,28},{20,24},{24,20},{28,16},{1,13},{... | collective-permute-start | bytes 245768 | tf_op jit(solution)/shard_map/ppermute | solution.py:352
  108.8 6.9 %attend.2 = (bf16[160,256]{1,0:T(8,128)(2,1)S(1)}, bf16[160,256]{1,0:T(8,128)(2,1)S(1)}, bf16[160,256]{1,0:T(8,128)(2,1)S(1)}, bf16[160,256]{1,0:T(8,128)(2,1)S(1)}) custom-call(bf16[160,512]{1,0:T(8,128)(2,1)S(1)} %get-tuple-element.31.refs_0_, bf16[160,512]{1,0:T(8,128)(2,1)S(1)} %collective-permute-done.refs_1_, ...), custom_call_target="tpu_custom_call" | custom-call | flops 838860800 | bytes 1966080 | tf_op jit(solution)/shard_map/attend/pallas_call | solution.py:277
  115.8 0.0 collective-permute-done.17.refs_5_
  115.8 0.2 collective-permute-start.7
  116.0 0.0 collective-permute-done.18.refs_6_
  116.0 1.3 %collective-permute-start.8 = (bf16[160,256]{1,0:T(8,128)(2,1)S(1)}, bf16[160,256]{1,0:T(8,128)(2,1)S(1)}, u32[]{:S(2)}, u32[]{:S(2)}) collective-permute-start(bf16[160,256]{1,0:T(8,128)(2,1)S(1)} %get-tuple-element.41), channel_id=1, source_target_pairs={{0,8},{4,12},{8,0},{12,4},{16,24},{20,28},{24,16},{28,20},{1,9},{5... | collective-permute-start | bytes 245768 | tf_op jit(solution)/shard_map/ppermute | solution.py:352
  117.3 2.1 %collective-permute-start.9 = (bf16[160,256]{1,0:T(8,128)(2,1)S(1)}, bf16[160,256]{1,0:T(8,128)(2,1)S(1)}, u32[]{:S(2)}, u32[]{:S(2)}) collective-permute-start(bf16[160,256]{1,0:T(8,128)(2,1)S(1)} %get-tuple-element.42), channel_id=1, source_target_pairs={{0,12},{4,8},{8,4},{12,0},{16,28},{20,24},{24,20},{28,16},{1,13},{... | collective-permute-start | bytes 245768 | tf_op jit(solution)/shard_map/ppermute | solution.py:352
  119.4 0.9 collective-permute-done.7.refs_1_
  120.3 0.1 collective-permute-done.8.refs_2_
  120.4 2.3 %collective-permute-done.9.refs_3_ = bf16[160,256]{1,0:T(8,128)(2,1)S(1)} collective-permute-done((bf16[160,256]{1,0:T(8,128)(2,1)S(1)}, bf16[160,256]{1,0:T(8,128)(2,1)S(1)}, u32[]{:S(2)}, u32[]{:S(2)}) %collective-permute-start.9) | collective-permute-done | bytes 81952 | tf_op jit(solution)/shard_map/ppermute | solution.py:352
  122.7 0.0 collective-permute-done.22.refs_9_
  122.7 0.8 project.2
  123.5 3.9 %project.3 = bf16[160,2048]{1,0:T(8,128)(2,1)} custom-call(bf16[160,256]{1,0:T(8,128)(2,1)S(1)} %get-tuple-element.39.refs_0_, bf16[160,256]{1,0:T(8,128)(2,1)S(1)} %collective-permute-done.7.refs_1_, bf16[160,256]{1,0:T(8,128)(2,1)S(1)} %collective-permute-done.8.refs_2_, bf16[160,256]{1,0:T(8,128)(2,1)S(1)} %collective-permute-done.9.refs_3_, ...), custom_call_target="tpu_custom_call" | custom-call | flops 671088640 | bytes 4194304 | tf_op jit(solution)/shard_map/project/pallas_call | solution.py:336
  (21 shorter events, 0.1 us)
Async XLA Ops:
  0.0 48.9 %collective-permute-start.20 = (bf16[2048,512]{1,0:T(8,128)(2,1)}, bf16[2048,512]{1,0:T(8,128)(2,1)}, u32[]{:S(2)}, u32[]{:S(2)}) collective-permute-start(bf16[2048,512]{1,0:T(8,128)(2,1)} %refs_8_.1), channel_id=1, source_target_pairs={{0,2},{1,3},{2,0},{3,1},{4,6},{5,7},{6,4},{7,5},{8,10},{9,11},{10,... | collective-permute-start | bytes 6291464 | tf_op jit(solution)/shard_map/ppermute | solution.py:352
  3.0 119.7 %collective-permute-start.22 = (bf16[2048,512]{1,0:T(8,128)(2,1)}, bf16[2048,512]{1,0:T(8,128)(2,1)S(1)}, u32[]{:S(2)}, u32[]{:S(2)}) collective-permute-start(bf16[2048,512]{1,0:T(8,128)(2,1)} %refs_8_.1), channel_id=1, source_target_pairs={{0,1},{1,0},{2,3},{3,2},{4,5},{5,4},{6,7},{7,6},{8,9},{9,8},{10,11... | collective-permute-start | bytes 6291464 | tf_op jit(solution)/shard_map/ppermute | solution.py:352
  48.9 74.6 %collective-permute-start.21 = (bf16[2048,512]{1,0:T(8,128)(2,1)}, bf16[2048,512]{1,0:T(8,128)(2,1)}, u32[]{:S(2)}, u32[]{:S(2)}) collective-permute-start(bf16[2048,512]{1,0:T(8,128)(2,1)} %collective-permute-done.20.refs_8_), channel_id=1, source_target_pairs={{0,1},{1,0},{2,3},{3,2},{4,5},{5,4},{6,7},{7,6},{8,9},{9,8},{10,11... | collective-permute-start | bytes 6291464 | tf_op jit(solution)/shard_map/ppermute | solution.py:352
  49.4 1.1 copy-start.1
  50.5 1.0 copy-start.2
  51.5 1.0 copy-start.3
  52.4 0.7 copy-start.4
  53.1 0.7 copy-start.5
  55.9 8.0 %collective-permute-start.13 = (bf16[160,256]{1,0:T(8,128)(2,1)S(1)}, bf16[160,256]{1,0:T(8,128)(2,1)S(1)}, u32[]{:S(2)}, u32[]{:S(2)}) collective-permute-start(bf16[160,256]{1,0:T(8,128)(2,1)S(1)} %get-tuple-element.47), channel_id=1, source_target_pairs={{0,16},{4,20},{8,24},{12,28},{16,0},{20,4},{24,8},{28,12},{1,17},{... | collective-permute-start | bytes 245768 | tf_op jit(solution)/shard_map/ppermute | solution.py:352
  58.8 12.9 %collective-permute-start.14 = (bf16[160,256]{1,0:T(8,128)(2,1)S(1)}, bf16[160,256]{1,0:T(8,128)(2,1)S(1)}, u32[]{:S(2)}, u32[]{:S(2)}) collective-permute-start(bf16[160,256]{1,0:T(8,128)(2,1)S(1)} %get-tuple-element.48), channel_id=1, source_target_pairs={{0,20},{4,16},{8,28},{12,24},{16,4},{20,0},{24,12},{28,8},{1,21},{... | collective-permute-start | bytes 245768 | tf_op jit(solution)/shard_map/ppermute | solution.py:352
  60.1 11.6 %collective-permute-start.15 = (bf16[160,256]{1,0:T(8,128)(2,1)S(1)}, bf16[160,256]{1,0:T(8,128)(2,1)S(1)}, u32[]{:S(2)}, u32[]{:S(2)}) collective-permute-start(bf16[160,256]{1,0:T(8,128)(2,1)S(1)} %get-tuple-element.49), channel_id=1, source_target_pairs={{0,24},{4,28},{8,16},{12,20},{16,8},{20,12},{24,0},{28,4},{1,25},{... | collective-permute-start | bytes 245768 | tf_op jit(solution)/shard_map/ppermute | solution.py:352
  63.8 10.7 %collective-permute-start.16 = (bf16[160,256]{1,0:T(8,128)(2,1)S(1)}, bf16[160,256]{1,0:T(8,128)(2,1)S(1)}, u32[]{:S(2)}, u32[]{:S(2)}) collective-permute-start(bf16[160,256]{1,0:T(8,128)(2,1)S(1)} %get-tuple-element.50), channel_id=1, source_target_pairs={{0,28},{4,24},{8,20},{12,16},{16,12},{20,8},{24,4},{28,0},{1,29},{... | collective-permute-start | bytes 245768 | tf_op jit(solution)/shard_map/ppermute | solution.py:352
  71.7 10.3 %collective-permute-start.3 = (bf16[160,256]{1,0:T(8,128)(2,1)S(1)}, bf16[160,256]{1,0:T(8,128)(2,1)S(1)}, u32[]{:S(2)}, u32[]{:S(2)}) collective-permute-start(bf16[160,256]{1,0:T(8,128)(2,1)S(1)} %get-tuple-element.35), channel_id=1, source_target_pairs={{0,16},{4,20},{8,24},{12,28},{16,0},{20,4},{24,8},{28,12},{1,17},{... | collective-permute-start | bytes 245768 | tf_op jit(solution)/shard_map/ppermute | solution.py:352
  71.7 13.2 %collective-permute-start.4 = (bf16[160,256]{1,0:T(8,128)(2,1)S(1)}, bf16[160,256]{1,0:T(8,128)(2,1)S(1)}, u32[]{:S(2)}, u32[]{:S(2)}) collective-permute-start(bf16[160,256]{1,0:T(8,128)(2,1)S(1)} %get-tuple-element.36), channel_id=1, source_target_pairs={{0,20},{4,16},{8,28},{12,24},{16,4},{20,0},{24,12},{28,8},{1,21},{... | collective-permute-start | bytes 245768 | tf_op jit(solution)/shard_map/ppermute | solution.py:352
  74.6 11.0 %collective-permute-start.5 = (bf16[160,256]{1,0:T(8,128)(2,1)S(1)}, bf16[160,256]{1,0:T(8,128)(2,1)S(1)}, u32[]{:S(2)}, u32[]{:S(2)}) collective-permute-start(bf16[160,256]{1,0:T(8,128)(2,1)S(1)} %get-tuple-element.37), channel_id=1, source_target_pairs={{0,24},{4,28},{8,16},{12,20},{16,8},{20,12},{24,0},{28,4},{1,25},{... | collective-permute-start | bytes 245768 | tf_op jit(solution)/shard_map/ppermute | solution.py:352
  82.0 7.2 %collective-permute-start.6 = (bf16[160,256]{1,0:T(8,128)(2,1)S(1)}, bf16[160,256]{1,0:T(8,128)(2,1)S(1)}, u32[]{:S(2)}, u32[]{:S(2)}) collective-permute-start(bf16[160,256]{1,0:T(8,128)(2,1)S(1)} %get-tuple-element.38), channel_id=1, source_target_pairs={{0,28},{4,24},{8,20},{12,16},{16,12},{20,8},{24,4},{28,0},{1,29},{... | collective-permute-start | bytes 245768 | tf_op jit(solution)/shard_map/ppermute | solution.py:352
  84.9 8.2 %collective-permute-start.10 = (bf16[160,512]{1,0:T(8,128)(2,1)S(1)}, bf16[160,512]{1,0:T(8,128)(2,1)S(1)}, u32[]{:S(2)}, u32[]{:S(2)}) collective-permute-start(bf16[160,512]{1,0:T(8,128)(2,1)S(1)} %get-tuple-element.44), channel_id=1, source_target_pairs={{0,4},{4,0},{8,12},{12,8},{16,20},{20,16},{24,28},{28,24},{1,5},{5... | collective-permute-start | bytes 491528 | tf_op jit(solution)/shard_map/ppermute | solution.py:352
  85.6 7.5 %collective-permute-start.11 = (bf16[160,512]{1,0:T(8,128)(2,1)S(1)}, bf16[160,512]{1,0:T(8,128)(2,1)S(1)}, u32[]{:S(2)}, u32[]{:S(2)}) collective-permute-start(bf16[160,512]{1,0:T(8,128)(2,1)S(1)} %get-tuple-element.45), channel_id=1, source_target_pairs={{0,8},{4,12},{8,0},{12,4},{16,24},{20,28},{24,16},{28,20},{1,9},{5... | collective-permute-start | bytes 491528 | tf_op jit(solution)/shard_map/ppermute | solution.py:352
  89.2 7.0 %collective-permute-start.12 = (bf16[160,512]{1,0:T(8,128)(2,1)S(1)}, bf16[160,512]{1,0:T(8,128)(2,1)S(1)}, u32[]{:S(2)}, u32[]{:S(2)}) collective-permute-start(bf16[160,512]{1,0:T(8,128)(2,1)S(1)} %get-tuple-element.46), channel_id=1, source_target_pairs={{0,12},{4,8},{8,4},{12,0},{16,28},{20,24},{24,20},{28,16},{1,13},{... | collective-permute-start | bytes 491528 | tf_op jit(solution)/shard_map/ppermute | solution.py:352
  93.1 12.2 %collective-permute-start = (bf16[160,512]{1,0:T(8,128)(2,1)S(1)}, bf16[160,512]{1,0:T(8,128)(2,1)S(1)}, u32[]{:S(2)}, u32[]{:S(2)}) collective-permute-start(bf16[160,512]{1,0:T(8,128)(2,1)S(1)} %get-tuple-element.32), channel_id=1, source_target_pairs={{0,4},{4,0},{8,12},{12,8},{16,20},{20,16},{24,28},{28,24},{1,5},{5... | collective-permute-start | bytes 491528 | tf_op jit(solution)/shard_map/ppermute | solution.py:352
  93.1 12.3 %collective-permute-start.1 = (bf16[160,512]{1,0:T(8,128)(2,1)S(1)}, bf16[160,512]{1,0:T(8,128)(2,1)S(1)}, u32[]{:S(2)}, u32[]{:S(2)}) collective-permute-start(bf16[160,512]{1,0:T(8,128)(2,1)S(1)} %get-tuple-element.33), channel_id=1, source_target_pairs={{0,8},{4,12},{8,0},{12,4},{16,24},{20,28},{24,16},{28,20},{1,9},{5... | collective-permute-start | bytes 491528 | tf_op jit(solution)/shard_map/ppermute | solution.py:352
  96.2 10.5 %collective-permute-start.2 = (bf16[160,512]{1,0:T(8,128)(2,1)S(1)}, bf16[160,512]{1,0:T(8,128)(2,1)S(1)}, u32[]{:S(2)}, u32[]{:S(2)}) collective-permute-start(bf16[160,512]{1,0:T(8,128)(2,1)S(1)} %get-tuple-element.34), channel_id=1, source_target_pairs={{0,12},{4,8},{8,4},{12,0},{16,28},{20,24},{24,20},{28,16},{1,13},{... | collective-permute-start | bytes 491528 | tf_op jit(solution)/shard_map/ppermute | solution.py:352
  105.3 17.4 %copy-start = (bf16[2048,512]{1,0:T(8,128)(2,1)S(1)}, bf16[2048,512]{1,0:T(8,128)(2,1)}, u32[]{:S(2)}) copy-start(bf16[2048,512]{1,0:T(8,128)(2,1)} %refs_8_.1) | copy-start | bytes 6291460
  105.3 10.5 %collective-permute-start.17 = (bf16[160,256]{1,0:T(8,128)(2,1)S(1)}, bf16[160,256]{1,0:T(8,128)(2,1)S(1)}, u32[]{:S(2)}, u32[]{:S(2)}) collective-permute-start(bf16[160,256]{1,0:T(8,128)(2,1)S(1)} %get-tuple-element.52), channel_id=1, source_target_pairs={{0,4},{4,0},{8,12},{12,8},{16,20},{20,16},{24,28},{28,24},{1,5},{5... | collective-permute-start | bytes 245768 | tf_op jit(solution)/shard_map/ppermute | solution.py:352
  105.4 10.6 %collective-permute-start.18 = (bf16[160,256]{1,0:T(8,128)(2,1)S(1)}, bf16[160,256]{1,0:T(8,128)(2,1)S(1)}, u32[]{:S(2)}, u32[]{:S(2)}) collective-permute-start(bf16[160,256]{1,0:T(8,128)(2,1)S(1)} %get-tuple-element.53), channel_id=1, source_target_pairs={{0,8},{4,12},{8,0},{12,4},{16,24},{20,28},{24,16},{28,20},{1,9},{5... | collective-permute-start | bytes 245768 | tf_op jit(solution)/shard_map/ppermute | solution.py:352
  106.8 10.5 %collective-permute-start.19 = (bf16[160,256]{1,0:T(8,128)(2,1)S(1)}, bf16[160,256]{1,0:T(8,128)(2,1)S(1)}, u32[]{:S(2)}, u32[]{:S(2)}) collective-permute-start(bf16[160,256]{1,0:T(8,128)(2,1)S(1)} %get-tuple-element.54), channel_id=1, source_target_pairs={{0,12},{4,8},{8,4},{12,0},{16,28},{20,24},{24,20},{28,16},{1,13},{... | collective-permute-start | bytes 245768 | tf_op jit(solution)/shard_map/ppermute | solution.py:352
  115.8 4.5 %collective-permute-start.7 = (bf16[160,256]{1,0:T(8,128)(2,1)S(1)}, bf16[160,256]{1,0:T(8,128)(2,1)S(1)}, u32[]{:S(2)}, u32[]{:S(2)}) collective-permute-start(bf16[160,256]{1,0:T(8,128)(2,1)S(1)} %get-tuple-element.40), channel_id=1, source_target_pairs={{0,4},{4,0},{8,12},{12,8},{16,20},{20,16},{24,28},{28,24},{1,5},{5... | collective-permute-start | bytes 245768 | tf_op jit(solution)/shard_map/ppermute | solution.py:352
  116.0 4.4 %collective-permute-start.8 = (bf16[160,256]{1,0:T(8,128)(2,1)S(1)}, bf16[160,256]{1,0:T(8,128)(2,1)S(1)}, u32[]{:S(2)}, u32[]{:S(2)}) collective-permute-start(bf16[160,256]{1,0:T(8,128)(2,1)S(1)} %get-tuple-element.41), channel_id=1, source_target_pairs={{0,8},{4,12},{8,0},{12,4},{16,24},{20,28},{24,16},{28,20},{1,9},{5... | collective-permute-start | bytes 245768 | tf_op jit(solution)/shard_map/ppermute | solution.py:352
  117.3 5.4 %collective-permute-start.9 = (bf16[160,256]{1,0:T(8,128)(2,1)S(1)}, bf16[160,256]{1,0:T(8,128)(2,1)S(1)}, u32[]{:S(2)}, u32[]{:S(2)}) collective-permute-start(bf16[160,256]{1,0:T(8,128)(2,1)S(1)} %get-tuple-element.42), channel_id=1, source_target_pairs={{0,12},{4,8},{8,4},{12,0},{16,28},{20,24},{24,20},{28,16},{1,13},{... | collective-permute-start | bytes 245768 | tf_op jit(solution)/shard_map/ppermute | solution.py:352
where the time goes:
time: 128 us; the launch traced here: 127 us
  waiting for transfers between devices  60.6 us (47%)
  starting transfers between devices  41.1 us (32%)
  Pallas kernels  20.8 us (16%)
  local copies, waits for them, and re-layouts  4.34 us (3%)
    ppermute x23, waiting for transfers between devices, exchanged(): return lax.ppermute(block, axis, [(i, i ^ flip) for i in range(count)])  60.6 us
    ppermute x23, starting transfers between devices, exchanged(): return lax.ppermute(block, axis, [(i, i ^ flip) for i in range(count)])  41.1 us
    pallas_call x2, Pallas kernels, attend(): pl.pallas_call(functools.partial(attend_kernel, groups), grid=(2,), in_sp...  13.9 us
    pallas_call x2, Pallas kernels, project(): pl.pallas_call(functools.partial(project_kernel, groups, chunks, early, l...  4.76 us
    unnamed x12, local copies, waits for them, and re-layouts  4.34 us
  transfers between devices with their start and end apart: 23, of which 9 were waited for; matrix products, arithmetic and copies ran while one was open for 0% of the time, Pallas kernels for 13%

commit v1 on v0

--- a/solution.py
+++ b/solution.py
@@ -218,7 +218,7 @@
         scratch_shapes=[pltpu.VMEM(x.shape, x.dtype) for x in (queries, keys, values)]
         + [pltpu.VMEM((1, HD), jnp.float32)] * 2
         + [pltpu.SemaphoreType.DMA((5,))],
-        compiler_params=params(16),
+        compiler_params=params(60),
         cost_estimate=pl.CostEstimate(flops=40 * 3072 * tok, bytes_accessed=6 * 4096 * tok, transcendentals=0),
         name="turn",
     )(queries, keys, values, q_gain[None], k_gain[None], cos_table, sin_table)
@@ -227,98 +227,126 @@
     return both, kv
 
 
-SOFT_ROWS = 16
-
-
-def attend_kernel(groups, *refs):
-    both_refs, far_refs, out_refs = refs[:groups], refs[groups : 2 * groups], refs[2 * groups : 3 * groups]
-    keys_scr, vals_scr, s_scr, w_scr = refs[3 * groups :]
-    rows = both_refs[0].shape[0]
+def spread_kernel(groups, *refs):
+    near_refs, far_refs, (keys_ref, vals_ref) = refs[:groups], refs[groups : 2 * groups], refs[2 * groups :]
+    rows = near_refs[0].shape[0]
     seq = 2 * groups * rows
-    pair = pl.program_id(0)
-    first = pair == 0
     low = lax.broadcasted_iota(jnp.int32, (rows, TILE), 1) < HD
-
-    def spread(tile, scr, i):
-        tile = tile.astype(jnp.float32)
-        other = pltpu.roll(tile, HD, 1)
-        here, there = jnp.where(first, tile, other), jnp.where(first, other, tile)
-        scr[i * rows : (i + 1) * rows, :] = jnp.where(low, here, 0.0).astype(jnp.bfloat16)
-        scr[seq + i * rows : seq + (i + 1) * rows, :] = jnp.where(low, 0.0, there).astype(jnp.bfloat16)
-
-    for i in range(groups):
-        spread(both_refs[i][:, 2 * TILE : 3 * TILE], keys_scr, i)
-        spread(both_refs[i][:, 3 * TILE :], vals_scr, i)
-        spread(far_refs[i][:, :TILE], keys_scr, groups + i)
-        spread(far_refs[i][:, TILE:], vals_scr, groups + i)
-
+    tiles = [(ref[:, 2 * TILE : 3 * TILE], ref[:, 3 * TILE :]) for ref in near_refs]
+    tiles += [(ref[:, :TILE], ref[:, TILE:]) for ref in far_refs]
+    for i, pair in enumerate(tiles):
+        for tile, out_ref in zip(pair, (keys_ref, vals_ref)):
+            tile = tile.astype(jnp.float32)
+            other = pltpu.roll(tile, HD, 1)
+            here = slice(i * rows, (i + 1) * rows)
+            there = slice(seq + i * rows, seq + (i + 1) * rows)
+            out_ref[0, here, :] = jnp.where(low, tile, 0.0).astype(jnp.bfloat16)
+            out_ref[0, there, :] = jnp.where(low, 0.0, other).astype(jnp.bfloat16)
+            out_ref[1, here, :] = jnp.where(low, other, 0.0).astype(jnp.bfloat16)
+            out_ref[1, there, :] = jnp.where(low, 0.0, tile).astype(jnp.bfloat16)
+
+
+def spread(near, far):
+    groups, rows = len(near), near[0].shape[0]
+    made = jax.ShapeDtypeStruct((2, GROUP * 2 * groups * rows, TILE), jnp.bfloat16)
+    return pl.pallas_call(
+        functools.partial(spread_kernel, groups),
+        in_specs=in_vmem(2 * groups),
+        out_specs=in_vmem(2),
+        out_shape=[made] * 2,
+        compiler_params=params(16),
+        cost_estimate=pl.CostEstimate(flops=1 << 22, bytes_accessed=1 << 22, transcendentals=0),
+        name="spread",
+    )(*near, *far)
+
+
+SOFT_ROWS = 8
+
+
+def attend_kernel(count, *refs):
+    query_refs, (keys_ref, vals_ref), out_refs = refs[:count], refs[count : count + 2], refs[count + 2 : -2]
+    s_scr, w_scr = refs[-2:]
+    rows = query_refs[0].shape[0]
+    seq = keys_ref.shape[1] // GROUP
     factor = HD ** (-0.5) * 1.4426950408889634
-    lanes = pl.ds(pl.multiple_of(pair * TILE, TILE), TILE)
-    for j in range(groups):
-        slot = j % 2
-        s_scr[slot] = lax.dot_general(
-            both_refs[j][:, lanes], keys_scr[...], (((1,), (1,)), ((), ())), preferred_element_type=jnp.float32
+
+    def scores(p):
+        query = jnp.concatenate([ref[:, p * TILE : (p + 1) * TILE] for ref in query_refs], axis=0)
+        s_scr[p] = lax.dot_general(
+            query, keys_ref[p], (((1,), (1,)), ((), ())), preferred_element_type=jnp.float32
         )
+
+    scores(0)
+    for p in range(2):
+        if p == 0:
+            scores(1)
         for g in range(GROUP):
-            for r in range(0, rows, SOFT_ROWS):
-                s = s_scr[slot, r : r + SOFT_ROWS, g * seq : (g + 1) * seq]
+            for r in range(0, count * rows, SOFT_ROWS):
+                s = s_scr[p, r : r + SOFT_ROWS, g * seq : (g + 1) * seq]
                 e = jnp.exp2((s - jnp.max(s, axis=-1, keepdims=True)) * factor)
                 w = e * (1.0 / jnp.sum(e, axis=-1, keepdims=True))
-                w_scr[slot, r : r + SOFT_ROWS, g * seq : (g + 1) * seq] = w.astype(jnp.bfloat16)
-        out_refs[j][:, lanes] = jnp.dot(
-            w_scr[slot], vals_scr[...], preferred_element_type=jnp.float32
-        ).astype(jnp.bfloat16)
-
-
-def attend(both, far):
-    groups = len(both)
-    rows = both[0].shape[0]
-    seq = 2 * groups * rows
+                w_scr[p, r : r + SOFT_ROWS, g * seq : (g + 1) * seq] = w.astype(jnp.bfloat16)
+        attended = jnp.dot(w_scr[p], vals_ref[p], preferred_element_type=jnp.float32).astype(jnp.bfloat16)
+        for i, out_ref in enumerate(out_refs):
+            out_ref[:, p * TILE : (p + 1) * TILE] = attended[i * rows : (i + 1) * rows]
+
+
+def attend(near, keys, vals):
+    count, rows = len(near), near[0].shape[0]
+    wide = keys.shape[1]
     return pl.pallas_call(
-        functools.partial(attend_kernel, groups),
-        grid=(2,),
-        in_specs=in_vmem(2 * groups),
-        out_specs=in_vmem(groups),
-        out_shape=[jax.ShapeDtypeStruct((rows, 2 * TILE), jnp.bfloat16)] * groups,
+        functools.partial(attend_kernel, count),
+        in_specs=in_vmem(count + 2),
+        out_specs=in_vmem(count),
+        out_shape=[jax.ShapeDtypeStruct((rows, 2 * TILE), jnp.bfloat16)] * count,
         scratch_shapes=[
-            pltpu.VMEM((GROUP * seq, TILE), jnp.bfloat16),
-            pltpu.VMEM((GROUP * seq, TILE), jnp.bfloat16),
-            pltpu.VMEM((2, rows, GROUP * seq), jnp.float32),
-            pltpu.VMEM((2, rows, GROUP * seq), jnp.bfloat16),
+            pltpu.VMEM((2, count * rows, wide), jnp.float32),
+            pltpu.VMEM((2, count * rows, wide), jnp.bfloat16),
         ],
         compiler_params=params(24),
         cost_estimate=pl.CostEstimate(
-            flops=16 * groups * rows * seq * HD, bytes_accessed=12 * seq * TILE, transcendentals=0
+            flops=8 * count * rows * wide * TILE, bytes_accessed=8 * wide * TILE, transcendentals=0
         ),
         name="attend",
-    )(*both, *far)
+    )(*near, keys, vals)
 
 
 def project_kernel(groups, chunks, early, late, *refs):
     att_refs, refs = refs[: groups * chunks], refs[groups * chunks :]
+    bufs, sems = refs[-2:]
     home = lax.axis_index("sp") % groups
-
-    def product(w_ref):
+    which = early if late is None else late
+    w_refs = refs[: len(which)]
+    deep = chunks * 2 * TILE
+    row = lambda j: pl.ds(pl.multiple_of((home ^ j) * deep, deep), deep)
+    copies = [
+        [pltpu.make_async_copy(w_ref.at[row(j), :], bufs.at[i, j], sems.at[i, j]) for j in range(groups)]
+        for i, w_ref in enumerate(w_refs)
+    ]
+    for copy in sum(copies, []):
+        copy.start()
+    parts = [jnp.concatenate([att_refs[c * groups + j][...] for c in range(chunks)], axis=1) for j in range(groups)]
+
+    def product(i):
         total = None
-        for c in range(chunks):
-            for j in range(groups):
-                row = pl.ds(pl.multiple_of(((home ^ j) * chunks + c) * 2 * TILE, 2 * TILE), 2 * TILE)
-                term = jnp.dot(att_refs[c * groups + j][...], w_ref[row, :], preferred_element_type=jnp.float32)
-                total = term if total is None else total + term
+        for j in range(groups):
+            copies[i][j].wait()
+            term = jnp.dot(parts[j], bufs[i, j], preferred_element_type=jnp.float32)
+            total = term if total is None else total + term
         return total.astype(jnp.bfloat16)
 
     if late is None:
-        for i, w_ref, out_ref in zip(early, refs[: len(early)], refs[len(early) :]):
-            out_ref[...] = product(w_ref)
+        for i, out_ref in enumerate(refs[len(which) : -2]):
+            out_ref[...] = product(i)
         return
     me = lax.axis_index("dp")
-    w_refs, early_refs, out_ref = refs[: len(late)], refs[len(late) : -1], refs[-1]
+    early_refs, out_ref = refs[len(which) : -3], refs[-3]
     width = w_refs[0].shape[1]
     column = lambda i: pl.ds(pl.multiple_of((me ^ i) * width, width), width)
     for i, early_ref in zip(early, early_refs):
         out_ref[:, column(i)] = early_ref[...]
-    for i, w_ref in zip(late, w_refs):
-        out_ref[:, column(i)] = product(w_ref)
+    for n, i in enumerate(late):
+        out_ref[:, column(i)] = product(n)
 
 
 def project(attended, blocks, early, late=None, made=()):
@@ -335,9 +363,13 @@
         out_specs = pl.BlockSpec(memory_space=pltpu.VMEM)
     return pl.pallas_call(
         functools.partial(project_kernel, groups, chunks, early, late),
-        in_specs=in_vmem(len(flat) + len(which) + len(made)),
+        in_specs=in_vmem(len(flat)) + [pl.BlockSpec(memory_space=pl.ANY)] * len(which) + in_vmem(len(made)),
         out_specs=out_specs,
         out_shape=out_shape,
+        scratch_shapes=[
+            pltpu.VMEM((len(which), groups, depth // groups, width), jnp.bfloat16),
+            pltpu.SemaphoreType.DMA((len(which), groups)),
+        ],
         compiler_params=params(16),
         cost_estimate=pl.CostEstimate(
             flops=2 * tok * depth * width * len(which), bytes_accessed=2 * depth * width * len(which),
@@ -366,6 +398,7 @@
             for key in list(listed):
                 blocks[key | 1 << bit] = exchanged(blocks[key], "dp", 1 << bit)
                 listed.append(key | 1 << bit)
+    early, late = early + late[:1], late[1:]
     cos_table, sin_table = rotary_lanes(lax.axis_index("sp") * tok, tok)
     both, kv = turn_and_pack(queries[0].T, keys[0].T, values[0].T, q_gain, k_gain, cos_table, sin_table, groups, chunks)
     near, far = [], []
@@ -374,8 +407,13 @@
         far.append([exchanged(kv[c][j], "sp", groups + j) for j in range(groups)])
     back = []
     for c in range(chunks):
-        done = attend(near[c], far[c])
-        back.append([done[0]] + [exchanged(done[j], "sp", j) for j in range(1, groups)])
+        ready = spread(near[c], far[c])
+        got = [None] * groups
+        for first in reversed(range(0, groups, 2)):
+            done = attend(near[c][first : first + 2], *ready)
+            for j in (first + 1, first):
+                got[j] = exchanged(done[j - first], "sp", j) if j else done[0]
+        back.append(got)
     listed = [blocks[i] for i in range(dp_count)]
     made = project(back, listed, early)
     mixed = project(back, listed, early, late, made)

time: 128 us -> 126 us (0.984)
  local copies, waits for them, and re-layouts: 4.34 us -> 0.93 us
    unnamed x12 -> x8, local copies, waits for them, and re-layouts: 4.34 us -> 0.93 us
    pallas_call x2 -> x6, Pallas kernels: 13.9 us -> 11.2 us  [the longest x4 10.4 us: attend(): pl.pallas_call(functools.partial(attend_kernel, count), in_specs=in_vmem(...]
    pallas_call x1, Pallas kernels: 2.13 us -> 4.7 us  [turn_and_pack(): pl.pallas_call(functools.partial(turn_kernel, groups, chunks), in_specs=[...]
  transfers between devices with their start and end apart: 23 -> 23, of which waited for: 9 -> 10; matrix products, arithmetic and copies ran while one was open for 0% -> 1% of each run, Pallas kernels for 13% -> 15%
where the time goes in v1:
time: 126 us
  waiting for transfers between devices  60.6 us (48%)
  starting transfers between devices  41.4 us (33%)
  Pallas kernels  21.3 us (17%)
    ppermute x23, waiting for transfers between devices, exchanged(): return lax.ppermute(block, axis, [(i, i ^ flip) for i in range(count)])  60.6 us
    ppermute x23, starting transfers between devices, exchanged(): return lax.ppermute(block, axis, [(i, i ^ flip) for i in range(count)])  41.4 us
    pallas_call x4, Pallas kernels, attend(): pl.pallas_call(functools.partial(attend_kernel, count), in_specs=in_vmem(...  10.4 us
    pallas_call x2, Pallas kernels, project(): pl.pallas_call(functools.partial(project_kernel, groups, chunks, early, l...  5.43 us
    pallas_call x1, Pallas kernels, turn_and_pack(): pl.pallas_call(functools.partial(turn_kernel, groups, chunks), in_specs=[...  4.7 us
  transfers between devices with their start and end apart: 23, of which 10 were waited for; matrix products, arithmetic and copies ran while one was open for 1% of the time, Pallas kernels for 15%

profile of v1, /device:TPU:0, one launch (start us, length us, event | category | flops | bytes accessed | tf_op | source)
XLA Modules:
  0.0 125.6 jit_solution(567764189400351210)
XLA Ops:
  0.0 3.0 %collective-permute-start.20 = (bf16[2048,512]{1,0:T(8,128)(2,1)}, bf16[2048,512]{1,0:T(8,128)(2,1)S(1)}, u32[]{:S(2)}, u32[]{:S(2)}) collective-permute-start(bf16[2048,512]{1,0:T(8,128)(2,1)} %refs_8_.1), channel_id=1, source_target_pairs={{0,2},{1,3},{2,0},{3,1},{4,6},{5,7},{6,4},{7,5},{8,10},{9,11},{10,... | collective-permute-start | bytes 6291464 | tf_op jit(solution)/shard_map/ppermute | solution.py:384
  3.0 45.8 %collective-permute-done.20.refs_10_ = bf16[2048,512]{1,0:T(8,128)(2,1)S(1)} collective-permute-done((bf16[2048,512]{1,0:T(8,128)(2,1)}, bf16[2048,512]{1,0:T(8,128)(2,1)S(1)}, u32[]{:S(2)}, u32[]{:S(2)}) %collective-permute-start.20) | collective-permute-done | bytes 2097184 | tf_op jit(solution)/shard_map/ppermute | solution.py:384
  48.9 1.1 negate_select_fusion
  49.9 4.7 %turn.1 = (bf16[160,512]{1,0:T(8,128)(2,1)}, bf16[160,512]{1,0:T(8,128)(2,1)}, bf16[160,512]{1,0:T(8,128)(2,1)}, bf16[160,512]{1,0:T(8,128)(2,1)}, bf16[160,512]...) custom-call(bf16[160,2048]{1,0:T(8,128)(2,1)} %bitcast.12, ...), custom_call_target="tpu_custom_call" | custom-call | flops 19660800 | bytes 3932160 | tf_op jit(solution)/shard_map/turn/pallas_call | solution.py:212
  54.7 2.9 %collective-permute-start.13 = (bf16[160,256]{1,0:T(8,128)(2,1)}, bf16[160,256]{1,0:T(8,128)(2,1)S(1)}, u32[]{:S(2)}, u32[]{:S(2)}) collective-permute-start(bf16[160,256]{1,0:T(8,128)(2,1)} %get-tuple-element.54), channel_id=1, source_target_pairs={{0,16},{4,20},{8,24},{12,28},{16,0},{20,4},{24,8},{28,12},{1,17},{... | collective-permute-start | bytes 245768 | tf_op jit(solution)/shard_map/ppermute | solution.py:384
  57.6 1.3 %collective-permute-start.14 = (bf16[160,256]{1,0:T(8,128)(2,1)}, bf16[160,256]{1,0:T(8,128)(2,1)S(1)}, u32[]{:S(2)}, u32[]{:S(2)}) collective-permute-start(bf16[160,256]{1,0:T(8,128)(2,1)} %get-tuple-element.55), channel_id=1, source_target_pairs={{0,20},{4,16},{8,28},{12,24},{16,4},{20,0},{24,12},{28,8},{1,21},{... | collective-permute-start | bytes 245768 | tf_op jit(solution)/shard_map/ppermute | solution.py:384
  58.9 3.6 %collective-permute-start.15 = (bf16[160,256]{1,0:T(8,128)(2,1)}, bf16[160,256]{1,0:T(8,128)(2,1)S(1)}, u32[]{:S(2)}, u32[]{:S(2)}) collective-permute-start(bf16[160,256]{1,0:T(8,128)(2,1)} %get-tuple-element.56), channel_id=1, source_target_pairs={{0,24},{4,28},{8,16},{12,20},{16,8},{20,12},{24,0},{28,4},{1,25},{... | collective-permute-start | bytes 245768 | tf_op jit(solution)/shard_map/ppermute | solution.py:384
  62.4 0.4 collective-permute-done.13.refs_4_
  62.8 7.9 %collective-permute-start.16 = (bf16[160,256]{1,0:T(8,128)(2,1)}, bf16[160,256]{1,0:T(8,128)(2,1)S(1)}, u32[]{:S(2)}, u32[]{:S(2)}) collective-permute-start(bf16[160,256]{1,0:T(8,128)(2,1)} %get-tuple-element.57), channel_id=1, source_target_pairs={{0,28},{4,24},{8,20},{12,16},{16,12},{20,8},{24,4},{28,0},{1,29},{... | collective-permute-start | bytes 245768 | tf_op jit(solution)/shard_map/ppermute | solution.py:384
  70.7 0.0 collective-permute-done.15.refs_6_
  70.7 2.9 %collective-permute-start.4 = (bf16[160,256]{1,0:T(8,128)(2,1)}, bf16[160,256]{1,0:T(8,128)(2,1)S(1)}, u32[]{:S(2)}, u32[]{:S(2)}) collective-permute-start(bf16[160,256]{1,0:T(8,128)(2,1)} %get-tuple-element.41), channel_id=1, source_target_pairs={{0,20},{4,16},{8,28},{12,24},{16,4},{20,0},{24,12},{28,8},{1,21},{... | collective-permute-start | bytes 245768 | tf_op jit(solution)/shard_map/ppermute | solution.py:384
  73.6 0.3 collective-permute-done.16.refs_7_
  73.9 4.1 %collective-permute-start.5 = (bf16[160,256]{1,0:T(8,128)(2,1)}, bf16[160,256]{1,0:T(8,128)(2,1)S(1)}, u32[]{:S(2)}, u32[]{:S(2)}) collective-permute-start(bf16[160,256]{1,0:T(8,128)(2,1)} %get-tuple-element.42), channel_id=1, source_target_pairs={{0,24},{4,28},{8,16},{12,20},{16,8},{20,12},{24,0},{28,4},{1,25},{... | collective-permute-start | bytes 245768 | tf_op jit(solution)/shard_map/ppermute | solution.py:384
  78.0 3.2 %collective-permute-done.3.refs_4_ = bf16[160,256]{1,0:T(8,128)(2,1)S(1)} collective-permute-done((bf16[160,256]{1,0:T(8,128)(2,1)}, bf16[160,256]{1,0:T(8,128)(2,1)S(1)}, u32[]{:S(2)}, u32[]{:S(2)}) %collective-permute-start.3) | collective-permute-done | bytes 81952 | tf_op jit(solution)/shard_map/ppermute | solution.py:384
  81.2 2.7 %collective-permute-start.6 = (bf16[160,256]{1,0:T(8,128)(2,1)}, bf16[160,256]{1,0:T(8,128)(2,1)S(1)}, u32[]{:S(2)}, u32[]{:S(2)}) collective-permute-start(bf16[160,256]{1,0:T(8,128)(2,1)} %get-tuple-element.43), channel_id=1, source_target_pairs={{0,28},{4,24},{8,20},{12,16},{16,12},{20,8},{24,4},{28,0},{1,29},{... | collective-permute-start | bytes 245768 | tf_op jit(solution)/shard_map/ppermute | solution.py:384
  83.9 0.9 collective-permute-start.10
  84.8 1.4 %collective-permute-start.11 = (bf16[160,512]{1,0:T(8,128)(2,1)}, bf16[160,512]{1,0:T(8,128)(2,1)S(1)}, u32[]{:S(2)}, u32[]{:S(2)}) collective-permute-start(bf16[160,512]{1,0:T(8,128)(2,1)} %get-tuple-element.52), channel_id=1, source_target_pairs={{0,8},{4,12},{8,0},{12,4},{16,24},{20,28},{24,16},{28,20},{1,9},{5... | collective-permute-start | bytes 491528 | tf_op jit(solution)/shard_map/ppermute | solution.py:384
  86.1 2.5 %collective-permute-done.6.refs_7_ = bf16[160,256]{1,0:T(8,128)(2,1)S(1)} collective-permute-done((bf16[160,256]{1,0:T(8,128)(2,1)}, bf16[160,256]{1,0:T(8,128)(2,1)S(1)}, u32[]{:S(2)}, u32[]{:S(2)}) %collective-permute-start.6) | collective-permute-done | bytes 81952 | tf_op jit(solution)/shard_map/ppermute | solution.py:384
  88.6 1.0 collective-permute-start.12
  89.7 2.3 %collective-permute-done.10.refs_1_ = bf16[160,512]{1,0:T(8,128)(2,1)S(1)} collective-permute-done((bf16[160,512]{1,0:T(8,128)(2,1)}, bf16[160,512]{1,0:T(8,128)(2,1)S(1)}, u32[]{:S(2)}, u32[]{:S(2)}) %collective-permute-start.10) | collective-permute-done | bytes 163872 | tf_op jit(solution)/shard_map/ppermute | solution.py:384
  92.0 0.2 collective-permute-start
  92.1 0.2 collective-permute-start.1
  92.4 3.2 %collective-permute-done.12.refs_3_.refs_1_ = bf16[160,512]{1,0:T(8,128)(2,1)S(1)} collective-permute-done((bf16[160,512]{1,0:T(8,128)(2,1)}, bf16[160,512]{1,0:T(8,128)(2,1)S(1)}, u32[]{:S(2)}, u32[]{:S(2)}) %collective-permute-start.12) | collective-permute-done | bytes 163872 | tf_op jit(solution)/shard_map/ppermute | solution.py:384
  95.6 2.3 %collective-permute-start.2 = (bf16[160,512]{1,0:T(8,128)(2,1)}, bf16[160,512]{1,0:T(8,128)(2,1)S(1)}, u32[]{:S(2)}, u32[]{:S(2)}) collective-permute-start(bf16[160,512]{1,0:T(8,128)(2,1)} %get-tuple-element.39), channel_id=1, source_target_pairs={{0,12},{4,8},{8,4},{12,0},{16,28},{20,24},{24,20},{28,16},{1,13},{... | collective-permute-start | bytes 491528 | tf_op jit(solution)/shard_map/ppermute | solution.py:384
  97.9 0.9 copy-done.2
  98.8 0.4 spread.3
  99.2 2.6 %attend.7 = (bf16[160,256]{1,0:T(8,128)(2,1)S(1)}, bf16[160,256]{1,0:T(8,128)(2,1)S(1)}) custom-call(bf16[160,512]{1,0:T(8,128)(2,1)S(1)} %collective-permute-done.11.refs_2_.refs_0_, bf16[160,512]{1,0:T(8,128)(2,1)S(1)} %collective-permute-done.12.refs_3_.refs_1_, bf16[2,2560,128]{2,1,0:T(8,128)(2,1)S(1)} %get-tuple-element.58.refs_2_, ...), custom_call_target="tpu_custom_call" | custom-call | flops 838860800 | bytes 2621440 | tf_op jit(solution)/shard_map/attend/pallas_call | solution.py:297
  101.7 0.0 copy-start.1
  101.7 2.6 %attend.6 = (bf16[160,256]{1,0:T(8,128)(2,1)S(1)}, bf16[160,256]{1,0:T(8,128)(2,1)S(1)}) custom-call(bf16[160,512]{1,0:T(8,128)(2,1)S(1)} %copy-done.3, bf16[160,512]{1,0:T(8,128)(2,1)S(1)} %collective-permute-done.10.refs_1_, bf16[2,2560,128]{2,1,0:T(8,128)(2,1)S(1)} %get-tuple-element.58.refs_2_, bf16[2,2560,128]{2,1,0:T(8,128)(2,1)S(1)} %get-tuple-element.59.refs_3_), custom_call_target="tpu_custom_call" | custom-call | flops 838860800 | bytes 2621440 | tf_op jit(solution)/shard_map/attend/pallas_call | solution.py:297
  104.3 0.1 collective-permute-start.18
  104.4 0.0 collective-permute-done.1.refs_2_.refs_0_
  104.4 1.1 collective-permute-start.19
  105.5 0.0 collective-permute-done.2.refs_3_.refs_1_
  105.5 2.3 %collective-permute-start.17 = (bf16[160,256]{1,0:T(8,128)(2,1)S(1)}, bf16[160,256]{1,0:T(8,128)(2,1)S(1)}, u32[]{:S(2)}, u32[]{:S(2)}) collective-permute-start(bf16[160,256]{1,0:T(8,128)(2,1)S(1)} %get-tuple-element.61), channel_id=1, source_target_pairs={{0,4},{4,0},{8,12},{12,8},{16,20},{20,16},{24,28},{28,24},{1,5},{5... | collective-permute-start | bytes 245768 | tf_op jit(solution)/shard_map/ppermute | solution.py:384
  107.9 0.4 spread.2
  108.3 2.6 %attend.5 = (bf16[160,256]{1,0:T(8,128)(2,1)S(1)}, bf16[160,256]{1,0:T(8,128)(2,1)S(1)}) custom-call(bf16[160,512]{1,0:T(8,128)(2,1)S(1)} %collective-permute-done.1.refs_2_.refs_0_, bf16[160,512]{1,0:T(8,128)(2,1)S(1)} %collective-permute-done.2.refs_3_.refs_1_, bf16[2,2560,128]{2,1,0:T(8,128)(2,1)S(1)} %get-tuple-element.44.refs_2_, ...), custom_call_target="tpu_custom_call" | custom-call | flops 838860800 | bytes 2621440 | tf_op jit(solution)/shard_map/attend/pallas_call | solution.py:297
  110.8 0.0 copy-start
  110.8 2.8 %attend.4 = (bf16[160,256]{1,0:T(8,128)(2,1)S(1)}, bf16[160,256]{1,0:T(8,128)(2,1)S(1)}) custom-call(bf16[160,512]{1,0:T(8,128)(2,1)S(1)} %copy-done.1, bf16[160,512]{1,0:T(8,128)(2,1)S(1)} %collective-permute-done.refs_1_, bf16[2,2560,128]{2,1,0:T(8,128)(2,1)S(1)} %get-tuple-element.44.refs_2_, bf16[2,2560,128]{2,1,0:T(8,128)(2,1)S(1)} %get-tuple-element.45.refs_3_), custom_call_target="tpu_custom_call" | custom-call | flops 838860800 | bytes 2621440 | tf_op jit(solution)/shard_map/attend/pallas_call | solution.py:297
  113.6 0.1 collective-permute-start.8
  113.7 1.4 %collective-permute-start.9 = (bf16[160,256]{1,0:T(8,128)(2,1)S(1)}, bf16[160,256]{1,0:T(8,128)(2,1)S(1)}, u32[]{:S(2)}, u32[]{:S(2)}) collective-permute-start(bf16[160,256]{1,0:T(8,128)(2,1)S(1)} %get-tuple-element.49), channel_id=1, source_target_pairs={{0,12},{4,8},{8,4},{12,0},{16,28},{20,24},{24,20},{28,16},{1,13},{... | collective-permute-start | bytes 245768 | tf_op jit(solution)/shard_map/ppermute | solution.py:384
  115.1 0.0 collective-permute-done.17.refs_5_
  115.1 2.0 %collective-permute-start.7 = (bf16[160,256]{1,0:T(8,128)(2,1)S(1)}, bf16[160,256]{1,0:T(8,128)(2,1)S(1)}, u32[]{:S(2)}, u32[]{:S(2)}) collective-permute-start(bf16[160,256]{1,0:T(8,128)(2,1)S(1)} %get-tuple-element.47), channel_id=1, source_target_pairs={{0,4},{4,0},{8,12},{12,8},{16,20},{20,16},{24,28},{28,24},{1,5},{5... | collective-permute-start | bytes 245768 | tf_op jit(solution)/shard_map/ppermute | solution.py:384
  117.2 0.9 collective-permute-done.8.refs_2_
  118.1 1.0 collective-permute-done.9.refs_3_
  119.1 0.8 collective-permute-done.7.refs_1_
  120.0 0.0 collective-permute-done.22.refs_9_
  120.0 2.7 %project.2 = (bf16[160,512]{1,0:T(8,128)(2,1)S(1)}, bf16[160,512]{1,0:T(8,128)(2,1)S(1)}, bf16[160,512]{1,0:T(8,128)(2,1)S(1)}) custom-call(bf16[160,256]{1,0:T(8,128)(2,1)S(1)} %get-tuple-element.46.refs_0_, bf16[160,256]{1,0:T(8,128)(2,1)S(1)} %collective-permute-done.7.refs_1_, bf16[160,256]{1,0:T(8,128)(2,1)S(1)} %collective-permute-done.8.refs_2_, ...), custom_call_target="tpu_custom_call" | custom-call | flops 1006632960 | bytes 6291456 | tf_op jit(solution)/shard_map/project/pallas_call | solution.py:364
  122.7 2.7 %project.3 = bf16[160,2048]{1,0:T(8,128)(2,1)} custom-call(bf16[160,256]{1,0:T(8,128)(2,1)S(1)} %get-tuple-element.46.refs_0_, bf16[160,256]{1,0:T(8,128)(2,1)S(1)} %collective-permute-done.7.refs_1_, bf16[160,256]{1,0:T(8,128)(2,1)S(1)} %collective-permute-done.8.refs_2_, bf16[160,256]{1,0:T(8,128)(2,1)S(1)} %collective-permute-done.9.refs_3_, ...), custom_call_target="tpu_custom_call" | custom-call | flops 335544320 | bytes 2097152 | tf_op jit(solution)/shard_map/project/pallas_call | solution.py:364
  (21 shorter events, 0.1 us)
Async XLA Ops:
  0.0 48.8 %collective-permute-start.20 = (bf16[2048,512]{1,0:T(8,128)(2,1)}, bf16[2048,512]{1,0:T(8,128)(2,1)S(1)}, u32[]{:S(2)}, u32[]{:S(2)}) collective-permute-start(bf16[2048,512]{1,0:T(8,128)(2,1)} %refs_8_.1), channel_id=1, source_target_pairs={{0,2},{1,3},{2,0},{3,1},{4,6},{5,7},{6,4},{7,5},{8,10},{9,11},{10,... | collective-permute-start | bytes 6291464 | tf_op jit(solution)/shard_map/ppermute | solution.py:384
  3.0 117.0 %collective-permute-start.22 = (bf16[2048,512]{1,0:T(8,128)(2,1)}, bf16[2048,512]{1,0:T(8,128)(2,1)}, u32[]{:S(2)}, u32[]{:S(2)}) collective-permute-start(bf16[2048,512]{1,0:T(8,128)(2,1)} %refs_8_.1), channel_id=1, source_target_pairs={{0,1},{1,0},{2,3},{3,2},{4,5},{5,4},{6,7},{7,6},{8,9},{9,8},{10,11... | collective-permute-start | bytes 6291464 | tf_op jit(solution)/shard_map/ppermute | solution.py:384
  48.8 73.9 %collective-permute-start.21 = (bf16[2048,512]{1,0:T(8,128)(2,1)S(1)}, bf16[2048,512]{1,0:T(8,128)(2,1)}, u32[]{:S(2)}, u32[]{:S(2)}) collective-permute-start(bf16[2048,512]{1,0:T(8,128)(2,1)S(1)} %collective-permute-done.20.refs_10_), channel_id=1, source_target_pairs={{0,1},{1,0},{2,3},{3,2},{4,5},{5,4},{6,7},{7,6},{8,9},{9,8},{10,11... | collective-permute-start | bytes 6291464 | tf_op jit(solution)/shard_map/ppermute | solution.py:384
  54.7 8.2 %collective-permute-start.13 = (bf16[160,256]{1,0:T(8,128)(2,1)}, bf16[160,256]{1,0:T(8,128)(2,1)S(1)}, u32[]{:S(2)}, u32[]{:S(2)}) collective-permute-start(bf16[160,256]{1,0:T(8,128)(2,1)} %get-tuple-element.54), channel_id=1, source_target_pairs={{0,16},{4,20},{8,24},{12,28},{16,0},{20,4},{24,8},{28,12},{1,17},{... | collective-permute-start | bytes 245768 | tf_op jit(solution)/shard_map/ppermute | solution.py:384
  57.6 13.1 %collective-permute-start.14 = (bf16[160,256]{1,0:T(8,128)(2,1)}, bf16[160,256]{1,0:T(8,128)(2,1)S(1)}, u32[]{:S(2)}, u32[]{:S(2)}) collective-permute-start(bf16[160,256]{1,0:T(8,128)(2,1)} %get-tuple-element.55), channel_id=1, source_target_pairs={{0,20},{4,16},{8,28},{12,24},{16,4},{20,0},{24,12},{28,8},{1,21},{... | collective-permute-start | bytes 245768 | tf_op jit(solution)/shard_map/ppermute | solution.py:384
  58.9 11.8 %collective-permute-start.15 = (bf16[160,256]{1,0:T(8,128)(2,1)}, bf16[160,256]{1,0:T(8,128)(2,1)S(1)}, u32[]{:S(2)}, u32[]{:S(2)}) collective-permute-start(bf16[160,256]{1,0:T(8,128)(2,1)} %get-tuple-element.56), channel_id=1, source_target_pairs={{0,24},{4,28},{8,16},{12,20},{16,8},{20,12},{24,0},{28,4},{1,25},{... | collective-permute-start | bytes 245768 | tf_op jit(solution)/shard_map/ppermute | solution.py:384
  62.8 11.0 %collective-permute-start.16 = (bf16[160,256]{1,0:T(8,128)(2,1)}, bf16[160,256]{1,0:T(8,128)(2,1)S(1)}, u32[]{:S(2)}, u32[]{:S(2)}) collective-permute-start(bf16[160,256]{1,0:T(8,128)(2,1)} %get-tuple-element.57), channel_id=1, source_target_pairs={{0,28},{4,24},{8,20},{12,16},{16,12},{20,8},{24,4},{28,0},{1,29},{... | collective-permute-start | bytes 245768 | tf_op jit(solution)/shard_map/ppermute | solution.py:384
  70.7 10.5 %collective-permute-start.3 = (bf16[160,256]{1,0:T(8,128)(2,1)}, bf16[160,256]{1,0:T(8,128)(2,1)S(1)}, u32[]{:S(2)}, u32[]{:S(2)}) collective-permute-start(bf16[160,256]{1,0:T(8,128)(2,1)} %get-tuple-element.40), channel_id=1, source_target_pairs={{0,16},{4,20},{8,24},{12,28},{16,0},{20,4},{24,8},{28,12},{1,17},{... | collective-permute-start | bytes 245768 | tf_op jit(solution)/shard_map/ppermute | solution.py:384
  70.7 13.2 %collective-permute-start.4 = (bf16[160,256]{1,0:T(8,128)(2,1)}, bf16[160,256]{1,0:T(8,128)(2,1)S(1)}, u32[]{:S(2)}, u32[]{:S(2)}) collective-permute-start(bf16[160,256]{1,0:T(8,128)(2,1)} %get-tuple-element.41), channel_id=1, source_target_pairs={{0,20},{4,16},{8,28},{12,24},{16,4},{20,0},{24,12},{28,8},{1,21},{... | collective-permute-start | bytes 245768 | tf_op jit(solution)/shard_map/ppermute | solution.py:384
  73.9 10.9 %collective-permute-start.5 = (bf16[160,256]{1,0:T(8,128)(2,1)}, bf16[160,256]{1,0:T(8,128)(2,1)S(1)}, u32[]{:S(2)}, u32[]{:S(2)}) collective-permute-start(bf16[160,256]{1,0:T(8,128)(2,1)} %get-tuple-element.42), channel_id=1, source_target_pairs={{0,24},{4,28},{8,16},{12,20},{16,8},{20,12},{24,0},{28,4},{1,25},{... | collective-permute-start | bytes 245768 | tf_op jit(solution)/shard_map/ppermute | solution.py:384
  81.2 7.5 %collective-permute-start.6 = (bf16[160,256]{1,0:T(8,128)(2,1)}, bf16[160,256]{1,0:T(8,128)(2,1)S(1)}, u32[]{:S(2)}, u32[]{:S(2)}) collective-permute-start(bf16[160,256]{1,0:T(8,128)(2,1)} %get-tuple-element.43), channel_id=1, source_target_pairs={{0,28},{4,24},{8,20},{12,16},{16,12},{20,8},{24,4},{28,0},{1,29},{... | collective-permute-start | bytes 245768 | tf_op jit(solution)/shard_map/ppermute | solution.py:384
  83.9 8.1 %collective-permute-start.10 = (bf16[160,512]{1,0:T(8,128)(2,1)}, bf16[160,512]{1,0:T(8,128)(2,1)S(1)}, u32[]{:S(2)}, u32[]{:S(2)}) collective-permute-start(bf16[160,512]{1,0:T(8,128)(2,1)} %get-tuple-element.51), channel_id=1, source_target_pairs={{0,4},{4,0},{8,12},{12,8},{16,20},{20,16},{24,28},{28,24},{1,5},{5... | collective-permute-start | bytes 491528 | tf_op jit(solution)/shard_map/ppermute | solution.py:384
  84.8 7.4 %collective-permute-start.11 = (bf16[160,512]{1,0:T(8,128)(2,1)}, bf16[160,512]{1,0:T(8,128)(2,1)S(1)}, u32[]{:S(2)}, u32[]{:S(2)}) collective-permute-start(bf16[160,512]{1,0:T(8,128)(2,1)} %get-tuple-element.52), channel_id=1, source_target_pairs={{0,8},{4,12},{8,0},{12,4},{16,24},{20,28},{24,16},{28,20},{1,9},{5... | collective-permute-start | bytes 491528 | tf_op jit(solution)/shard_map/ppermute | solution.py:384
  88.6 7.0 %collective-permute-start.12 = (bf16[160,512]{1,0:T(8,128)(2,1)}, bf16[160,512]{1,0:T(8,128)(2,1)S(1)}, u32[]{:S(2)}, u32[]{:S(2)}) collective-permute-start(bf16[160,512]{1,0:T(8,128)(2,1)} %get-tuple-element.53), channel_id=1, source_target_pairs={{0,12},{4,8},{8,4},{12,0},{16,28},{20,24},{24,20},{28,16},{1,13},{... | collective-permute-start | bytes 491528 | tf_op jit(solution)/shard_map/ppermute | solution.py:384
  92.0 12.3 %collective-permute-start = (bf16[160,512]{1,0:T(8,128)(2,1)}, bf16[160,512]{1,0:T(8,128)(2,1)S(1)}, u32[]{:S(2)}, u32[]{:S(2)}) collective-permute-start(bf16[160,512]{1,0:T(8,128)(2,1)} %get-tuple-element.37), channel_id=1, source_target_pairs={{0,4},{4,0},{8,12},{12,8},{16,20},{20,16},{24,28},{28,24},{1,5},{5... | collective-permute-start | bytes 491528 | tf_op jit(solution)/shard_map/ppermute | solution.py:384
  92.1 12.3 %collective-permute-start.1 = (bf16[160,512]{1,0:T(8,128)(2,1)}, bf16[160,512]{1,0:T(8,128)(2,1)S(1)}, u32[]{:S(2)}, u32[]{:S(2)}) collective-permute-start(bf16[160,512]{1,0:T(8,128)(2,1)} %get-tuple-element.38), channel_id=1, source_target_pairs={{0,8},{4,12},{8,0},{12,4},{16,24},{20,28},{24,16},{28,20},{1,9},{5... | collective-permute-start | bytes 491528 | tf_op jit(solution)/shard_map/ppermute | solution.py:384
  95.6 10.0 %collective-permute-start.2 = (bf16[160,512]{1,0:T(8,128)(2,1)}, bf16[160,512]{1,0:T(8,128)(2,1)S(1)}, u32[]{:S(2)}, u32[]{:S(2)}) collective-permute-start(bf16[160,512]{1,0:T(8,128)(2,1)} %get-tuple-element.39), channel_id=1, source_target_pairs={{0,12},{4,8},{8,4},{12,0},{16,28},{20,24},{24,20},{28,16},{1,13},{... | collective-permute-start | bytes 491528 | tf_op jit(solution)/shard_map/ppermute | solution.py:384
  97.9 0.9 copy-start.2
  98.8 2.9 %copy-start.3 = (bf16[160,512]{1,0:T(8,128)(2,1)S(1)}, bf16[160,512]{1,0:T(8,128)(2,1)}, u32[]{:S(2)}) copy-start(bf16[160,512]{1,0:T(8,128)(2,1)} %get-tuple-element.50.refs_0_) | copy-start | bytes 491524
  101.7 6.2 %copy-start.1 = (bf16[160,512]{1,0:T(8,128)(2,1)S(1)}, bf16[160,512]{1,0:T(8,128)(2,1)}, u32[]{:S(2)}) copy-start(bf16[160,512]{1,0:T(8,128)(2,1)} %get-tuple-element.36.refs_0_) | copy-start | bytes 491524
  104.3 9.3 %collective-permute-start.18 = (bf16[160,256]{1,0:T(8,128)(2,1)S(1)}, bf16[160,256]{1,0:T(8,128)(2,1)S(1)}, u32[]{:S(2)}, u32[]{:S(2)}) collective-permute-start(bf16[160,256]{1,0:T(8,128)(2,1)S(1)} %get-tuple-element.62), channel_id=1, source_target_pairs={{0,8},{4,12},{8,0},{12,4},{16,24},{20,28},{24,16},{28,20},{1,9},{5... | collective-permute-start | bytes 245768 | tf_op jit(solution)/shard_map/ppermute | solution.py:384
  104.4 9.3 %collective-permute-start.19 = (bf16[160,256]{1,0:T(8,128)(2,1)S(1)}, bf16[160,256]{1,0:T(8,128)(2,1)S(1)}, u32[]{:S(2)}, u32[]{:S(2)}) collective-permute-start(bf16[160,256]{1,0:T(8,128)(2,1)S(1)} %get-tuple-element.63), channel_id=1, source_target_pairs={{0,12},{4,8},{8,4},{12,0},{16,28},{20,24},{24,20},{28,16},{1,13},{... | collective-permute-start | bytes 245768 | tf_op jit(solution)/shard_map/ppermute | solution.py:384
  105.5 9.6 %collective-permute-start.17 = (bf16[160,256]{1,0:T(8,128)(2,1)S(1)}, bf16[160,256]{1,0:T(8,128)(2,1)S(1)}, u32[]{:S(2)}, u32[]{:S(2)}) collective-permute-start(bf16[160,256]{1,0:T(8,128)(2,1)S(1)} %get-tuple-element.61), channel_id=1, source_target_pairs={{0,4},{4,0},{8,12},{12,8},{16,20},{20,16},{24,28},{28,24},{1,5},{5... | collective-permute-start | bytes 245768 | tf_op jit(solution)/shard_map/ppermute | solution.py:384
  110.8 9.2 %copy-start = (bf16[2048,512]{1,0:T(8,128)(2,1)S(1)}, bf16[2048,512]{1,0:T(8,128)(2,1)}, u32[]{:S(2)}) copy-start(bf16[2048,512]{1,0:T(8,128)(2,1)} %refs_8_.1) | copy-start | bytes 6291460
  113.6 4.5 %collective-permute-start.8 = (bf16[160,256]{1,0:T(8,128)(2,1)S(1)}, bf16[160,256]{1,0:T(8,128)(2,1)S(1)}, u32[]{:S(2)}, u32[]{:S(2)}) collective-permute-start(bf16[160,256]{1,0:T(8,128)(2,1)S(1)} %get-tuple-element.48), channel_id=1, source_target_pairs={{0,8},{4,12},{8,0},{12,4},{16,24},{20,28},{24,16},{28,20},{1,9},{5... | collective-permute-start | bytes 245768 | tf_op jit(solution)/shard_map/ppermute | solution.py:384
  113.7 5.4 %collective-permute-start.9 = (bf16[160,256]{1,0:T(8,128)(2,1)S(1)}, bf16[160,256]{1,0:T(8,128)(2,1)S(1)}, u32[]{:S(2)}, u32[]{:S(2)}) collective-permute-start(bf16[160,256]{1,0:T(8,128)(2,1)S(1)} %get-tuple-element.49), channel_id=1, source_target_pairs={{0,12},{4,8},{8,4},{12,0},{16,28},{20,24},{24,20},{28,16},{1,13},{... | collective-permute-start | bytes 245768 | tf_op jit(solution)/shard_map/ppermute | solution.py:384
  115.1 4.8 %collective-permute-start.7 = (bf16[160,256]{1,0:T(8,128)(2,1)S(1)}, bf16[160,256]{1,0:T(8,128)(2,1)S(1)}, u32[]{:S(2)}, u32[]{:S(2)}) collective-permute-start(bf16[160,256]{1,0:T(8,128)(2,1)S(1)} %get-tuple-element.47), channel_id=1, source_target_pairs={{0,4},{4,0},{8,12},{12,8},{16,20},{20,16},{24,28},{28,24},{1,5},{5... | collective-permute-start | bytes 245768 | tf_op jit(solution)/shard_map/ppermute | solution.py:384

commit v2 on v1

--- a/solution.py
+++ b/solution.py
@@ -151,24 +151,21 @@
 
 
 def turn_kernel(groups, chunks, *refs):
-    sources, (cos_ref, sin_ref), out_refs = refs[:5], refs[5:7], refs[7:-6]
-    held, sems = refs[-6:-1], refs[-1]
-    copies = [pltpu.make_async_copy(src, dst, sems.at[i]) for i, (src, dst) in enumerate(zip(sources, held))]
+    sources, (gain_ref, cos_ref, sin_ref), out_refs = refs[:3], refs[3:6], refs[6:-4]
+    (q_ref, k_ref, v_ref), sems = refs[-4:-1], refs[-1]
+    copies = [pltpu.make_async_copy(src, dst, sems.at[i]) for i, (src, dst) in enumerate(zip(sources, refs[-4:-1]))]
     for copy in copies:
         copy.start()
-    for copy in copies:
-        copy.wait()
-    q_ref, k_ref, v_ref, qg_ref, kg_ref = held
-    home = lax.axis_index("sp") % groups
-    cos_table, sin_table = cos_ref[...], sin_ref[...]
-    q_gain = jnp.concatenate([qg_ref[...]] * 2, axis=1)
-    k_gain = jnp.concatenate([kg_ref[...]] * 2, axis=1)
     quarter = HD // 4
-    lane = lax.broadcasted_iota(jnp.int32, cos_table.shape, 1)
-    even = (lane // quarter) % 2 == 0
+    home = home_of(groups)
     row_head = (lax.broadcasted_iota(jnp.int32, (2 * TILE, TILE), 0) % TILE) // HD
     col_head = lax.broadcasted_iota(jnp.int32, (2 * TILE, TILE), 1) // HD
     average = jnp.where(row_head == col_head, 1.0 / HD, 0.0).astype(jnp.bfloat16)
+    cos_table, sin_table = cos_ref[...], sin_ref[...]
+    even = (lax.broadcasted_iota(jnp.int32, cos_table.shape, 1) // quarter) % 2 == 0
+    q_gain, k_gain = gain_ref[0:1, :], gain_ref[1:2, :]
+    for copy in copies:
+        copy.wait()
 
     def turned(tile, gain):
         field = tile.astype(jnp.float32)
@@ -182,11 +179,10 @@
         partner = jnp.where(even, pltpu.roll(normed, TILE - quarter, 1), pltpu.roll(normed, quarter, 1))
         return (normed * cos_table + partner * sin_table).astype(jnp.bfloat16)
 
-    both_refs, kv_refs = out_refs[: groups * chunks], out_refs[groups * chunks :]
     for c in range(chunks):
         for j in range(groups):
             place = (home ^ j) * chunks + c
-            both, kv = both_refs[c * groups + j], kv_refs[c * groups + j]
+            both, kv = out_refs[c * groups + j], out_refs[groups * chunks + c * groups + j]
             for p in range(2):
                 lanes = pl.ds(pl.multiple_of((place * 2 + p) * TILE, TILE), TILE)
                 both[:, p * TILE : (p + 1) * TILE] = turned(q_ref[:, lanes], q_gain)
@@ -209,19 +205,20 @@
 def turn_and_pack(queries, keys, values, q_gain, k_gain, cos_table, sin_table, groups, chunks):
     tok = queries.shape[0]
     made = groups * chunks
+    shapes = [jax.ShapeDtypeStruct((tok, 4 * TILE), jnp.bfloat16)] * made
+    shapes += [jax.ShapeDtypeStruct((tok, 2 * TILE), jnp.bfloat16)] * made
+    gains = jnp.concatenate([q_gain, q_gain, k_gain, k_gain]).reshape(2, TILE)
     out = pl.pallas_call(
         functools.partial(turn_kernel, groups, chunks),
-        in_specs=[pl.BlockSpec(memory_space=pltpu.HBM)] * 5 + in_vmem(2),
+        in_specs=[pl.BlockSpec(memory_space=pltpu.HBM)] * 3 + in_vmem(3),
         out_specs=in_vmem(2 * made),
-        out_shape=[jax.ShapeDtypeStruct((tok, 4 * TILE), jnp.bfloat16)] * made
-        + [jax.ShapeDtypeStruct((tok, 2 * TILE), jnp.bfloat16)] * made,
+        out_shape=shapes,
         scratch_shapes=[pltpu.VMEM(x.shape, x.dtype) for x in (queries, keys, values)]
-        + [pltpu.VMEM((1, HD), jnp.float32)] * 2
-        + [pltpu.SemaphoreType.DMA((5,))],
-        compiler_params=params(60),
+        + [pltpu.SemaphoreType.DMA((3,))],
+        compiler_params=params(52),
         cost_estimate=pl.CostEstimate(flops=40 * 3072 * tok, bytes_accessed=6 * 4096 * tok, transcendentals=0),
         name="turn",
-    )(queries, keys, values, q_gain[None], k_gain[None], cos_table, sin_table)
+    )(queries, keys, values, gains, cos_table, sin_table)
     both = [out[c * groups : (c + 1) * groups] for c in range(chunks)]
     kv = [out[made + c * groups : made + (c + 1) * groups] for c in range(chunks)]
     return both, kv
@@ -303,7 +300,7 @@
             pltpu.VMEM((2, count * rows, wide), jnp.float32),
             pltpu.VMEM((2, count * rows, wide), jnp.bfloat16),
         ],
-        compiler_params=params(24),
+        compiler_params=params(32),
         cost_estimate=pl.CostEstimate(
             flops=8 * count * rows * wide * TILE, bytes_accessed=8 * wide * TILE, transcendentals=0
         ),
@@ -311,72 +308,101 @@
     )(*near, keys, vals)
 
 
-def project_kernel(groups, chunks, early, late, *refs):
-    att_refs, refs = refs[: groups * chunks], refs[groups * chunks :]
-    bufs, sems = refs[-2:]
-    home = lax.axis_index("sp") % groups
-    which = early if late is None else late
-    w_refs = refs[: len(which)]
-    deep = chunks * 2 * TILE
-    row = lambda j: pl.ds(pl.multiple_of((home ^ j) * deep, deep), deep)
-    copies = [
-        [pltpu.make_async_copy(w_ref.at[row(j), :], bufs.at[i, j], sems.at[i, j]) for j in range(groups)]
-        for i, w_ref in enumerate(w_refs)
-    ]
-    for copy in sum(copies, []):
-        copy.start()
-    parts = [jnp.concatenate([att_refs[c * groups + j][...] for c in range(chunks)], axis=1) for j in range(groups)]
-
-    def product(i):
+def home_of(groups):
+    return lax.axis_index("sp") % groups
+
+
+def loads(sources, held, sems, groups):
+    copies = []
+    for i, source in enumerate(sources):
+        deep = source.shape[0] // groups
+        rows = [pl.ds(pl.multiple_of((home_of(groups) ^ j) * deep, deep), deep) for j in range(groups)]
+        copies.append(
+            [pltpu.make_async_copy(source.at[rows[j], :], held[i].at[j], sems.at[i, j]) for j in range(groups)]
+        )
+    for row in copies:
+        for copy in row:
+            copy.start()
+    return copies
+
+
+def term(att_ref, held_ref, j, c):
+    rows = slice(c * 2 * TILE, (c + 1) * 2 * TILE)
+    return jnp.dot(att_ref[...], held_ref[j, rows, :], preferred_element_type=jnp.float32)
+
+
+def first_kernel(groups, *refs):
+    att_refs, sources, refs = refs[:groups], refs[groups : groups + 2], refs[groups + 2 :]
+    held, sums, sems = refs[0:2], refs[2:4], refs[4]
+    copies = loads(sources, held, sems, groups)
+    for i in range(2):
         total = None
         for j in range(groups):
             copies[i][j].wait()
-            term = jnp.dot(parts[j], bufs[i, j], preferred_element_type=jnp.float32)
-            total = term if total is None else total + term
-        return total.astype(jnp.bfloat16)
-
-    if late is None:
-        for i, out_ref in enumerate(refs[len(which) : -2]):
-            out_ref[...] = product(i)
-        return
+            part = term(att_refs[j], held[i], j, 0)
+            total = part if total is None else total + part
+        sums[i][...] = total
+
+
+def second_kernel(groups, *refs):
+    att_refs, own_ref, source, refs = refs[:groups], refs[groups], refs[groups + 1], refs[groups + 2 :]
+    held_a, held_b, sum_a, sum_b = refs[0:4]
+    held, sums, sems = refs[4], refs[5:8], refs[8]
+    copies = loads([source], [held], sems, groups)
+    sums[0][...] = sum_a[...] + term(own_ref, held_a, 0, 1)
+    sums[1][...] = sum_b[...] + term(own_ref, held_b, 0, 1)
+    total = None
+    for j in range(groups):
+        copies[0][j].wait()
+        part = term(att_refs[j], held, j, 0)
+        total = part if total is None else total + part
+    sums[2][...] = total + term(own_ref, held, 0, 1)
+
+
+def third_kernel(groups, *refs):
+    first_refs, second_refs, refs = refs[:groups], refs[groups : 2 * groups], refs[2 * groups :]
+    source, held, sums, out_ref = refs[0], refs[1:4], refs[4:7], refs[7]
+    last, made, sems, out_sems = refs[8:]
+    copies = loads([source], [last], sems, groups)
     me = lax.axis_index("dp")
-    early_refs, out_ref = refs[len(which) : -3], refs[-3]
-    width = w_refs[0].shape[1]
-    column = lambda i: pl.ds(pl.multiple_of((me ^ i) * width, width), width)
-    for i, early_ref in zip(early, early_refs):
-        out_ref[:, column(i)] = early_ref[...]
-    for n, i in enumerate(late):
-        out_ref[:, column(i)] = product(n)
-
-
-def project(attended, blocks, early, late=None, made=()):
-    chunks, groups = len(attended), len(attended[0])
-    tok = attended[0][0].shape[0]
-    depth, width = blocks[0].shape
-    flat = [piece for chunk in attended for piece in chunk]
-    which = early if late is None else late
-    if late is None:
-        out_shape = [jax.ShapeDtypeStruct((tok, width), jnp.bfloat16)] * len(early)
-        out_specs = in_vmem(len(early))
-    else:
-        out_shape = jax.ShapeDtypeStruct((tok, len(blocks) * width), jnp.bfloat16)
-        out_specs = pl.BlockSpec(memory_space=pltpu.VMEM)
+    width = source.shape[1]
+
+    def leave(i):
+        column = pl.ds(pl.multiple_of((me ^ i) * width, width), width)
+        copy = pltpu.make_async_copy(made.at[i], out_ref.at[:, column], out_sems.at[i])
+        copy.start()
+        return copy
+
+    leaving = []
+    for i in range(3):
+        total = sums[i][...]
+        for j in range(1, groups):
+            total = total + term(second_refs[j], held[i], j, 1)
+        made[i] = total.astype(jnp.bfloat16)
+        leaving.append(leave(i))
+    total = None
+    for j in range(groups):
+        copies[0][j].wait()
+        part = term(first_refs[j], last, j, 0) + term(second_refs[j], last, j, 1)
+        total = part if total is None else total + part
+    made[3] = total.astype(jnp.bfloat16)
+    leaving.append(leave(3))
+    for copy in leaving:
+        copy.wait()
+
+
+def project_call(kernel, groups, inputs, spaces, out_shape, scratch, flops):
+    many = isinstance(out_shape, list)
     return pl.pallas_call(
-        functools.partial(project_kernel, groups, chunks, early, late),
-        in_specs=in_vmem(len(flat)) + [pl.BlockSpec(memory_space=pl.ANY)] * len(which) + in_vmem(len(made)),
-        out_specs=out_specs,
+        functools.partial(kernel, groups),
+        in_specs=[pl.BlockSpec(memory_space=space) for space in spaces],
+        out_specs=in_vmem(len(out_shape)) if many else pl.BlockSpec(memory_space=pl.ANY),
         out_shape=out_shape,
-        scratch_shapes=[
-            pltpu.VMEM((len(which), groups, depth // groups, width), jnp.bfloat16),
-            pltpu.SemaphoreType.DMA((len(which), groups)),
-        ],
+        scratch_shapes=scratch,
         compiler_params=params(16),
-        cost_estimate=pl.CostEstimate(
-            flops=2 * tok * depth * width * len(which), bytes_accessed=2 * depth * width * len(which),
-            transcendentals=0,
-        ),
+        cost_estimate=pl.CostEstimate(flops=flops, bytes_accessed=1 << 22, transcendentals=0),
         name="project",
-    )(*flat, *[blocks[i] for i in which], *made)
+    )(*inputs)
 
 
 def exchanged(block, axis, flip):
@@ -385,20 +411,14 @@
 
 
 def group_form(queries, keys, values, q_gain, k_gain, w_out):
-    sp_count, dp_count = lax.axis_size("sp"), lax.axis_size("dp")
+    sp_count = lax.axis_size("sp")
     tok = queries.shape[2]
     groups = sp_count // 2
     chunks = KV // groups // 2
-    bits = dp_count.bit_length() - 1
-    top = 1 << (bits - 1)
-    blocks = {0: w_out, top: exchanged(w_out, "dp", top)}
-    early, late = [0], [top]
-    for bit in reversed(range(bits - 1)):
-        for listed in (early, late):
-            for key in list(listed):
-                blocks[key | 1 << bit] = exchanged(blocks[key], "dp", 1 << bit)
-                listed.append(key | 1 << bit)
-    early, late = early + late[:1], late[1:]
+    deep, width = w_out.shape[0] // groups, w_out.shape[1]
+    across = exchanged(w_out, "dp", 2)
+    beside = exchanged(w_out, "dp", 1)
+    corner = exchanged(across, "dp", 1)
     cos_table, sin_table = rotary_lanes(lax.axis_index("sp") * tok, tok)
     both, kv = turn_and_pack(queries[0].T, keys[0].T, values[0].T, q_gain, k_gain, cos_table, sin_table, groups, chunks)
     near, far = [], []
@@ -408,21 +428,51 @@
     back = []
     for c in range(chunks):
         ready = spread(near[c], far[c])
-        got = [None] * groups
-        for first in reversed(range(0, groups, 2)):
-            done = attend(near[c][first : first + 2], *ready)
-            for j in (first + 1, first):
-                got[j] = exchanged(done[j - first], "sp", j) if j else done[0]
-        back.append(got)
-    listed = [blocks[i] for i in range(dp_count)]
-    made = project(back, listed, early)
-    mixed = project(back, listed, early, late, made)
+        away = attend(near[c][1:], *ready)
+        local = attend(near[c][:1], *ready)
+        back.append(list(local) + [exchanged(away[j - 1], "sp", j) for j in range(1, groups)])
+
+    vmem, hbm = pltpu.VMEM, pl.ANY
+    held = jax.ShapeDtypeStruct((groups, deep, width), jnp.bfloat16)
+    summed = jax.ShapeDtypeStruct((tok, width), jnp.float32)
+    flops = 2 * tok * groups * deep * width
+    held_a, held_b, sum_a, sum_b = project_call(
+        first_kernel,
+        groups,
+        [*back[0], w_out, beside],
+        [vmem] * groups + [hbm] * 2,
+        [held] * 2 + [summed] * 2,
+        [pltpu.SemaphoreType.DMA((2, groups))],
+        flops,
+    )
+    held_c, *sums = project_call(
+        second_kernel,
+        groups,
+        [*back[0], back[1][0], across, held_a, held_b, sum_a, sum_b],
+        [vmem] * (groups + 1) + [hbm] + [vmem] * 4,
+        [held] + [summed] * 3,
+        [pltpu.SemaphoreType.DMA((1, groups))],
+        flops,
+    )
+    mixed = project_call(
+        third_kernel,
+        groups,
+        [*back[0], *back[1], corner, held_a, held_b, held_c, *sums],
+        [vmem] * (2 * groups) + [hbm] + [vmem] * 6,
+        jax.ShapeDtypeStruct((tok, 4 * width), jnp.bfloat16),
+        [
+            pltpu.VMEM(held.shape, held.dtype),
+            pltpu.VMEM((4, tok, width), jnp.bfloat16),
+            pltpu.SemaphoreType.DMA((1, groups)),
+            pltpu.SemaphoreType.DMA((4,)),
+        ],
+        2 * flops,
+    )
     return mixed[None]
 
 
 def grouped(sp_count, dp_count):
-    powers = sp_count & (sp_count - 1) == 0 and dp_count & (dp_count - 1) == 0
-    return powers and sp_count > 2 and dp_count > 1 and KV % sp_count == 0
+    return dp_count == 4 and KV == 2 * sp_count and sp_count // 2 == 4
 
 
 def on_device(*args):

time: 126 us -> 121 us (0.960)
  waiting for transfers between devices: 60.6 us -> 57.2 us
    ppermute x23, waiting for transfers between devices: 60.6 us -> 57.2 us  [exchanged(): return lax.ppermute(block, axis, [(i, i ^ flip) for i in range(count)])]
    pallas_call x1, Pallas kernels: 4.7 us -> 3.35 us  [turn_and_pack(): pl.pallas_call(functools.partial(turn_kernel, groups, chunks), in_specs=[...]
    pallas_call x2 -> x3, Pallas kernels: 5.43 us -> 5.95 us  [project_call(): pl.pallas_call(functools.partial(kernel, groups), in_specs=[pl.BlockSpec(...]
  transfers between devices with their start and end apart: 23 -> 23, of which waited for: 10 -> 6; matrix products, arithmetic and copies ran while one was open for 1% -> 1% of each run, Pallas kernels for 15% -> 15%
where the time goes in v2:
time: 121 us
  waiting for transfers between devices  57.2 us (47%)
  starting transfers between devices  41.1 us (34%)
  Pallas kernels  20.6 us (17%)
  other arithmetic  1.26 us (1%)
    ppermute x23, waiting for transfers between devices, exchanged(): return lax.ppermute(block, axis, [(i, i ^ flip) for i in range(count)])  57.2 us
    ppermute x23, starting transfers between devices, exchanged(): return lax.ppermute(block, axis, [(i, i ^ flip) for i in range(count)])  41.1 us
    pallas_call x4, Pallas kernels, attend(): pl.pallas_call(functools.partial(attend_kernel, count), in_specs=in_vmem(...  10.6 us
    pallas_call x3, Pallas kernels, project_call(): pl.pallas_call(functools.partial(kernel, groups), in_specs=[pl.BlockSpec(...  5.95 us
    pallas_call x1, Pallas kernels, turn_and_pack(): pl.pallas_call(functools.partial(turn_kernel, groups, chunks), in_specs=[...  3.35 us
  transfers between devices with their start and end apart: 23, of which 6 were waited for; matrix products, arithmetic and copies ran while one was open for 1% of the time, Pallas kernels for 15%

profile of v2, /device:TPU:0, one launch (start us, length us, event | category | flops | bytes accessed | tf_op | source)
XLA Modules:
  0.0 120.6 jit_solution(18194063478542910550)
XLA Ops:
  0.0 3.0 %collective-permute-start.20 = (bf16[2048,512]{1,0:T(8,128)(2,1)}, bf16[2048,512]{1,0:T(8,128)(2,1)S(1)}, u32[]{:S(2)}, u32[]{:S(2)}) collective-permute-start(bf16[2048,512]{1,0:T(8,128)(2,1)} %refs_4_.1), channel_id=1, source_target_pairs={{0,2},{1,3},{2,0},{3,1},{4,6},{5,7},{6,4},{7,5},{8,10},{9,11},{10,... | collective-permute-start | bytes 6291464 | tf_op jit(solution)/shard_map/ppermute | solution.py:410
  3.0 0.0 collective-permute-start.22
  3.0 45.8 %collective-permute-done.20.refs_5_ = bf16[2048,512]{1,0:T(8,128)(2,1)S(1)} collective-permute-done((bf16[2048,512]{1,0:T(8,128)(2,1)}, bf16[2048,512]{1,0:T(8,128)(2,1)S(1)}, u32[]{:S(2)}, u32[]{:S(2)}) %collective-permute-start.20) | collective-permute-done | bytes 2097184 | tf_op jit(solution)/shard_map/ppermute | solution.py:410
  48.8 0.0 collective-permute-start.21
  48.8 0.8 maximum_bitcast_fusion.refs_3_
  49.7 0.4 negate_select_fusion
  50.1 3.4 %turn.1 = (bf16[160,512]{1,0:T(8,128)(2,1)S(1)}, bf16[160,512]{1,0:T(8,128)(2,1)S(1)}, bf16[160,512]{1,0:T(8,128)(2,1)S(1)}, bf16[160,512]{1,0:T(8,128)(2,1)S(1)...) custom-call(bf16[160,2048]{1,0:T(8,128)(2,1)} %bitcast.12, ...), custom_call_target="tpu_custom_call" | custom-call | flops 19660800 | bytes 3932160 | tf_op jit(solution)/shard_map/turn/pallas_call | solution.py:211
  53.5 2.9 %collective-permute-start.3 = (bf16[160,256]{1,0:T(8,128)(2,1)S(1)}, bf16[160,256]{1,0:T(8,128)(2,1)S(1)}, u32[]{:S(2)}, u32[]{:S(2)}) collective-permute-start(bf16[160,256]{1,0:T(8,128)(2,1)S(1)} %get-tuple-element.43), channel_id=1, source_target_pairs={{0,16},{4,20},{8,24},{12,28},{16,0},{20,4},{24,8},{28,12},{1,17},{... | collective-permute-start | bytes 245768 | tf_op jit(solution)/shard_map/ppermute | solution.py:410
  56.4 1.3 %collective-permute-start.4 = (bf16[160,256]{1,0:T(8,128)(2,1)S(1)}, bf16[160,256]{1,0:T(8,128)(2,1)S(1)}, u32[]{:S(2)}, u32[]{:S(2)}) collective-permute-start(bf16[160,256]{1,0:T(8,128)(2,1)S(1)} %get-tuple-element.44), channel_id=1, source_target_pairs={{0,20},{4,16},{8,28},{12,24},{16,4},{20,0},{24,12},{28,8},{1,21},{... | collective-permute-start | bytes 245768 | tf_op jit(solution)/shard_map/ppermute | solution.py:410
  57.7 3.6 %collective-permute-start.5 = (bf16[160,256]{1,0:T(8,128)(2,1)S(1)}, bf16[160,256]{1,0:T(8,128)(2,1)S(1)}, u32[]{:S(2)}, u32[]{:S(2)}) collective-permute-start(bf16[160,256]{1,0:T(8,128)(2,1)S(1)} %get-tuple-element.45), channel_id=1, source_target_pairs={{0,24},{4,28},{8,16},{12,20},{16,8},{20,12},{24,0},{28,4},{1,25},{... | collective-permute-start | bytes 245768 | tf_op jit(solution)/shard_map/ppermute | solution.py:410
  61.3 0.2 collective-permute-done.3.refs_4_
  61.4 7.9 %collective-permute-start.6 = (bf16[160,256]{1,0:T(8,128)(2,1)S(1)}, bf16[160,256]{1,0:T(8,128)(2,1)S(1)}, u32[]{:S(2)}, u32[]{:S(2)}) collective-permute-start(bf16[160,256]{1,0:T(8,128)(2,1)S(1)} %get-tuple-element.46), channel_id=1, source_target_pairs={{0,28},{4,24},{8,20},{12,16},{16,12},{20,8},{24,4},{28,0},{1,29},{... | collective-permute-start | bytes 245768 | tf_op jit(solution)/shard_map/ppermute | solution.py:410
  69.3 0.0 collective-permute-done.4.refs_5_
  69.3 0.0 collective-permute-start.13
  69.3 2.9 %collective-permute-start.14 = (bf16[160,256]{1,0:T(8,128)(2,1)S(1)}, bf16[160,256]{1,0:T(8,128)(2,1)S(1)}, u32[]{:S(2)}, u32[]{:S(2)}) collective-permute-start(bf16[160,256]{1,0:T(8,128)(2,1)S(1)} %get-tuple-element.57), channel_id=1, source_target_pairs={{0,20},{4,16},{8,28},{12,24},{16,4},{20,0},{24,12},{28,8},{1,21},{... | collective-permute-start | bytes 245768 | tf_op jit(solution)/shard_map/ppermute | solution.py:410
  72.1 4.2 %collective-permute-start.15 = (bf16[160,256]{1,0:T(8,128)(2,1)S(1)}, bf16[160,256]{1,0:T(8,128)(2,1)S(1)}, u32[]{:S(2)}, u32[]{:S(2)}) collective-permute-start(bf16[160,256]{1,0:T(8,128)(2,1)S(1)} %get-tuple-element.58), channel_id=1, source_target_pairs={{0,24},{4,28},{8,16},{12,20},{16,8},{20,12},{24,0},{28,4},{1,25},{... | collective-permute-start | bytes 245768 | tf_op jit(solution)/shard_map/ppermute | solution.py:410
  76.4 3.2 %collective-permute-done.13.refs_4_ = bf16[160,256]{1,0:T(8,128)(2,1)S(1)} collective-permute-done((bf16[160,256]{1,0:T(8,128)(2,1)S(1)}, bf16[160,256]{1,0:T(8,128)(2,1)S(1)}, u32[]{:S(2)}, u32[]{:S(2)}) %collective-permute-start.13) | collective-permute-done | bytes 81952 | tf_op jit(solution)/shard_map/ppermute | solution.py:410
  79.6 2.9 %collective-permute-start.16 = (bf16[160,256]{1,0:T(8,128)(2,1)S(1)}, bf16[160,256]{1,0:T(8,128)(2,1)S(1)}, u32[]{:S(2)}, u32[]{:S(2)}) collective-permute-start(bf16[160,256]{1,0:T(8,128)(2,1)S(1)} %get-tuple-element.59), channel_id=1, source_target_pairs={{0,28},{4,24},{8,20},{12,16},{16,12},{20,8},{24,4},{28,0},{1,29},{... | collective-permute-start | bytes 245768 | tf_op jit(solution)/shard_map/ppermute | solution.py:410
  82.4 0.0 collective-permute-done.14.refs_5_
  82.4 0.7 collective-permute-start
  83.1 1.4 %collective-permute-start.1 = (bf16[160,512]{1,0:T(8,128)(2,1)S(1)}, bf16[160,512]{1,0:T(8,128)(2,1)S(1)}, u32[]{:S(2)}, u32[]{:S(2)}) collective-permute-start(bf16[160,512]{1,0:T(8,128)(2,1)S(1)} %get-tuple-element.41), channel_id=1, source_target_pairs={{0,8},{4,12},{8,0},{12,4},{16,24},{20,28},{24,16},{28,20},{1,9},{5... | collective-permute-start | bytes 491528 | tf_op jit(solution)/shard_map/ppermute | solution.py:410
  84.5 2.3 %collective-permute-done.16.refs_7_ = bf16[160,256]{1,0:T(8,128)(2,1)S(1)} collective-permute-done((bf16[160,256]{1,0:T(8,128)(2,1)S(1)}, bf16[160,256]{1,0:T(8,128)(2,1)S(1)}, u32[]{:S(2)}, u32[]{:S(2)}) %collective-permute-start.16) | collective-permute-done | bytes 81952 | tf_op jit(solution)/shard_map/ppermute | solution.py:410
  86.8 1.3 %collective-permute-start.2 = (bf16[160,512]{1,0:T(8,128)(2,1)S(1)}, bf16[160,512]{1,0:T(8,128)(2,1)S(1)}, u32[]{:S(2)}, u32[]{:S(2)}) collective-permute-start(bf16[160,512]{1,0:T(8,128)(2,1)S(1)} %get-tuple-element.42), channel_id=1, source_target_pairs={{0,12},{4,8},{8,4},{12,0},{16,28},{20,24},{24,20},{28,16},{1,13},{... | collective-permute-start | bytes 491528 | tf_op jit(solution)/shard_map/ppermute | solution.py:410
  88.1 2.6 %collective-permute-done.refs_1_.refs_0_ = bf16[160,512]{1,0:T(8,128)(2,1)S(1)} collective-permute-done((bf16[160,512]{1,0:T(8,128)(2,1)S(1)}, bf16[160,512]{1,0:T(8,128)(2,1)S(1)}, u32[]{:S(2)}, u32[]{:S(2)}) %collective-permute-start) | collective-permute-done | bytes 163872 | tf_op jit(solution)/shard_map/ppermute | solution.py:410
  90.6 0.0 collective-permute-start.10
  90.7 3.2 %collective-permute-done.2.refs_3_.refs_2_ = bf16[160,512]{1,0:T(8,128)(2,1)S(1)} collective-permute-done((bf16[160,512]{1,0:T(8,128)(2,1)S(1)}, bf16[160,512]{1,0:T(8,128)(2,1)S(1)}, u32[]{:S(2)}, u32[]{:S(2)}) %collective-permute-start.2) | collective-permute-done | bytes 163872 | tf_op jit(solution)/shard_map/ppermute | solution.py:410
  93.8 2.1 %collective-permute-start.12 = (bf16[160,512]{1,0:T(8,128)(2,1)}, bf16[160,512]{1,0:T(8,128)(2,1)S(1)}, u32[]{:S(2)}, u32[]{:S(2)}) collective-permute-start(bf16[160,512]{1,0:T(8,128)(2,1)} %get-tuple-element.55), channel_id=1, source_target_pairs={{0,12},{4,8},{8,4},{12,0},{16,28},{20,24},{24,20},{28,16},{1,13},{... | collective-permute-start | bytes 491528 | tf_op jit(solution)/shard_map/ppermute | solution.py:410
  95.9 0.4 spread.2
  96.3 3.7 %attend.5 = (bf16[160,256]{1,0:T(8,128)(2,1)S(1)}, bf16[160,256]{1,0:T(8,128)(2,1)S(1)}, bf16[160,256]{1,0:T(8,128)(2,1)S(1)}) custom-call(bf16[160,512]{1,0:T(8,128)(2,1)S(1)} %collective-permute-done.refs_1_.refs_0_, bf16[160,512]{1,0:T(8,128)(2,1)S(1)} %collective-permute-done.1.refs_2_.refs_1_, ...), custom_call_target="tpu_custom_call" | custom-call | flops 1258291200 | bytes 2621440 | tf_op jit(solution)/shard_map/attend/pallas_call | solution.py:294
  100.0 0.0 collective-permute-done.10.refs_1_.refs_0_
  100.0 0.1 collective-permute-start.7
  100.1 1.4 %collective-permute-start.8 = (bf16[160,256]{1,0:T(8,128)(2,1)S(1)}, bf16[160,256]{1,0:T(8,128)(2,1)S(1)}, u32[]{:S(2)}, u32[]{:S(2)}) collective-permute-start(bf16[160,256]{1,0:T(8,128)(2,1)S(1)} %get-tuple-element.50), channel_id=1, source_target_pairs={{0,8},{4,12},{8,0},{12,4},{16,24},{20,28},{24,16},{28,20},{1,9},{5... | collective-permute-start | bytes 245768 | tf_op jit(solution)/shard_map/ppermute | solution.py:410
  101.4 0.0 collective-permute-done.12.refs_3_.refs_2_
  101.4 2.1 %collective-permute-start.9 = (bf16[160,256]{1,0:T(8,128)(2,1)S(1)}, bf16[160,256]{1,0:T(8,128)(2,1)S(1)}, u32[]{:S(2)}, u32[]{:S(2)}) collective-permute-start(bf16[160,256]{1,0:T(8,128)(2,1)S(1)} %get-tuple-element.51), channel_id=1, source_target_pairs={{0,12},{4,8},{8,4},{12,0},{16,28},{20,24},{24,20},{28,16},{1,13},{... | collective-permute-start | bytes 245768 | tf_op jit(solution)/shard_map/ppermute | solution.py:410
  103.5 0.4 spread.3
  103.9 1.5 %attend.6.refs_4_ = bf16[160,256]{1,0:T(8,128)(2,1)S(1)} custom-call(bf16[160,512]{1,0:T(8,128)(2,1)S(1)} %get-tuple-element.52.refs_0_, bf16[2,2560,128]{2,1,0:T(8,128)(2,1)S(1)} %get-tuple-element.60.refs_1_.refs_3_, bf16[2,2560,128]{2,1,0:T(8,128)(2,1)S(1)} %get-tuple-element.61.refs_2_.refs_4_), custom_call_target="tpu_custom_call" | custom-call | flops 419430400 | bytes 2621440 | tf_op jit(solution)/shard_map/attend/pallas_call | solution.py:294
  105.4 3.9 %attend.7 = (bf16[160,256]{1,0:T(8,128)(2,1)S(1)}, bf16[160,256]{1,0:T(8,128)(2,1)S(1)}, bf16[160,256]{1,0:T(8,128)(2,1)S(1)}) custom-call(bf16[160,512]{1,0:T(8,128)(2,1)S(1)} %collective-permute-done.10.refs_1_.refs_0_, bf16[160,512]{1,0:T(8,128)(2,1)S(1)} %collective-permute-done.11.refs_2_.refs_1_, ...), custom_call_target="tpu_custom_call" | custom-call | flops 1258291200 | bytes 2621440 | tf_op jit(solution)/shard_map/attend/pallas_call | solution.py:294
  109.3 0.0 copy-start
  109.3 0.2 collective-permute-start.17
  109.5 1.3 %collective-permute-start.18 = (bf16[160,256]{1,0:T(8,128)(2,1)S(1)}, bf16[160,256]{1,0:T(8,128)(2,1)S(1)}, u32[]{:S(2)}, u32[]{:S(2)}) collective-permute-start(bf16[160,256]{1,0:T(8,128)(2,1)S(1)} %get-tuple-element.63), channel_id=1, source_target_pairs={{0,8},{4,12},{8,0},{12,4},{16,24},{20,28},{24,16},{28,20},{1,9},{5... | collective-permute-start | bytes 245768 | tf_op jit(solution)/shard_map/ppermute | solution.py:410
  110.8 2.1 %collective-permute-start.19 = (bf16[160,256]{1,0:T(8,128)(2,1)S(1)}, bf16[160,256]{1,0:T(8,128)(2,1)S(1)}, u32[]{:S(2)}, u32[]{:S(2)}) collective-permute-start(bf16[160,256]{1,0:T(8,128)(2,1)S(1)} %get-tuple-element.64), channel_id=1, source_target_pairs={{0,12},{4,8},{8,4},{12,0},{16,28},{20,24},{24,20},{28,16},{1,13},{... | collective-permute-start | bytes 245768 | tf_op jit(solution)/shard_map/ppermute | solution.py:410
  112.9 1.5 %attend.4.refs_0_ = bf16[160,256]{1,0:T(8,128)(2,1)S(1)} custom-call(bf16[160,512]{1,0:T(8,128)(2,1)S(1)} %get-tuple-element.39.refs_0_, bf16[2,2560,128]{2,1,0:T(8,128)(2,1)S(1)} %get-tuple-element.47.refs_1_.refs_3_, bf16[2,2560,128]{2,1,0:T(8,128)(2,1)S(1)} %get-tuple-element.48.refs_2_.refs_4_), custom_call_target="tpu_custom_call" | custom-call | flops 419430400 | bytes 2621440 | tf_op jit(solution)/shard_map/attend/pallas_call | solution.py:294
  114.4 0.0 collective-permute-done.22.refs_5_
  114.4 1.9 %project.3 = (bf16[4,512,512]{2,1,0:T(8,128)(2,1)S(1)}, bf16[4,512,512]{2,1,0:T(8,128)(2,1)S(1)}, f32[160,512]{1,0:T(8,128)S(1)}, f32[160,512]{1,0:T(8,128)S(1)}) custom-call(bf16[160,256]{1,0:T(8,128)(2,1)S(1)} %attend.4.refs_0_, bf16[160,256]{1,0:T(8,128)(2,1)S(1)} %collective-permute-done.7.refs_1_, bf16[160,256]{1,0:T(8,128)(2,1)S(1)} %collective-permute-done.8.refs_2_, ...), custom_call_target="tpu_custom_call" | custom-call | flops 335544320 | bytes 4194304 | tf_op jit(solution)/shard_map/project/pallas_call | solution.py:396
  116.4 0.9 project.4
  117.3 0.0 collective-permute-done.18.refs_6_
  117.3 0.0 collective-permute-done.19.refs_7_
  117.3 3.1 %project.5 = bf16[160,2048]{1,0:T(8,128)(2,1)} custom-call(bf16[160,256]{1,0:T(8,128)(2,1)S(1)} %attend.4.refs_0_, bf16[160,256]{1,0:T(8,128)(2,1)S(1)} %collective-permute-done.7.refs_1_, bf16[160,256]{1,0:T(8,128)(2,1)S(1)} %collective-permute-done.8.refs_2_, bf16[160,256]{1,0:T(8,128)(2,1)S(1)} %collective-permute-done.9.refs_3_, ...), custom_call_target="tpu_custom_call" | custom-call | flops 671088640 | bytes 4194304 | tf_op jit(solution)/shard_map/project/pallas_call | solution.py:396
  (17 shorter events, 0.1 us)
Async XLA Ops:
  0.0 48.8 %collective-permute-start.20 = (bf16[2048,512]{1,0:T(8,128)(2,1)}, bf16[2048,512]{1,0:T(8,128)(2,1)S(1)}, u32[]{:S(2)}, u32[]{:S(2)}) collective-permute-start(bf16[2048,512]{1,0:T(8,128)(2,1)} %refs_4_.1), channel_id=1, source_target_pairs={{0,2},{1,3},{2,0},{3,1},{4,6},{5,7},{6,4},{7,5},{8,10},{9,11},{10,... | collective-permute-start | bytes 6291464 | tf_op jit(solution)/shard_map/ppermute | solution.py:410
  3.0 111.4 %collective-permute-start.22 = (bf16[2048,512]{1,0:T(8,128)(2,1)}, bf16[2048,512]{1,0:T(8,128)(2,1)}, u32[]{:S(2)}, u32[]{:S(2)}) collective-permute-start(bf16[2048,512]{1,0:T(8,128)(2,1)} %refs_4_.1), channel_id=1, source_target_pairs={{0,1},{1,0},{2,3},{3,2},{4,5},{5,4},{6,7},{7,6},{8,9},{9,8},{10,11... | collective-permute-start | bytes 6291464 | tf_op jit(solution)/shard_map/ppermute | solution.py:410
  48.8 68.5 %collective-permute-start.21 = (bf16[2048,512]{1,0:T(8,128)(2,1)S(1)}, bf16[2048,512]{1,0:T(8,128)(2,1)}, u32[]{:S(2)}, u32[]{:S(2)}) collective-permute-start(bf16[2048,512]{1,0:T(8,128)(2,1)S(1)} %collective-permute-done.20.refs_5_), channel_id=1, source_target_pairs={{0,1},{1,0},{2,3},{3,2},{4,5},{5,4},{6,7},{7,6},{8,9},{9,8},{10,11... | collective-permute-start | bytes 6291464 | tf_op jit(solution)/shard_map/ppermute | solution.py:410
  53.5 8.0 %collective-permute-start.3 = (bf16[160,256]{1,0:T(8,128)(2,1)S(1)}, bf16[160,256]{1,0:T(8,128)(2,1)S(1)}, u32[]{:S(2)}, u32[]{:S(2)}) collective-permute-start(bf16[160,256]{1,0:T(8,128)(2,1)S(1)} %get-tuple-element.43), channel_id=1, source_target_pairs={{0,16},{4,20},{8,24},{12,28},{16,0},{20,4},{24,8},{28,12},{1,17},{... | collective-permute-start | bytes 245768 | tf_op jit(solution)/shard_map/ppermute | solution.py:410
  56.4 12.9 %collective-permute-start.4 = (bf16[160,256]{1,0:T(8,128)(2,1)S(1)}, bf16[160,256]{1,0:T(8,128)(2,1)S(1)}, u32[]{:S(2)}, u32[]{:S(2)}) collective-permute-start(bf16[160,256]{1,0:T(8,128)(2,1)S(1)} %get-tuple-element.44), channel_id=1, source_target_pairs={{0,20},{4,16},{8,28},{12,24},{16,4},{20,0},{24,12},{28,8},{1,21},{... | collective-permute-start | bytes 245768 | tf_op jit(solution)/shard_map/ppermute | solution.py:410
  57.7 11.6 %collective-permute-start.5 = (bf16[160,256]{1,0:T(8,128)(2,1)S(1)}, bf16[160,256]{1,0:T(8,128)(2,1)S(1)}, u32[]{:S(2)}, u32[]{:S(2)}) collective-permute-start(bf16[160,256]{1,0:T(8,128)(2,1)S(1)} %get-tuple-element.45), channel_id=1, source_target_pairs={{0,24},{4,28},{8,16},{12,20},{16,8},{20,12},{24,0},{28,4},{1,25},{... | collective-permute-start | bytes 245768 | tf_op jit(solution)/shard_map/ppermute | solution.py:410
  61.4 10.7 %collective-permute-start.6 = (bf16[160,256]{1,0:T(8,128)(2,1)S(1)}, bf16[160,256]{1,0:T(8,128)(2,1)S(1)}, u32[]{:S(2)}, u32[]{:S(2)}) collective-permute-start(bf16[160,256]{1,0:T(8,128)(2,1)S(1)} %get-tuple-element.46), channel_id=1, source_target_pairs={{0,28},{4,24},{8,20},{12,16},{16,12},{20,8},{24,4},{28,0},{1,29},{... | collective-permute-start | bytes 245768 | tf_op jit(solution)/shard_map/ppermute | solution.py:410
  69.3 10.3 %collective-permute-start.13 = (bf16[160,256]{1,0:T(8,128)(2,1)S(1)}, bf16[160,256]{1,0:T(8,128)(2,1)S(1)}, u32[]{:S(2)}, u32[]{:S(2)}) collective-permute-start(bf16[160,256]{1,0:T(8,128)(2,1)S(1)} %get-tuple-element.56), channel_id=1, source_target_pairs={{0,16},{4,20},{8,24},{12,28},{16,0},{20,4},{24,8},{28,12},{1,17},{... | collective-permute-start | bytes 245768 | tf_op jit(solution)/shard_map/ppermute | solution.py:410
  69.3 13.2 %collective-permute-start.14 = (bf16[160,256]{1,0:T(8,128)(2,1)S(1)}, bf16[160,256]{1,0:T(8,128)(2,1)S(1)}, u32[]{:S(2)}, u32[]{:S(2)}) collective-permute-start(bf16[160,256]{1,0:T(8,128)(2,1)S(1)} %get-tuple-element.57), channel_id=1, source_target_pairs={{0,20},{4,16},{8,28},{12,24},{16,4},{20,0},{24,12},{28,8},{1,21},{... | collective-permute-start | bytes 245768 | tf_op jit(solution)/shard_map/ppermute | solution.py:410
  72.1 11.0 %collective-permute-start.15 = (bf16[160,256]{1,0:T(8,128)(2,1)S(1)}, bf16[160,256]{1,0:T(8,128)(2,1)S(1)}, u32[]{:S(2)}, u32[]{:S(2)}) collective-permute-start(bf16[160,256]{1,0:T(8,128)(2,1)S(1)} %get-tuple-element.58), channel_id=1, source_target_pairs={{0,24},{4,28},{8,16},{12,20},{16,8},{20,12},{24,0},{28,4},{1,25},{... | collective-permute-start | bytes 245768 | tf_op jit(solution)/shard_map/ppermute | solution.py:410
  79.6 7.2 %collective-permute-start.16 = (bf16[160,256]{1,0:T(8,128)(2,1)S(1)}, bf16[160,256]{1,0:T(8,128)(2,1)S(1)}, u32[]{:S(2)}, u32[]{:S(2)}) collective-permute-start(bf16[160,256]{1,0:T(8,128)(2,1)S(1)} %get-tuple-element.59), channel_id=1, source_target_pairs={{0,28},{4,24},{8,20},{12,16},{16,12},{20,8},{24,4},{28,0},{1,29},{... | collective-permute-start | bytes 245768 | tf_op jit(solution)/shard_map/ppermute | solution.py:410
  82.4 8.2 %collective-permute-start = (bf16[160,512]{1,0:T(8,128)(2,1)S(1)}, bf16[160,512]{1,0:T(8,128)(2,1)S(1)}, u32[]{:S(2)}, u32[]{:S(2)}) collective-permute-start(bf16[160,512]{1,0:T(8,128)(2,1)S(1)} %get-tuple-element.40), channel_id=1, source_target_pairs={{0,4},{4,0},{8,12},{12,8},{16,20},{20,16},{24,28},{28,24},{1,5},{5... | collective-permute-start | bytes 491528 | tf_op jit(solution)/shard_map/ppermute | solution.py:410
  83.1 7.5 %collective-permute-start.1 = (bf16[160,512]{1,0:T(8,128)(2,1)S(1)}, bf16[160,512]{1,0:T(8,128)(2,1)S(1)}, u32[]{:S(2)}, u32[]{:S(2)}) collective-permute-start(bf16[160,512]{1,0:T(8,128)(2,1)S(1)} %get-tuple-element.41), channel_id=1, source_target_pairs={{0,8},{4,12},{8,0},{12,4},{16,24},{20,28},{24,16},{28,20},{1,9},{5... | collective-permute-start | bytes 491528 | tf_op jit(solution)/shard_map/ppermute | solution.py:410
  86.8 7.0 %collective-permute-start.2 = (bf16[160,512]{1,0:T(8,128)(2,1)S(1)}, bf16[160,512]{1,0:T(8,128)(2,1)S(1)}, u32[]{:S(2)}, u32[]{:S(2)}) collective-permute-start(bf16[160,512]{1,0:T(8,128)(2,1)S(1)} %get-tuple-element.42), channel_id=1, source_target_pairs={{0,12},{4,8},{8,4},{12,0},{16,28},{20,24},{24,20},{28,16},{1,13},{... | collective-permute-start | bytes 491528 | tf_op jit(solution)/shard_map/ppermute | solution.py:410
  90.6 9.3 %collective-permute-start.10 = (bf16[160,512]{1,0:T(8,128)(2,1)S(1)}, bf16[160,512]{1,0:T(8,128)(2,1)S(1)}, u32[]{:S(2)}, u32[]{:S(2)}) collective-permute-start(bf16[160,512]{1,0:T(8,128)(2,1)S(1)} %get-tuple-element.53), channel_id=1, source_target_pairs={{0,4},{4,0},{8,12},{12,8},{16,20},{20,16},{24,28},{28,24},{1,5},{5... | collective-permute-start | bytes 491528 | tf_op jit(solution)/shard_map/ppermute | solution.py:410
  90.6 9.4 %collective-permute-start.11 = (bf16[160,512]{1,0:T(8,128)(2,1)S(1)}, bf16[160,512]{1,0:T(8,128)(2,1)S(1)}, u32[]{:S(2)}, u32[]{:S(2)}) collective-permute-start(bf16[160,512]{1,0:T(8,128)(2,1)S(1)} %get-tuple-element.54), channel_id=1, source_target_pairs={{0,8},{4,12},{8,0},{12,4},{16,24},{20,28},{24,16},{28,20},{1,9},{5... | collective-permute-start | bytes 491528 | tf_op jit(solution)/shard_map/ppermute | solution.py:410
  93.8 7.6 %collective-permute-start.12 = (bf16[160,512]{1,0:T(8,128)(2,1)}, bf16[160,512]{1,0:T(8,128)(2,1)S(1)}, u32[]{:S(2)}, u32[]{:S(2)}) collective-permute-start(bf16[160,512]{1,0:T(8,128)(2,1)} %get-tuple-element.55), channel_id=1, source_target_pairs={{0,12},{4,8},{8,4},{12,0},{16,28},{20,24},{24,20},{28,16},{1,13},{... | collective-permute-start | bytes 491528 | tf_op jit(solution)/shard_map/ppermute | solution.py:410
  100.0 9.4 %collective-permute-start.7 = (bf16[160,256]{1,0:T(8,128)(2,1)S(1)}, bf16[160,256]{1,0:T(8,128)(2,1)S(1)}, u32[]{:S(2)}, u32[]{:S(2)}) collective-permute-start(bf16[160,256]{1,0:T(8,128)(2,1)S(1)} %get-tuple-element.49), channel_id=1, source_target_pairs={{0,4},{4,0},{8,12},{12,8},{16,20},{20,16},{24,28},{28,24},{1,5},{5... | collective-permute-start | bytes 245768 | tf_op jit(solution)/shard_map/ppermute | solution.py:410
  100.1 9.4 %collective-permute-start.8 = (bf16[160,256]{1,0:T(8,128)(2,1)S(1)}, bf16[160,256]{1,0:T(8,128)(2,1)S(1)}, u32[]{:S(2)}, u32[]{:S(2)}) collective-permute-start(bf16[160,256]{1,0:T(8,128)(2,1)S(1)} %get-tuple-element.50), channel_id=1, source_target_pairs={{0,8},{4,12},{8,0},{12,4},{16,24},{20,28},{24,16},{28,20},{1,9},{5... | collective-permute-start | bytes 245768 | tf_op jit(solution)/shard_map/ppermute | solution.py:410
  101.4 9.4 %collective-permute-start.9 = (bf16[160,256]{1,0:T(8,128)(2,1)S(1)}, bf16[160,256]{1,0:T(8,128)(2,1)S(1)}, u32[]{:S(2)}, u32[]{:S(2)}) collective-permute-start(bf16[160,256]{1,0:T(8,128)(2,1)S(1)} %get-tuple-element.51), channel_id=1, source_target_pairs={{0,12},{4,8},{8,4},{12,0},{16,28},{20,24},{24,20},{28,16},{1,13},{... | collective-permute-start | bytes 245768 | tf_op jit(solution)/shard_map/ppermute | solution.py:410
  109.3 5.1 %copy-start = (bf16[2048,512]{1,0:T(8,128)(2,1)S(1)}, bf16[2048,512]{1,0:T(8,128)(2,1)}, u32[]{:S(2)}) copy-start(bf16[2048,512]{1,0:T(8,128)(2,1)} %refs_4_.1) | copy-start | bytes 6291460
  109.3 8.0 %collective-permute-start.17 = (bf16[160,256]{1,0:T(8,128)(2,1)S(1)}, bf16[160,256]{1,0:T(8,128)(2,1)S(1)}, u32[]{:S(2)}, u32[]{:S(2)}) collective-permute-start(bf16[160,256]{1,0:T(8,128)(2,1)S(1)} %get-tuple-element.62), channel_id=1, source_target_pairs={{0,4},{4,0},{8,12},{12,8},{16,20},{20,16},{24,28},{28,24},{1,5},{5... | collective-permute-start | bytes 245768 | tf_op jit(solution)/shard_map/ppermute | solution.py:410
  109.5 7.8 %collective-permute-start.18 = (bf16[160,256]{1,0:T(8,128)(2,1)S(1)}, bf16[160,256]{1,0:T(8,128)(2,1)S(1)}, u32[]{:S(2)}, u32[]{:S(2)}) collective-permute-start(bf16[160,256]{1,0:T(8,128)(2,1)S(1)} %get-tuple-element.63), channel_id=1, source_target_pairs={{0,8},{4,12},{8,0},{12,4},{16,24},{20,28},{24,16},{28,20},{1,9},{5... | collective-permute-start | bytes 245768 | tf_op jit(solution)/shard_map/ppermute | solution.py:410
  110.8 6.5 %collective-permute-start.19 = (bf16[160,256]{1,0:T(8,128)(2,1)S(1)}, bf16[160,256]{1,0:T(8,128)(2,1)S(1)}, u32[]{:S(2)}, u32[]{:S(2)}) collective-permute-start(bf16[160,256]{1,0:T(8,128)(2,1)S(1)} %get-tuple-element.64), channel_id=1, source_target_pairs={{0,12},{4,8},{8,4},{12,0},{16,28},{20,24},{24,20},{28,16},{1,13},{... | collective-permute-start | bytes 245768 | tf_op jit(solution)/shard_map/ppermute | solution.py:410

commit v3 on v2

--- a/solution.py
+++ b/solution.py
@@ -143,7 +143,10 @@
     position = first_row + lax.broadcasted_iota(jnp.int32, (row_count, TILE), 0)
     lane = lax.broadcasted_iota(jnp.int32, (row_count, TILE), 1) % HD
     quarter = HD // 4
-    inv_freq = rotary_base ** (-(2.0 * (lane % quarter).astype(jnp.float32)) / (HD // 2))
+    index = lax.broadcasted_iota(jnp.int32, (1, TILE), 1) % quarter
+    inv_freq = jnp.zeros((1, TILE), jnp.float32)
+    for i in range(quarter):
+        inv_freq = jnp.where(index == i, rotary_base ** (-(2.0 * i) / (HD // 2)), inv_freq)
     place = jnp.where(lane < HD // 2, position // GRID_W, position % GRID_W).astype(jnp.float32)
     angle = inv_freq * place
     sine = jnp.sin(angle)
@@ -151,9 +154,9 @@
 
 
 def turn_kernel(groups, chunks, *refs):
-    sources, (gain_ref, cos_ref, sin_ref), out_refs = refs[:3], refs[3:6], refs[6:-4]
-    (q_ref, k_ref, v_ref), sems = refs[-4:-1], refs[-1]
-    copies = [pltpu.make_async_copy(src, dst, sems.at[i]) for i, (src, dst) in enumerate(zip(sources, refs[-4:-1]))]
+    sources, gain_ref, out_refs, held, sems = refs[:3], refs[3], refs[4:-4], refs[-4:-1], refs[-1]
+    q_ref, k_ref, v_ref = held
+    copies = [pltpu.make_async_copy(src, dst, sems.at[i]) for i, (src, dst) in enumerate(zip(sources, held))]
     for copy in copies:
         copy.start()
     quarter = HD // 4
@@ -161,11 +164,12 @@
     row_head = (lax.broadcasted_iota(jnp.int32, (2 * TILE, TILE), 0) % TILE) // HD
     col_head = lax.broadcasted_iota(jnp.int32, (2 * TILE, TILE), 1) // HD
     average = jnp.where(row_head == col_head, 1.0 / HD, 0.0).astype(jnp.bfloat16)
-    cos_table, sin_table = cos_ref[...], sin_ref[...]
+    tok = q_ref.shape[0]
+    cos_table, sin_table = rotary_lanes(lax.axis_index("sp") * tok, tok)
     even = (lax.broadcasted_iota(jnp.int32, cos_table.shape, 1) // quarter) % 2 == 0
-    q_gain, k_gain = gain_ref[0:1, :], gain_ref[1:2, :]
     for copy in copies:
         copy.wait()
+    q_gain, k_gain = gain_ref[0:1, :], gain_ref[1:2, :]
 
     def turned(tile, gain):
         field = tile.astype(jnp.float32)
@@ -202,15 +206,14 @@
     return pltpu.CompilerParams(vmem_limit_bytes=mib << 20)
 
 
-def turn_and_pack(queries, keys, values, q_gain, k_gain, cos_table, sin_table, groups, chunks):
+def turn_and_pack(queries, keys, values, q_gain, k_gain, groups, chunks):
     tok = queries.shape[0]
     made = groups * chunks
     shapes = [jax.ShapeDtypeStruct((tok, 4 * TILE), jnp.bfloat16)] * made
     shapes += [jax.ShapeDtypeStruct((tok, 2 * TILE), jnp.bfloat16)] * made
-    gains = jnp.concatenate([q_gain, q_gain, k_gain, k_gain]).reshape(2, TILE)
     out = pl.pallas_call(
         functools.partial(turn_kernel, groups, chunks),
-        in_specs=[pl.BlockSpec(memory_space=pltpu.HBM)] * 3 + in_vmem(3),
+        in_specs=[pl.BlockSpec(memory_space=pltpu.HBM)] * 3 + in_vmem(1),
         out_specs=in_vmem(2 * made),
         out_shape=shapes,
         scratch_shapes=[pltpu.VMEM(x.shape, x.dtype) for x in (queries, keys, values)]
@@ -218,7 +221,7 @@
         compiler_params=params(52),
         cost_estimate=pl.CostEstimate(flops=40 * 3072 * tok, bytes_accessed=6 * 4096 * tok, transcendentals=0),
         name="turn",
-    )(queries, keys, values, gains, cos_table, sin_table)
+    )(queries, keys, values, jnp.concatenate([q_gain, q_gain, k_gain, k_gain]).reshape(2, TILE))
     both = [out[c * groups : (c + 1) * groups] for c in range(chunks)]
     kv = [out[made + c * groups : made + (c + 1) * groups] for c in range(chunks)]
     return both, kv
@@ -331,67 +334,63 @@
     return jnp.dot(att_ref[...], held_ref[j, rows, :], preferred_element_type=jnp.float32)
 
 
+def load_kernel(groups, *refs):
+    for row in loads(refs[0:2], refs[2:4], refs[4], groups):
+        for copy in row:
+            copy.wait()
+
+
 def first_kernel(groups, *refs):
-    att_refs, sources, refs = refs[:groups], refs[groups : groups + 2], refs[groups + 2 :]
-    held, sums, sems = refs[0:2], refs[2:4], refs[4]
-    copies = loads(sources, held, sems, groups)
-    for i in range(2):
+    att_refs, own_ref, source, refs = refs[:groups], refs[groups], refs[groups + 1], refs[groups + 2 :]
+    held, last, sums, sems = refs[0:2], refs[2], refs[3:6], refs[6]
+    copies = loads([source], [last], sems, groups)
+    for i, held_ref in enumerate((*held, last)):
         total = None
         for j in range(groups):
-            copies[i][j].wait()
-            part = term(att_refs[j], held[i], j, 0)
+            if i == 2:
+                copies[0][j].wait()
+            part = term(att_refs[j], held_ref, j, 0)
             total = part if total is None else total + part
-        sums[i][...] = total
+        sums[i][...] = total + term(own_ref, held_ref, 0, 1)
+
+
+def corner_rows(source, groups, j, c):
+    deep = source.shape[0] // groups
+    return pl.ds(pl.multiple_of((home_of(groups) ^ j) * deep + c * 2 * TILE, 2 * TILE), 2 * TILE)
+
+
+def leave(total, i, width, made, out_ref, sem):
+    made[...] = total.astype(jnp.bfloat16)
+    column = pl.ds(pl.multiple_of((lax.axis_index("dp") ^ i) * width, width), width)
+    copy = pltpu.make_async_copy(made, out_ref.at[:, column], sem)
+    copy.start()
+    return copy
 
 
 def second_kernel(groups, *refs):
-    att_refs, own_ref, source, refs = refs[:groups], refs[groups], refs[groups + 1], refs[groups + 2 :]
-    held_a, held_b, sum_a, sum_b = refs[0:4]
-    held, sums, sems = refs[4], refs[5:8], refs[8]
-    copies = loads([source], [held], sems, groups)
-    sums[0][...] = sum_a[...] + term(own_ref, held_a, 0, 1)
-    sums[1][...] = sum_b[...] + term(own_ref, held_b, 0, 1)
-    total = None
-    for j in range(groups):
-        copies[0][j].wait()
-        part = term(att_refs[j], held, j, 0)
-        total = part if total is None else total + part
-    sums[2][...] = total + term(own_ref, held, 0, 1)
-
-
-def third_kernel(groups, *refs):
-    first_refs, second_refs, refs = refs[:groups], refs[groups : 2 * groups], refs[2 * groups :]
-    source, held, sums, out_ref = refs[0], refs[1:4], refs[4:7], refs[7]
-    last, made, sems, out_sems = refs[8:]
-    copies = loads([source], [last], sems, groups)
-    me = lax.axis_index("dp")
-    width = source.shape[1]
-
-    def leave(i):
-        column = pl.ds(pl.multiple_of((me ^ i) * width, width), width)
-        copy = pltpu.make_async_copy(made.at[i], out_ref.at[:, column], out_sems.at[i])
-        copy.start()
-        return copy
-
+    att_refs, held, sums, (out_ref, made, sems) = refs[:-9], refs[-9:-6], refs[-6:-3], refs[-3:]
     leaving = []
     for i in range(3):
         total = sums[i][...]
         for j in range(1, groups):
-            total = total + term(second_refs[j], held[i], j, 1)
-        made[i] = total.astype(jnp.bfloat16)
-        leaving.append(leave(i))
-    total = None
-    for j in range(groups):
-        copies[0][j].wait()
-        part = term(first_refs[j], last, j, 0) + term(second_refs[j], last, j, 1)
-        total = part if total is None else total + part
-    made[3] = total.astype(jnp.bfloat16)
-    leaving.append(leave(3))
+            total = total + term(att_refs[j - 1], held[i], j, 1)
+        leaving.append(leave(total, i, held[i].shape[2], made.at[i], out_ref, sems.at[i]))
     for copy in leaving:
         copy.wait()
 
 
-def project_call(kernel, groups, inputs, spaces, out_shape, scratch, flops):
+def third_kernel(groups, *refs):
+    parts, (source, _, out_ref, made, sem) = (refs[:groups], refs[groups : 2 * groups]), refs[2 * groups :]
+    total = None
+    for c in range(2):
+        for j in range(groups):
+            rows = corner_rows(source, groups, j, c)
+            part = jnp.dot(parts[c][j][...], source[rows, :], preferred_element_type=jnp.float32)
+            total = part if total is None else total + part
+    leave(total, 3, source.shape[1], made, out_ref, sem).wait()
+
+
+def project_call(kernel, groups, inputs, spaces, out_shape, scratch, flops, aliases={}):
     many = isinstance(out_shape, list)
     return pl.pallas_call(
         functools.partial(kernel, groups),
@@ -399,6 +398,7 @@
         out_specs=in_vmem(len(out_shape)) if many else pl.BlockSpec(memory_space=pl.ANY),
         out_shape=out_shape,
         scratch_shapes=scratch,
+        input_output_aliases=aliases,
         compiler_params=params(16),
         cost_estimate=pl.CostEstimate(flops=flops, bytes_accessed=1 << 22, transcendentals=0),
         name="project",
@@ -419,8 +419,7 @@
     across = exchanged(w_out, "dp", 2)
     beside = exchanged(w_out, "dp", 1)
     corner = exchanged(across, "dp", 1)
-    cos_table, sin_table = rotary_lanes(lax.axis_index("sp") * tok, tok)
-    both, kv = turn_and_pack(queries[0].T, keys[0].T, values[0].T, q_gain, k_gain, cos_table, sin_table, groups, chunks)
+    both, kv = turn_and_pack(queries[0].T, keys[0].T, values[0].T, q_gain, k_gain, groups, chunks)
     near, far = [], []
     for c in range(chunks):
         near.append([both[c][0]] + [exchanged(both[c][j], "sp", j) for j in range(1, groups)])
@@ -436,37 +435,37 @@
     held = jax.ShapeDtypeStruct((groups, deep, width), jnp.bfloat16)
     summed = jax.ShapeDtypeStruct((tok, width), jnp.float32)
     flops = 2 * tok * groups * deep * width
-    held_a, held_b, sum_a, sum_b = project_call(
+    held_a, held_b = project_call(
+        load_kernel, groups, [w_out, beside], [hbm] * 2, [held] * 2, [pltpu.SemaphoreType.DMA((2, groups))], flops
+    )
+    held_c, *sums = project_call(
         first_kernel,
         groups,
-        [*back[0], w_out, beside],
-        [vmem] * groups + [hbm] * 2,
-        [held] * 2 + [summed] * 2,
-        [pltpu.SemaphoreType.DMA((2, groups))],
-        flops,
-    )
-    held_c, *sums = project_call(
+        [*back[0], back[1][0], across, held_a, held_b],
+        [vmem] * (groups + 1) + [hbm] + [vmem] * 2,
+        [held] + [summed] * 3,
+        [pltpu.SemaphoreType.DMA((1, groups))],
+        2 * flops,
+    )
+    whole = jax.ShapeDtypeStruct((tok, 4 * width), jnp.bfloat16)
+    mixed = project_call(
         second_kernel,
         groups,
-        [*back[0], back[1][0], across, held_a, held_b, sum_a, sum_b],
-        [vmem] * (groups + 1) + [hbm] + [vmem] * 4,
-        [held] + [summed] * 3,
-        [pltpu.SemaphoreType.DMA((1, groups))],
+        [*back[1][1:], held_a, held_b, held_c, *sums],
+        [vmem] * (groups + 5),
+        whole,
+        [pltpu.VMEM((3, tok, width), jnp.bfloat16), pltpu.SemaphoreType.DMA((3,))],
         flops,
     )
     mixed = project_call(
         third_kernel,
         groups,
-        [*back[0], *back[1], corner, held_a, held_b, held_c, *sums],
-        [vmem] * (2 * groups) + [hbm] + [vmem] * 6,
-        jax.ShapeDtypeStruct((tok, 4 * width), jnp.bfloat16),
-        [
-            pltpu.VMEM(held.shape, held.dtype),
-            pltpu.VMEM((4, tok, width), jnp.bfloat16),
-            pltpu.SemaphoreType.DMA((1, groups)),
-            pltpu.SemaphoreType.DMA((4,)),
-        ],
-        2 * flops,
+        [*back[0], *back[1], corner, mixed],
+        [vmem] * (2 * groups + 1) + [hbm],
+        whole,
+        [pltpu.VMEM((tok, width), jnp.bfloat16), pltpu.SemaphoreType.DMA(())],
+        flops,
+        {2 * groups + 1: 0},
     )
     return mixed[None]
 

time: 121 us -> 119 us (0.983)
  Pallas kernels: 20.6 us -> 18.1 us
  waiting for transfers between devices: 57.2 us -> 58.8 us
    pallas_call x3 -> x4, Pallas kernels: 5.95 us -> 4.12 us  [project_call(): pl.pallas_call(functools.partial(kernel, groups), in_specs=[pl.BlockSpec(...]
    ppermute x23, waiting for transfers between devices: 57.2 us -> 58.8 us  [exchanged(): return lax.ppermute(block, axis, [(i, i ^ flip) for i in range(count)])]
  transfers between devices with their start and end apart: 23 -> 23, of which waited for: 6 -> 7; matrix products, arithmetic and copies ran while one was open for 1% -> 1% of each run, Pallas kernels for 15% -> 14%
where the time goes in v3:
time: 119 us
  waiting for transfers between devices  58.8 us (49%)
  starting transfers between devices  41.1 us (35%)
  Pallas kernels  18.1 us (15%)
    ppermute x23, waiting for transfers between devices, exchanged(): return lax.ppermute(block, axis, [(i, i ^ flip) for i in range(count)])  58.8 us
    ppermute x23, starting transfers between devices, exchanged(): return lax.ppermute(block, axis, [(i, i ^ flip) for i in range(count)])  41.1 us
    pallas_call x4, Pallas kernels, attend(): pl.pallas_call(functools.partial(attend_kernel, count), in_specs=in_vmem(...  10.6 us
    pallas_call x4, Pallas kernels, project_call(): pl.pallas_call(functools.partial(kernel, groups), in_specs=[pl.BlockSpec(...  4.12 us
    pallas_call x1, Pallas kernels, turn_and_pack(): pl.pallas_call(functools.partial(turn_kernel, groups, chunks), in_specs=[...  2.68 us
  transfers between devices with their start and end apart: 23, of which 7 were waited for; matrix products, arithmetic and copies ran while one was open for 1% of the time, Pallas kernels for 14%

profile of v3, /device:TPU:0, one launch (start us, length us, event | category | flops | bytes accessed | tf_op | source)
XLA Modules:
  0.0 119.1 jit_solution(1012386628716947501)
XLA Ops:
  0.0 3.0 %collective-permute-start.20 = (bf16[2048,512]{1,0:T(8,128)(2,1)}, bf16[2048,512]{1,0:T(8,128)(2,1)S(1)}, u32[]{:S(2)}, u32[]{:S(2)}) collective-permute-start(bf16[2048,512]{1,0:T(8,128)(2,1)} %refs_0_.1), channel_id=1, source_target_pairs={{0,2},{1,3},{2,0},{3,1},{4,6},{5,7},{6,4},{7,5},{8,10},{9,11},{10,... | collective-permute-start | bytes 6291464 | tf_op jit(solution)/shard_map/ppermute | solution.py:410
  3.0 0.0 collective-permute-start.22
  3.0 45.8 %collective-permute-done.20.refs_5_ = bf16[2048,512]{1,0:T(8,128)(2,1)S(1)} collective-permute-done((bf16[2048,512]{1,0:T(8,128)(2,1)}, bf16[2048,512]{1,0:T(8,128)(2,1)S(1)}, u32[]{:S(2)}, u32[]{:S(2)}) %collective-permute-start.20) | collective-permute-done | bytes 2097184 | tf_op jit(solution)/shard_map/ppermute | solution.py:410
  48.8 0.0 collective-permute-start.21
  48.8 0.8 maximum_bitcast_fusion.refs_3_
  49.6 2.7 %turn.1 = (bf16[160,512]{1,0:T(8,128)(2,1)S(1)}, bf16[160,512]{1,0:T(8,128)(2,1)S(1)}, bf16[160,512]{1,0:T(8,128)(2,1)S(1)}, bf16[160,512]{1,0:T(8,128)(2,1)S(1)...) custom-call(bf16[160,2048]{1,0:T(8,128)(2,1)} %bitcast.12, ...), custom_call_target="tpu_custom_call" | custom-call | flops 19660800 | bytes 3932160 | tf_op jit(solution)/shard_map/turn/pallas_call | solution.py:214
  52.3 2.9 %collective-permute-start.3 = (bf16[160,256]{1,0:T(8,128)(2,1)S(1)}, bf16[160,256]{1,0:T(8,128)(2,1)S(1)}, u32[]{:S(2)}, u32[]{:S(2)}) collective-permute-start(bf16[160,256]{1,0:T(8,128)(2,1)S(1)} %get-tuple-element.41), channel_id=1, source_target_pairs={{0,16},{4,20},{8,24},{12,28},{16,0},{20,4},{24,8},{28,12},{1,17},{... | collective-permute-start | bytes 245768 | tf_op jit(solution)/shard_map/ppermute | solution.py:410
  55.2 1.3 %collective-permute-start.4 = (bf16[160,256]{1,0:T(8,128)(2,1)S(1)}, bf16[160,256]{1,0:T(8,128)(2,1)S(1)}, u32[]{:S(2)}, u32[]{:S(2)}) collective-permute-start(bf16[160,256]{1,0:T(8,128)(2,1)S(1)} %get-tuple-element.42), channel_id=1, source_target_pairs={{0,20},{4,16},{8,28},{12,24},{16,4},{20,0},{24,12},{28,8},{1,21},{... | collective-permute-start | bytes 245768 | tf_op jit(solution)/shard_map/ppermute | solution.py:410
  56.5 3.6 %collective-permute-start.5 = (bf16[160,256]{1,0:T(8,128)(2,1)S(1)}, bf16[160,256]{1,0:T(8,128)(2,1)S(1)}, u32[]{:S(2)}, u32[]{:S(2)}) collective-permute-start(bf16[160,256]{1,0:T(8,128)(2,1)S(1)} %get-tuple-element.43), channel_id=1, source_target_pairs={{0,24},{4,28},{8,16},{12,20},{16,8},{20,12},{24,0},{28,4},{1,25},{... | collective-permute-start | bytes 245768 | tf_op jit(solution)/shard_map/ppermute | solution.py:410
  60.1 0.2 collective-permute-done.3.refs_4_
  60.3 7.8 %collective-permute-start.6 = (bf16[160,256]{1,0:T(8,128)(2,1)S(1)}, bf16[160,256]{1,0:T(8,128)(2,1)S(1)}, u32[]{:S(2)}, u32[]{:S(2)}) collective-permute-start(bf16[160,256]{1,0:T(8,128)(2,1)S(1)} %get-tuple-element.44), channel_id=1, source_target_pairs={{0,28},{4,24},{8,20},{12,16},{16,12},{20,8},{24,4},{28,0},{1,29},{... | collective-permute-start | bytes 245768 | tf_op jit(solution)/shard_map/ppermute | solution.py:410
  68.1 2.9 %collective-permute-start.14 = (bf16[160,256]{1,0:T(8,128)(2,1)S(1)}, bf16[160,256]{1,0:T(8,128)(2,1)S(1)}, u32[]{:S(2)}, u32[]{:S(2)}) collective-permute-start(bf16[160,256]{1,0:T(8,128)(2,1)S(1)} %get-tuple-element.55), channel_id=1, source_target_pairs={{0,20},{4,16},{8,28},{12,24},{16,4},{20,0},{24,12},{28,8},{1,21},{... | collective-permute-start | bytes 245768 | tf_op jit(solution)/shard_map/ppermute | solution.py:410
  71.0 0.0 collective-permute-done.6.refs_7_
  71.0 4.2 %collective-permute-start.15 = (bf16[160,256]{1,0:T(8,128)(2,1)S(1)}, bf16[160,256]{1,0:T(8,128)(2,1)S(1)}, u32[]{:S(2)}, u32[]{:S(2)}) collective-permute-start(bf16[160,256]{1,0:T(8,128)(2,1)S(1)} %get-tuple-element.56), channel_id=1, source_target_pairs={{0,24},{4,28},{8,16},{12,20},{16,8},{20,12},{24,0},{28,4},{1,25},{... | collective-permute-start | bytes 245768 | tf_op jit(solution)/shard_map/ppermute | solution.py:410
  75.2 3.2 %collective-permute-done.13.refs_4_ = bf16[160,256]{1,0:T(8,128)(2,1)S(1)} collective-permute-done((bf16[160,256]{1,0:T(8,128)(2,1)S(1)}, bf16[160,256]{1,0:T(8,128)(2,1)S(1)}, u32[]{:S(2)}, u32[]{:S(2)}) %collective-permute-start.13) | collective-permute-done | bytes 81952 | tf_op jit(solution)/shard_map/ppermute | solution.py:410
  78.4 2.9 %collective-permute-start.16 = (bf16[160,256]{1,0:T(8,128)(2,1)S(1)}, bf16[160,256]{1,0:T(8,128)(2,1)S(1)}, u32[]{:S(2)}, u32[]{:S(2)}) collective-permute-start(bf16[160,256]{1,0:T(8,128)(2,1)S(1)} %get-tuple-element.57), channel_id=1, source_target_pairs={{0,28},{4,24},{8,20},{12,16},{16,12},{20,8},{24,4},{28,0},{1,29},{... | collective-permute-start | bytes 245768 | tf_op jit(solution)/shard_map/ppermute | solution.py:410
  81.3 0.0 collective-permute-done.14.refs_5_
  81.3 0.7 collective-permute-start
  82.0 0.0 collective-permute-done.15.refs_6_
  82.0 1.4 %collective-permute-start.1 = (bf16[160,512]{1,0:T(8,128)(2,1)S(1)}, bf16[160,512]{1,0:T(8,128)(2,1)S(1)}, u32[]{:S(2)}, u32[]{:S(2)}) collective-permute-start(bf16[160,512]{1,0:T(8,128)(2,1)S(1)} %get-tuple-element.39), channel_id=1, source_target_pairs={{0,8},{4,12},{8,0},{12,4},{16,24},{20,28},{24,16},{28,20},{1,9},{5... | collective-permute-start | bytes 491528 | tf_op jit(solution)/shard_map/ppermute | solution.py:410
  83.4 2.3 %collective-permute-done.16.refs_7_ = bf16[160,256]{1,0:T(8,128)(2,1)S(1)} collective-permute-done((bf16[160,256]{1,0:T(8,128)(2,1)S(1)}, bf16[160,256]{1,0:T(8,128)(2,1)S(1)}, u32[]{:S(2)}, u32[]{:S(2)}) %collective-permute-start.16) | collective-permute-done | bytes 81952 | tf_op jit(solution)/shard_map/ppermute | solution.py:410
  85.6 1.3 %collective-permute-start.2 = (bf16[160,512]{1,0:T(8,128)(2,1)S(1)}, bf16[160,512]{1,0:T(8,128)(2,1)S(1)}, u32[]{:S(2)}, u32[]{:S(2)}) collective-permute-start(bf16[160,512]{1,0:T(8,128)(2,1)S(1)} %get-tuple-element.40), channel_id=1, source_target_pairs={{0,12},{4,8},{8,4},{12,0},{16,28},{20,24},{24,20},{28,16},{1,13},{... | collective-permute-start | bytes 491528 | tf_op jit(solution)/shard_map/ppermute | solution.py:410
  86.9 2.6 %collective-permute-done.refs_1_.refs_0_ = bf16[160,512]{1,0:T(8,128)(2,1)S(1)} collective-permute-done((bf16[160,512]{1,0:T(8,128)(2,1)S(1)}, bf16[160,512]{1,0:T(8,128)(2,1)S(1)}, u32[]{:S(2)}, u32[]{:S(2)}) %collective-permute-start) | collective-permute-done | bytes 163872 | tf_op jit(solution)/shard_map/ppermute | solution.py:410
  89.5 3.1 %collective-permute-done.2.refs_3_.refs_2_ = bf16[160,512]{1,0:T(8,128)(2,1)S(1)} collective-permute-done((bf16[160,512]{1,0:T(8,128)(2,1)S(1)}, bf16[160,512]{1,0:T(8,128)(2,1)S(1)}, u32[]{:S(2)}, u32[]{:S(2)}) %collective-permute-start.2) | collective-permute-done | bytes 163872 | tf_op jit(solution)/shard_map/ppermute | solution.py:410
  92.7 2.1 %collective-permute-start.12 = (bf16[160,512]{1,0:T(8,128)(2,1)S(1)}, bf16[160,512]{1,0:T(8,128)(2,1)S(1)}, u32[]{:S(2)}, u32[]{:S(2)}) collective-permute-start(bf16[160,512]{1,0:T(8,128)(2,1)S(1)} %get-tuple-element.53), channel_id=1, source_target_pairs={{0,12},{4,8},{8,4},{12,0},{16,28},{20,24},{24,20},{28,16},{1,13},{... | collective-permute-start | bytes 491528 | tf_op jit(solution)/shard_map/ppermute | solution.py:410
  94.7 0.4 spread.2
  95.1 3.7 %attend.5 = (bf16[160,256]{1,0:T(8,128)(2,1)S(1)}, bf16[160,256]{1,0:T(8,128)(2,1)S(1)}, bf16[160,256]{1,0:T(8,128)(2,1)S(1)}) custom-call(bf16[160,512]{1,0:T(8,128)(2,1)S(1)} %collective-permute-done.refs_1_.refs_0_, bf16[160,512]{1,0:T(8,128)(2,1)S(1)} %collective-permute-done.1.refs_2_.refs_1_, ...), custom_call_target="tpu_custom_call" | custom-call | flops 1258291200 | bytes 2621440 | tf_op jit(solution)/shard_map/attend/pallas_call | solution.py:297
  98.8 0.1 collective-permute-start.7
  98.9 0.0 collective-permute-done.11.refs_2_.refs_1_
  98.9 1.4 %collective-permute-start.8 = (bf16[160,256]{1,0:T(8,128)(2,1)S(1)}, bf16[160,256]{1,0:T(8,128)(2,1)S(1)}, u32[]{:S(2)}, u32[]{:S(2)}) collective-permute-start(bf16[160,256]{1,0:T(8,128)(2,1)S(1)} %get-tuple-element.48), channel_id=1, source_target_pairs={{0,8},{4,12},{8,0},{12,4},{16,24},{20,28},{24,16},{28,20},{1,9},{5... | collective-permute-start | bytes 245768 | tf_op jit(solution)/shard_map/ppermute | solution.py:410
  100.3 0.0 collective-permute-done.12.refs_3_.refs_2_
  100.3 2.1 %collective-permute-start.9 = (bf16[160,256]{1,0:T(8,128)(2,1)S(1)}, bf16[160,256]{1,0:T(8,128)(2,1)S(1)}, u32[]{:S(2)}, u32[]{:S(2)}) collective-permute-start(bf16[160,256]{1,0:T(8,128)(2,1)S(1)} %get-tuple-element.49), channel_id=1, source_target_pairs={{0,12},{4,8},{8,4},{12,0},{16,28},{20,24},{24,20},{28,16},{1,13},{... | collective-permute-start | bytes 245768 | tf_op jit(solution)/shard_map/ppermute | solution.py:410
  102.3 0.4 spread.3
  102.7 3.7 %attend.7 = (bf16[160,256]{1,0:T(8,128)(2,1)S(1)}, bf16[160,256]{1,0:T(8,128)(2,1)S(1)}, bf16[160,256]{1,0:T(8,128)(2,1)S(1)}) custom-call(bf16[160,512]{1,0:T(8,128)(2,1)S(1)} %collective-permute-done.10.refs_1_.refs_0_, bf16[160,512]{1,0:T(8,128)(2,1)S(1)} %collective-permute-done.11.refs_2_.refs_1_, ...), custom_call_target="tpu_custom_call" | custom-call | flops 1258291200 | bytes 2621440 | tf_op jit(solution)/shard_map/attend/pallas_call | solution.py:297
  106.4 1.7 %attend.4.refs_0_ = bf16[160,256]{1,0:T(8,128)(2,1)S(1)} custom-call(bf16[160,512]{1,0:T(8,128)(2,1)S(1)} %get-tuple-element.37.refs_0_, bf16[2,2560,128]{2,1,0:T(8,128)(2,1)S(1)} %get-tuple-element.45.refs_1_.refs_3_, bf16[2,2560,128]{2,1,0:T(8,128)(2,1)S(1)} %get-tuple-element.46.refs_2_.refs_4_), custom_call_target="tpu_custom_call" | custom-call | flops 419430400 | bytes 2621440 | tf_op jit(solution)/shard_map/attend/pallas_call | solution.py:297
  108.1 0.0 copy-start
  108.1 1.5 %attend.6.refs_4_ = bf16[160,256]{1,0:T(8,128)(2,1)S(1)} custom-call(bf16[160,512]{1,0:T(8,128)(2,1)S(1)} %get-tuple-element.50.refs_0_, bf16[2,2560,128]{2,1,0:T(8,128)(2,1)S(1)} %get-tuple-element.58.refs_1_.refs_3_, bf16[2,2560,128]{2,1,0:T(8,128)(2,1)S(1)} %get-tuple-element.59.refs_2_.refs_4_), custom_call_target="tpu_custom_call" | custom-call | flops 419430400 | bytes 2621440 | tf_op jit(solution)/shard_map/attend/pallas_call | solution.py:297
  109.6 0.2 collective-permute-start.17
  109.8 1.4 %collective-permute-start.18 = (bf16[160,256]{1,0:T(8,128)(2,1)S(1)}, bf16[160,256]{1,0:T(8,128)(2,1)S(1)}, u32[]{:S(2)}, u32[]{:S(2)}) collective-permute-start(bf16[160,256]{1,0:T(8,128)(2,1)S(1)} %get-tuple-element.61), channel_id=1, source_target_pairs={{0,8},{4,12},{8,0},{12,4},{16,24},{20,28},{24,16},{28,20},{1,9},{5... | collective-permute-start | bytes 245768 | tf_op jit(solution)/shard_map/ppermute | solution.py:410
  111.1 0.0 collective-permute-done.22.refs_1_
  111.1 2.1 %collective-permute-start.19 = (bf16[160,256]{1,0:T(8,128)(2,1)S(1)}, bf16[160,256]{1,0:T(8,128)(2,1)S(1)}, u32[]{:S(2)}, u32[]{:S(2)}) collective-permute-start(bf16[160,256]{1,0:T(8,128)(2,1)S(1)} %get-tuple-element.62), channel_id=1, source_target_pairs={{0,12},{4,8},{8,4},{12,0},{16,28},{20,24},{24,20},{28,16},{1,13},{... | collective-permute-start | bytes 245768 | tf_op jit(solution)/shard_map/ppermute | solution.py:410
  113.2 0.4 project.4
  113.6 0.0 collective-permute-done.9.refs_3_
  113.6 1.3 %project.5 = (bf16[4,512,512]{2,1,0:T(8,128)(2,1)S(1)}, f32[160,512]{1,0:T(8,128)S(1)}, f32[160,512]{1,0:T(8,128)S(1)}, f32[160,512]{1,0:T(8,128)S(1)}) custom-call(bf16[160,256]{1,0:T(8,128)(2,1)S(1)} %attend.4.refs_0_, bf16[160,256]{1,0:T(8,128)(2,1)S(1)} %collective-permute-done.7.refs_1_, bf16[160,256]{1,0:T(8,128)(2,1)S(1)} %collective-permute-done.8.refs_2_, ...), custom_call_target="tpu_custom_call" | custom-call | flops 671088640 | bytes 4194304 | tf_op jit(solution)/shard_map/project/pallas_call | solution.py:395
  114.9 0.0 collective-permute-done.18.refs_1_.refs_6_
  114.9 1.6 %collective-permute-done.19.refs_2_.refs_7_ = bf16[160,256]{1,0:T(8,128)(2,1)S(1)} collective-permute-done((bf16[160,256]{1,0:T(8,128)(2,1)S(1)}, bf16[160,256]{1,0:T(8,128)(2,1)S(1)}, u32[]{:S(2)}, u32[]{:S(2)}) %collective-permute-start.19) | collective-permute-done | bytes 81952 | tf_op jit(solution)/shard_map/ppermute | solution.py:410
  116.5 1.2 %project.6.refs_9_ = bf16[160,2048]{1,0:T(8,128)(2,1)} custom-call(bf16[160,256]{1,0:T(8,128)(2,1)S(1)} %collective-permute-done.17.refs_0_.refs_5_, bf16[160,256]{1,0:T(8,128)(2,1)S(1)} %collective-permute-done.18.refs_1_.refs_6_, bf16[160,256]{1,0:T(8,128)(2,1)S(1)} %collective-permute-done.19.refs_2_.refs_7_, ...), custom_call_target="tpu_custom_call" | custom-call | flops 335544320 | bytes 4194304 | tf_op jit(solution)/shard_map/project/pallas_call | solution.py:395
  117.7 1.2 %project.7 = bf16[160,2048]{1,0:T(8,128)(2,1)} custom-call(bf16[160,256]{1,0:T(8,128)(2,1)S(1)} %attend.4.refs_0_, bf16[160,256]{1,0:T(8,128)(2,1)S(1)} %collective-permute-done.7.refs_1_, bf16[160,256]{1,0:T(8,128)(2,1)S(1)} %collective-permute-done.8.refs_2_, bf16[160,256]{1,0:T(8,128)(2,1)S(1)} %collective-permute-done.9.refs_3_, ...), custom_call_target="tpu_custom_call", output_to_operand_aliasing={{}: (9, {})} | custom-call | flops 335544320 | bytes 4194304 | tf_op jit(solution)/shard_map/project/pallas_call | solution.py:395
  (12 shorter events, 0.0 us)
Async XLA Ops:
  0.0 48.8 %collective-permute-start.20 = (bf16[2048,512]{1,0:T(8,128)(2,1)}, bf16[2048,512]{1,0:T(8,128)(2,1)S(1)}, u32[]{:S(2)}, u32[]{:S(2)}) collective-permute-start(bf16[2048,512]{1,0:T(8,128)(2,1)} %refs_0_.1), channel_id=1, source_target_pairs={{0,2},{1,3},{2,0},{3,1},{4,6},{5,7},{6,4},{7,5},{8,10},{9,11},{10,... | collective-permute-start | bytes 6291464 | tf_op jit(solution)/shard_map/ppermute | solution.py:410
  3.0 108.2 %collective-permute-start.22 = (bf16[2048,512]{1,0:T(8,128)(2,1)}, bf16[2048,512]{1,0:T(8,128)(2,1)S(1)}, u32[]{:S(2)}, u32[]{:S(2)}) collective-permute-start(bf16[2048,512]{1,0:T(8,128)(2,1)} %refs_0_.1), channel_id=1, source_target_pairs={{0,1},{1,0},{2,3},{3,2},{4,5},{5,4},{6,7},{7,6},{8,9},{9,8},{10,11... | collective-permute-start | bytes 6291464 | tf_op jit(solution)/shard_map/ppermute | solution.py:410
  48.8 68.9 %collective-permute-start.21 = (bf16[2048,512]{1,0:T(8,128)(2,1)S(1)}, bf16[2048,512]{1,0:T(8,128)(2,1)S(1)}, u32[]{:S(2)}, u32[]{:S(2)}) collective-permute-start(bf16[2048,512]{1,0:T(8,128)(2,1)S(1)} %collective-permute-done.20.refs_5_), channel_id=1, source_target_pairs={{0,1},{1,0},{2,3},{3,2},{4,5},{5,4},{6,7},{7,6},{8,9},{9,8},{10,11... | collective-permute-start | bytes 6291464 | tf_op jit(solution)/shard_map/ppermute | solution.py:410
  52.3 8.0 %collective-permute-start.3 = (bf16[160,256]{1,0:T(8,128)(2,1)S(1)}, bf16[160,256]{1,0:T(8,128)(2,1)S(1)}, u32[]{:S(2)}, u32[]{:S(2)}) collective-permute-start(bf16[160,256]{1,0:T(8,128)(2,1)S(1)} %get-tuple-element.41), channel_id=1, source_target_pairs={{0,16},{4,20},{8,24},{12,28},{16,0},{20,4},{24,8},{28,12},{1,17},{... | collective-permute-start | bytes 245768 | tf_op jit(solution)/shard_map/ppermute | solution.py:410
  55.2 12.9 %collective-permute-start.4 = (bf16[160,256]{1,0:T(8,128)(2,1)S(1)}, bf16[160,256]{1,0:T(8,128)(2,1)S(1)}, u32[]{:S(2)}, u32[]{:S(2)}) collective-permute-start(bf16[160,256]{1,0:T(8,128)(2,1)S(1)} %get-tuple-element.42), channel_id=1, source_target_pairs={{0,20},{4,16},{8,28},{12,24},{16,4},{20,0},{24,12},{28,8},{1,21},{... | collective-permute-start | bytes 245768 | tf_op jit(solution)/shard_map/ppermute | solution.py:410
  56.5 11.6 %collective-permute-start.5 = (bf16[160,256]{1,0:T(8,128)(2,1)S(1)}, bf16[160,256]{1,0:T(8,128)(2,1)S(1)}, u32[]{:S(2)}, u32[]{:S(2)}) collective-permute-start(bf16[160,256]{1,0:T(8,128)(2,1)S(1)} %get-tuple-element.43), channel_id=1, source_target_pairs={{0,24},{4,28},{8,16},{12,20},{16,8},{20,12},{24,0},{28,4},{1,25},{... | collective-permute-start | bytes 245768 | tf_op jit(solution)/shard_map/ppermute | solution.py:410
  60.3 10.7 %collective-permute-start.6 = (bf16[160,256]{1,0:T(8,128)(2,1)S(1)}, bf16[160,256]{1,0:T(8,128)(2,1)S(1)}, u32[]{:S(2)}, u32[]{:S(2)}) collective-permute-start(bf16[160,256]{1,0:T(8,128)(2,1)S(1)} %get-tuple-element.44), channel_id=1, source_target_pairs={{0,28},{4,24},{8,20},{12,16},{16,12},{20,8},{24,4},{28,0},{1,29},{... | collective-permute-start | bytes 245768 | tf_op jit(solution)/shard_map/ppermute | solution.py:410
  68.1 10.3 %collective-permute-start.13 = (bf16[160,256]{1,0:T(8,128)(2,1)S(1)}, bf16[160,256]{1,0:T(8,128)(2,1)S(1)}, u32[]{:S(2)}, u32[]{:S(2)}) collective-permute-start(bf16[160,256]{1,0:T(8,128)(2,1)S(1)} %get-tuple-element.54), channel_id=1, source_target_pairs={{0,16},{4,20},{8,24},{12,28},{16,0},{20,4},{24,8},{28,12},{1,17},{... | collective-permute-start | bytes 245768 | tf_op jit(solution)/shard_map/ppermute | solution.py:410
  68.1 13.2 %collective-permute-start.14 = (bf16[160,256]{1,0:T(8,128)(2,1)S(1)}, bf16[160,256]{1,0:T(8,128)(2,1)S(1)}, u32[]{:S(2)}, u32[]{:S(2)}) collective-permute-start(bf16[160,256]{1,0:T(8,128)(2,1)S(1)} %get-tuple-element.55), channel_id=1, source_target_pairs={{0,20},{4,16},{8,28},{12,24},{16,4},{20,0},{24,12},{28,8},{1,21},{... | collective-permute-start | bytes 245768 | tf_op jit(solution)/shard_map/ppermute | solution.py:410
  71.0 11.0 %collective-permute-start.15 = (bf16[160,256]{1,0:T(8,128)(2,1)S(1)}, bf16[160,256]{1,0:T(8,128)(2,1)S(1)}, u32[]{:S(2)}, u32[]{:S(2)}) collective-permute-start(bf16[160,256]{1,0:T(8,128)(2,1)S(1)} %get-tuple-element.56), channel_id=1, source_target_pairs={{0,24},{4,28},{8,16},{12,20},{16,8},{20,12},{24,0},{28,4},{1,25},{... | collective-permute-start | bytes 245768 | tf_op jit(solution)/shard_map/ppermute | solution.py:410
  78.4 7.2 %collective-permute-start.16 = (bf16[160,256]{1,0:T(8,128)(2,1)S(1)}, bf16[160,256]{1,0:T(8,128)(2,1)S(1)}, u32[]{:S(2)}, u32[]{:S(2)}) collective-permute-start(bf16[160,256]{1,0:T(8,128)(2,1)S(1)} %get-tuple-element.57), channel_id=1, source_target_pairs={{0,28},{4,24},{8,20},{12,16},{16,12},{20,8},{24,4},{28,0},{1,29},{... | collective-permute-start | bytes 245768 | tf_op jit(solution)/shard_map/ppermute | solution.py:410
  81.3 8.2 %collective-permute-start = (bf16[160,512]{1,0:T(8,128)(2,1)S(1)}, bf16[160,512]{1,0:T(8,128)(2,1)S(1)}, u32[]{:S(2)}, u32[]{:S(2)}) collective-permute-start(bf16[160,512]{1,0:T(8,128)(2,1)S(1)} %get-tuple-element.38), channel_id=1, source_target_pairs={{0,4},{4,0},{8,12},{12,8},{16,20},{20,16},{24,28},{28,24},{1,5},{5... | collective-permute-start | bytes 491528 | tf_op jit(solution)/shard_map/ppermute | solution.py:410
  82.0 7.5 %collective-permute-start.1 = (bf16[160,512]{1,0:T(8,128)(2,1)S(1)}, bf16[160,512]{1,0:T(8,128)(2,1)S(1)}, u32[]{:S(2)}, u32[]{:S(2)}) collective-permute-start(bf16[160,512]{1,0:T(8,128)(2,1)S(1)} %get-tuple-element.39), channel_id=1, source_target_pairs={{0,8},{4,12},{8,0},{12,4},{16,24},{20,28},{24,16},{28,20},{1,9},{5... | collective-permute-start | bytes 491528 | tf_op jit(solution)/shard_map/ppermute | solution.py:410
  85.6 7.0 %collective-permute-start.2 = (bf16[160,512]{1,0:T(8,128)(2,1)S(1)}, bf16[160,512]{1,0:T(8,128)(2,1)S(1)}, u32[]{:S(2)}, u32[]{:S(2)}) collective-permute-start(bf16[160,512]{1,0:T(8,128)(2,1)S(1)} %get-tuple-element.40), channel_id=1, source_target_pairs={{0,12},{4,8},{8,4},{12,0},{16,28},{20,24},{24,20},{28,16},{1,13},{... | collective-permute-start | bytes 491528 | tf_op jit(solution)/shard_map/ppermute | solution.py:410
  89.5 9.3 %collective-permute-start.10 = (bf16[160,512]{1,0:T(8,128)(2,1)S(1)}, bf16[160,512]{1,0:T(8,128)(2,1)S(1)}, u32[]{:S(2)}, u32[]{:S(2)}) collective-permute-start(bf16[160,512]{1,0:T(8,128)(2,1)S(1)} %get-tuple-element.51), channel_id=1, source_target_pairs={{0,4},{4,0},{8,12},{12,8},{16,20},{20,16},{24,28},{28,24},{1,5},{5... | collective-permute-start | bytes 491528 | tf_op jit(solution)/shard_map/ppermute | solution.py:410
  89.5 9.3 %collective-permute-start.11 = (bf16[160,512]{1,0:T(8,128)(2,1)S(1)}, bf16[160,512]{1,0:T(8,128)(2,1)S(1)}, u32[]{:S(2)}, u32[]{:S(2)}) collective-permute-start(bf16[160,512]{1,0:T(8,128)(2,1)S(1)} %get-tuple-element.52), channel_id=1, source_target_pairs={{0,8},{4,12},{8,0},{12,4},{16,24},{20,28},{24,16},{28,20},{1,9},{5... | collective-permute-start | bytes 491528 | tf_op jit(solution)/shard_map/ppermute | solution.py:410
  92.7 7.6 %collective-permute-start.12 = (bf16[160,512]{1,0:T(8,128)(2,1)S(1)}, bf16[160,512]{1,0:T(8,128)(2,1)S(1)}, u32[]{:S(2)}, u32[]{:S(2)}) collective-permute-start(bf16[160,512]{1,0:T(8,128)(2,1)S(1)} %get-tuple-element.53), channel_id=1, source_target_pairs={{0,12},{4,8},{8,4},{12,0},{16,28},{20,24},{24,20},{28,16},{1,13},{... | collective-permute-start | bytes 491528 | tf_op jit(solution)/shard_map/ppermute | solution.py:410
  98.8 10.8 %collective-permute-start.7 = (bf16[160,256]{1,0:T(8,128)(2,1)S(1)}, bf16[160,256]{1,0:T(8,128)(2,1)S(1)}, u32[]{:S(2)}, u32[]{:S(2)}) collective-permute-start(bf16[160,256]{1,0:T(8,128)(2,1)S(1)} %get-tuple-element.47), channel_id=1, source_target_pairs={{0,4},{4,0},{8,12},{12,8},{16,20},{20,16},{24,28},{28,24},{1,5},{5... | collective-permute-start | bytes 245768 | tf_op jit(solution)/shard_map/ppermute | solution.py:410
  98.9 10.9 %collective-permute-start.8 = (bf16[160,256]{1,0:T(8,128)(2,1)S(1)}, bf16[160,256]{1,0:T(8,128)(2,1)S(1)}, u32[]{:S(2)}, u32[]{:S(2)}) collective-permute-start(bf16[160,256]{1,0:T(8,128)(2,1)S(1)} %get-tuple-element.48), channel_id=1, source_target_pairs={{0,8},{4,12},{8,0},{12,4},{16,24},{20,28},{24,16},{28,20},{1,9},{5... | collective-permute-start | bytes 245768 | tf_op jit(solution)/shard_map/ppermute | solution.py:410
  100.3 13.3 %collective-permute-start.9 = (bf16[160,256]{1,0:T(8,128)(2,1)S(1)}, bf16[160,256]{1,0:T(8,128)(2,1)S(1)}, u32[]{:S(2)}, u32[]{:S(2)}) collective-permute-start(bf16[160,256]{1,0:T(8,128)(2,1)S(1)} %get-tuple-element.49), channel_id=1, source_target_pairs={{0,12},{4,8},{8,4},{12,0},{16,28},{20,24},{24,20},{28,16},{1,13},{... | collective-permute-start | bytes 245768 | tf_op jit(solution)/shard_map/ppermute | solution.py:410
  108.1 5.1 %copy-start = (bf16[2048,512]{1,0:T(8,128)(2,1)S(1)}, bf16[2048,512]{1,0:T(8,128)(2,1)}, u32[]{:S(2)}) copy-start(bf16[2048,512]{1,0:T(8,128)(2,1)} %refs_0_.1) | copy-start | bytes 6291460
  109.6 5.3 %collective-permute-start.17 = (bf16[160,256]{1,0:T(8,128)(2,1)S(1)}, bf16[160,256]{1,0:T(8,128)(2,1)S(1)}, u32[]{:S(2)}, u32[]{:S(2)}) collective-permute-start(bf16[160,256]{1,0:T(8,128)(2,1)S(1)} %get-tuple-element.60), channel_id=1, source_target_pairs={{0,4},{4,0},{8,12},{12,8},{16,20},{20,16},{24,28},{28,24},{1,5},{5... | collective-permute-start | bytes 245768 | tf_op jit(solution)/shard_map/ppermute | solution.py:410
  109.8 5.1 %collective-permute-start.18 = (bf16[160,256]{1,0:T(8,128)(2,1)S(1)}, bf16[160,256]{1,0:T(8,128)(2,1)S(1)}, u32[]{:S(2)}, u32[]{:S(2)}) collective-permute-start(bf16[160,256]{1,0:T(8,128)(2,1)S(1)} %get-tuple-element.61), channel_id=1, source_target_pairs={{0,8},{4,12},{8,0},{12,4},{16,24},{20,28},{24,16},{28,20},{1,9},{5... | collective-permute-start | bytes 245768 | tf_op jit(solution)/shard_map/ppermute | solution.py:410
  111.1 5.3 %collective-permute-start.19 = (bf16[160,256]{1,0:T(8,128)(2,1)S(1)}, bf16[160,256]{1,0:T(8,128)(2,1)S(1)}, u32[]{:S(2)}, u32[]{:S(2)}) collective-permute-start(bf16[160,256]{1,0:T(8,128)(2,1)S(1)} %get-tuple-element.62), channel_id=1, source_target_pairs={{0,12},{4,8},{8,4},{12,0},{16,28},{20,24},{24,20},{28,16},{1,13},{... | collective-permute-start | bytes 245768 | tf_op jit(solution)/shard_map/ppermute | solution.py:410

commit v4 on v3

--- a/solution.py
+++ b/solution.py
@@ -315,90 +315,60 @@
     return lax.axis_index("sp") % groups
 
 
-def loads(sources, held, sems, groups):
-    copies = []
-    for i, source in enumerate(sources):
-        deep = source.shape[0] // groups
-        rows = [pl.ds(pl.multiple_of((home_of(groups) ^ j) * deep, deep), deep) for j in range(groups)]
-        copies.append(
-            [pltpu.make_async_copy(source.at[rows[j], :], held[i].at[j], sems.at[i, j]) for j in range(groups)]
-        )
-    for row in copies:
-        for copy in row:
-            copy.start()
-    return copies
-
-
-def term(att_ref, held_ref, j, c):
-    rows = slice(c * 2 * TILE, (c + 1) * 2 * TILE)
-    return jnp.dot(att_ref[...], held_ref[j, rows, :], preferred_element_type=jnp.float32)
-
-
-def load_kernel(groups, *refs):
-    for row in loads(refs[0:2], refs[2:4], refs[4], groups):
-        for copy in row:
-            copy.wait()
+def term(att_ref, w_ref, groups, j, c):
+    deep = w_ref.shape[0] // groups
+    start = pl.multiple_of((home_of(groups) ^ j) * deep + c * 2 * TILE, 2 * TILE)
+    return jnp.dot(att_ref[...], w_ref[pl.ds(start, 2 * TILE), :], preferred_element_type=jnp.float32)
 
 
 def first_kernel(groups, *refs):
-    att_refs, own_ref, source, refs = refs[:groups], refs[groups], refs[groups + 1], refs[groups + 2 :]
-    held, last, sums, sems = refs[0:2], refs[2], refs[3:6], refs[6]
-    copies = loads([source], [last], sems, groups)
-    for i, held_ref in enumerate((*held, last)):
-        total = None
+    att_refs, own_ref, w_refs, sums = refs[:groups], refs[groups], refs[groups + 1 : groups + 4], refs[groups + 4 :]
+    for w_ref, sum_ref in zip(w_refs, sums):
+        total = term(own_ref, w_ref, groups, 0, 1)
         for j in range(groups):
-            if i == 2:
-                copies[0][j].wait()
-            part = term(att_refs[j], held_ref, j, 0)
-            total = part if total is None else total + part
-        sums[i][...] = total + term(own_ref, held_ref, 0, 1)
-
-
-def corner_rows(source, groups, j, c):
-    deep = source.shape[0] // groups
-    return pl.ds(pl.multiple_of((home_of(groups) ^ j) * deep + c * 2 * TILE, 2 * TILE), 2 * TILE)
-
-
-def leave(total, i, width, made, out_ref, sem):
-    made[...] = total.astype(jnp.bfloat16)
-    column = pl.ds(pl.multiple_of((lax.axis_index("dp") ^ i) * width, width), width)
-    copy = pltpu.make_async_copy(made, out_ref.at[:, column], sem)
-    copy.start()
-    return copy
+            total = total + term(att_refs[j], w_ref, groups, j, 0)
+        sum_ref[...] = total
 
 
 def second_kernel(groups, *refs):
-    att_refs, held, sums, (out_ref, made, sems) = refs[:-9], refs[-9:-6], refs[-6:-3], refs[-3:]
-    leaving = []
-    for i in range(3):
-        total = sums[i][...]
+    att_refs, w_refs, sums, made = refs[:-9], refs[-9:-6], refs[-6:-3], refs[-3:]
+    for w_ref, sum_ref, made_ref in zip(w_refs, sums, made):
+        total = sum_ref[...]
         for j in range(1, groups):
-            total = total + term(att_refs[j - 1], held[i], j, 1)
-        leaving.append(leave(total, i, held[i].shape[2], made.at[i], out_ref, sems.at[i]))
-    for copy in leaving:
-        copy.wait()
+            total = total + term(att_refs[j - 1], w_ref, groups, j, 1)
+        made_ref[...] = total.astype(jnp.bfloat16)
 
 
 def third_kernel(groups, *refs):
-    parts, (source, _, out_ref, made, sem) = (refs[:groups], refs[groups : 2 * groups]), refs[2 * groups :]
+    parts, refs = (refs[:groups], refs[groups : 2 * groups]), refs[2 * groups :]
+    source, made, (out_ref, last, sems) = refs[0], refs[1:4], refs[4:]
+    width = source.shape[1]
+
+    def leave(i, ready):
+        column = pl.ds(pl.multiple_of((lax.axis_index("dp") ^ i) * width, width), width)
+        copy = pltpu.make_async_copy(ready, out_ref.at[:, column], sems.at[i])
+        copy.start()
+        return copy
+
+    leaving = [leave(i, ready) for i, ready in enumerate(made)]
     total = None
     for c in range(2):
         for j in range(groups):
-            rows = corner_rows(source, groups, j, c)
-            part = jnp.dot(parts[c][j][...], source[rows, :], preferred_element_type=jnp.float32)
+            part = term(parts[c][j], source, groups, j, c)
             total = part if total is None else total + part
-    leave(total, 3, source.shape[1], made, out_ref, sem).wait()
-
-
-def project_call(kernel, groups, inputs, spaces, out_shape, scratch, flops, aliases={}):
+    last[...] = total.astype(jnp.bfloat16)
+    for copy in leaving + [leave(3, last)]:
+        copy.wait()
+
+
+def project_call(kernel, groups, inputs, out_shape, scratch, flops):
     many = isinstance(out_shape, list)
     return pl.pallas_call(
         functools.partial(kernel, groups),
-        in_specs=[pl.BlockSpec(memory_space=space) for space in spaces],
+        in_specs=in_vmem(len(inputs)),
         out_specs=in_vmem(len(out_shape)) if many else pl.BlockSpec(memory_space=pl.ANY),
         out_shape=out_shape,
         scratch_shapes=scratch,
-        input_output_aliases=aliases,
         compiler_params=params(16),
         cost_estimate=pl.CostEstimate(flops=flops, bytes_accessed=1 << 22, transcendentals=0),
         name="project",
@@ -415,7 +385,7 @@
     tok = queries.shape[2]
     groups = sp_count // 2
     chunks = KV // groups // 2
-    deep, width = w_out.shape[0] // groups, w_out.shape[1]
+    width = w_out.shape[1]
     across = exchanged(w_out, "dp", 2)
     beside = exchanged(w_out, "dp", 1)
     corner = exchanged(across, "dp", 1)
@@ -431,41 +401,22 @@
         local = attend(near[c][:1], *ready)
         back.append(list(local) + [exchanged(away[j - 1], "sp", j) for j in range(1, groups)])
 
-    vmem, hbm = pltpu.VMEM, pl.ANY
-    held = jax.ShapeDtypeStruct((groups, deep, width), jnp.bfloat16)
-    summed = jax.ShapeDtypeStruct((tok, width), jnp.float32)
-    flops = 2 * tok * groups * deep * width
-    held_a, held_b = project_call(
-        load_kernel, groups, [w_out, beside], [hbm] * 2, [held] * 2, [pltpu.SemaphoreType.DMA((2, groups))], flops
-    )
-    held_c, *sums = project_call(
-        first_kernel,
-        groups,
-        [*back[0], back[1][0], across, held_a, held_b],
-        [vmem] * (groups + 1) + [hbm] + [vmem] * 2,
-        [held] + [summed] * 3,
-        [pltpu.SemaphoreType.DMA((1, groups))],
-        2 * flops,
-    )
-    whole = jax.ShapeDtypeStruct((tok, 4 * width), jnp.bfloat16)
-    mixed = project_call(
-        second_kernel,
-        groups,
-        [*back[1][1:], held_a, held_b, held_c, *sums],
-        [vmem] * (groups + 5),
-        whole,
-        [pltpu.VMEM((3, tok, width), jnp.bfloat16), pltpu.SemaphoreType.DMA((3,))],
-        flops,
+    near_blocks = [w_out, beside, across]
+    block = lambda dtype: jax.ShapeDtypeStruct((tok, width), dtype)
+    flops = 2 * tok * w_out.shape[0] * width
+    sums = project_call(
+        first_kernel, groups, [*back[0], back[1][0], *near_blocks], [block(jnp.float32)] * 3, [], 2 * flops
+    )
+    made = project_call(
+        second_kernel, groups, [*back[1][1:], *near_blocks, *sums], [block(jnp.bfloat16)] * 3, [], flops
     )
     mixed = project_call(
         third_kernel,
         groups,
-        [*back[0], *back[1], corner, mixed],
-        [vmem] * (2 * groups + 1) + [hbm],
-        whole,
-        [pltpu.VMEM((tok, width), jnp.bfloat16), pltpu.SemaphoreType.DMA(())],
+        [*back[0], *back[1], corner, *made],
+        jax.ShapeDtypeStruct((tok, 4 * width), jnp.bfloat16),
+        [pltpu.VMEM((tok, width), jnp.bfloat16), pltpu.SemaphoreType.DMA((4,))],
         flops,
-        {2 * groups + 1: 0},
     )
     return mixed[None]
 

time: 119 us -> 117 us (0.983)
  Pallas kernels: 18.1 us -> 16.6 us
    pallas_call x4 -> x3, Pallas kernels: 4.12 us -> 2.6 us  [project_call(): pl.pallas_call(functools.partial(kernel, groups), in_specs=in_vmem(len(in...]
  transfers between devices with their start and end apart: 23 -> 23, of which waited for: 7 -> 7; matrix products, arithmetic and copies ran while one was open for 1% -> 1% of each run, Pallas kernels for 14% -> 13%
where the time goes in v4:
time: 117 us
  waiting for transfers between devices  58.2 us (50%)
  starting transfers between devices  41.1 us (35%)
  Pallas kernels  16.6 us (14%)
    ppermute x23, waiting for transfers between devices, exchanged(): return lax.ppermute(block, axis, [(i, i ^ flip) for i in range(count)])  58.2 us
    ppermute x23, starting transfers between devices, exchanged(): return lax.ppermute(block, axis, [(i, i ^ flip) for i in range(count)])  41.1 us
    pallas_call x4, Pallas kernels, attend(): pl.pallas_call(functools.partial(attend_kernel, count), in_specs=in_vmem(...  10.6 us
    pallas_call x1, Pallas kernels, turn_and_pack(): pl.pallas_call(functools.partial(turn_kernel, groups, chunks), in_specs=[...  2.68 us
    pallas_call x3, Pallas kernels, project_call(): pl.pallas_call(functools.partial(kernel, groups), in_specs=in_vmem(len(in...  2.6 us
  transfers between devices with their start and end apart: 23, of which 7 were waited for; matrix products, arithmetic and copies ran while one was open for 1% of the time, Pallas kernels for 13%

profile of v4, /device:TPU:0, one launch (start us, length us, event | category | flops | bytes accessed | tf_op | source)
XLA Modules:
  0.0 117.0 jit_solution(3612463625301871179)
XLA Ops:
  0.0 3.0 %collective-permute-start.20 = (bf16[2048,512]{1,0:T(8,128)(2,1)}, bf16[2048,512]{1,0:T(8,128)(2,1)S(1)}, u32[]{:S(2)}, u32[]{:S(2)}) collective-permute-start(bf16[2048,512]{1,0:T(8,128)(2,1)} %refs_3_.1), channel_id=1, source_target_pairs={{0,2},{1,3},{2,0},{3,1},{4,6},{5,7},{6,4},{7,5},{8,10},{9,11},{10,... | collective-permute-start | bytes 6291464 | tf_op jit(solution)/shard_map/ppermute | solution.py:380
  3.0 0.0 collective-permute-start.22
  3.0 45.8 %collective-permute-done.20.refs_7_.refs_5_ = bf16[2048,512]{1,0:T(8,128)(2,1)S(1)} collective-permute-done((bf16[2048,512]{1,0:T(8,128)(2,1)}, bf16[2048,512]{1,0:T(8,128)(2,1)S(1)}, u32[]{:S(2)}, u32[]{:S(2)}) %collective-permute-start.20) | collective-permute-done | bytes 2097184 | tf_op jit(solution)/shard_map/ppermute | solution.py:380
  48.8 0.0 collective-permute-start.21
  48.8 0.8 maximum_bitcast_fusion.refs_3_
  49.6 2.7 %turn.1 = (bf16[160,512]{1,0:T(8,128)(2,1)S(1)}, bf16[160,512]{1,0:T(8,128)(2,1)S(1)}, bf16[160,512]{1,0:T(8,128)(2,1)S(1)}, bf16[160,512]{1,0:T(8,128)(2,1)S(1)...) custom-call(bf16[160,2048]{1,0:T(8,128)(2,1)} %bitcast.12, ...), custom_call_target="tpu_custom_call" | custom-call | flops 19660800 | bytes 3932160 | tf_op jit(solution)/shard_map/turn/pallas_call | solution.py:214
  52.3 2.9 %collective-permute-start.3 = (bf16[160,256]{1,0:T(8,128)(2,1)S(1)}, bf16[160,256]{1,0:T(8,128)(2,1)S(1)}, u32[]{:S(2)}, u32[]{:S(2)}) collective-permute-start(bf16[160,256]{1,0:T(8,128)(2,1)S(1)} %get-tuple-element.41), channel_id=1, source_target_pairs={{0,16},{4,20},{8,24},{12,28},{16,0},{20,4},{24,8},{28,12},{1,17},{... | collective-permute-start | bytes 245768 | tf_op jit(solution)/shard_map/ppermute | solution.py:380
  55.2 1.3 %collective-permute-start.4 = (bf16[160,256]{1,0:T(8,128)(2,1)S(1)}, bf16[160,256]{1,0:T(8,128)(2,1)S(1)}, u32[]{:S(2)}, u32[]{:S(2)}) collective-permute-start(bf16[160,256]{1,0:T(8,128)(2,1)S(1)} %get-tuple-element.42), channel_id=1, source_target_pairs={{0,20},{4,16},{8,28},{12,24},{16,4},{20,0},{24,12},{28,8},{1,21},{... | collective-permute-start | bytes 245768 | tf_op jit(solution)/shard_map/ppermute | solution.py:380
  56.5 3.6 %collective-permute-start.5 = (bf16[160,256]{1,0:T(8,128)(2,1)S(1)}, bf16[160,256]{1,0:T(8,128)(2,1)S(1)}, u32[]{:S(2)}, u32[]{:S(2)}) collective-permute-start(bf16[160,256]{1,0:T(8,128)(2,1)S(1)} %get-tuple-element.43), channel_id=1, source_target_pairs={{0,24},{4,28},{8,16},{12,20},{16,8},{20,12},{24,0},{28,4},{1,25},{... | collective-permute-start | bytes 245768 | tf_op jit(solution)/shard_map/ppermute | solution.py:380
  60.1 0.2 collective-permute-done.3.refs_4_
  60.3 7.8 %collective-permute-start.6 = (bf16[160,256]{1,0:T(8,128)(2,1)S(1)}, bf16[160,256]{1,0:T(8,128)(2,1)S(1)}, u32[]{:S(2)}, u32[]{:S(2)}) collective-permute-start(bf16[160,256]{1,0:T(8,128)(2,1)S(1)} %get-tuple-element.44), channel_id=1, source_target_pairs={{0,28},{4,24},{8,20},{12,16},{16,12},{20,8},{24,4},{28,0},{1,29},{... | collective-permute-start | bytes 245768 | tf_op jit(solution)/shard_map/ppermute | solution.py:380
  68.1 0.0 collective-permute-done.4.refs_5_
  68.1 0.0 collective-permute-start.13
  68.1 2.9 %collective-permute-start.14 = (bf16[160,256]{1,0:T(8,128)(2,1)S(1)}, bf16[160,256]{1,0:T(8,128)(2,1)S(1)}, u32[]{:S(2)}, u32[]{:S(2)}) collective-permute-start(bf16[160,256]{1,0:T(8,128)(2,1)S(1)} %get-tuple-element.55), channel_id=1, source_target_pairs={{0,20},{4,16},{8,28},{12,24},{16,4},{20,0},{24,12},{28,8},{1,21},{... | collective-permute-start | bytes 245768 | tf_op jit(solution)/shard_map/ppermute | solution.py:380
  71.0 0.0 collective-permute-done.6.refs_7_
  71.0 4.2 %collective-permute-start.15 = (bf16[160,256]{1,0:T(8,128)(2,1)S(1)}, bf16[160,256]{1,0:T(8,128)(2,1)S(1)}, u32[]{:S(2)}, u32[]{:S(2)}) collective-permute-start(bf16[160,256]{1,0:T(8,128)(2,1)S(1)} %get-tuple-element.56), channel_id=1, source_target_pairs={{0,24},{4,28},{8,16},{12,20},{16,8},{20,12},{24,0},{28,4},{1,25},{... | collective-permute-start | bytes 245768 | tf_op jit(solution)/shard_map/ppermute | solution.py:380
  75.2 3.2 %collective-permute-done.13.refs_4_ = bf16[160,256]{1,0:T(8,128)(2,1)S(1)} collective-permute-done((bf16[160,256]{1,0:T(8,128)(2,1)S(1)}, bf16[160,256]{1,0:T(8,128)(2,1)S(1)}, u32[]{:S(2)}, u32[]{:S(2)}) %collective-permute-start.13) | collective-permute-done | bytes 81952 | tf_op jit(solution)/shard_map/ppermute | solution.py:380
  78.4 2.9 %collective-permute-start.16 = (bf16[160,256]{1,0:T(8,128)(2,1)S(1)}, bf16[160,256]{1,0:T(8,128)(2,1)S(1)}, u32[]{:S(2)}, u32[]{:S(2)}) collective-permute-start(bf16[160,256]{1,0:T(8,128)(2,1)S(1)} %get-tuple-element.57), channel_id=1, source_target_pairs={{0,28},{4,24},{8,20},{12,16},{16,12},{20,8},{24,4},{28,0},{1,29},{... | collective-permute-start | bytes 245768 | tf_op jit(solution)/shard_map/ppermute | solution.py:380
  81.3 0.0 collective-permute-done.14.refs_5_
  81.3 0.7 collective-permute-start
  82.0 0.0 collective-permute-done.15.refs_6_
  82.0 1.4 %collective-permute-start.1 = (bf16[160,512]{1,0:T(8,128)(2,1)S(1)}, bf16[160,512]{1,0:T(8,128)(2,1)S(1)}, u32[]{:S(2)}, u32[]{:S(2)}) collective-permute-start(bf16[160,512]{1,0:T(8,128)(2,1)S(1)} %get-tuple-element.39), channel_id=1, source_target_pairs={{0,8},{4,12},{8,0},{12,4},{16,24},{20,28},{24,16},{28,20},{1,9},{5... | collective-permute-start | bytes 491528 | tf_op jit(solution)/shard_map/ppermute | solution.py:380
  83.4 2.3 %collective-permute-done.16.refs_7_ = bf16[160,256]{1,0:T(8,128)(2,1)S(1)} collective-permute-done((bf16[160,256]{1,0:T(8,128)(2,1)S(1)}, bf16[160,256]{1,0:T(8,128)(2,1)S(1)}, u32[]{:S(2)}, u32[]{:S(2)}) %collective-permute-start.16) | collective-permute-done | bytes 81952 | tf_op jit(solution)/shard_map/ppermute | solution.py:380
  85.6 1.3 %collective-permute-start.2 = (bf16[160,512]{1,0:T(8,128)(2,1)S(1)}, bf16[160,512]{1,0:T(8,128)(2,1)S(1)}, u32[]{:S(2)}, u32[]{:S(2)}) collective-permute-start(bf16[160,512]{1,0:T(8,128)(2,1)S(1)} %get-tuple-element.40), channel_id=1, source_target_pairs={{0,12},{4,8},{8,4},{12,0},{16,28},{20,24},{24,20},{28,16},{1,13},{... | collective-permute-start | bytes 491528 | tf_op jit(solution)/shard_map/ppermute | solution.py:380
  86.9 2.6 %collective-permute-done.refs_1_.refs_0_ = bf16[160,512]{1,0:T(8,128)(2,1)S(1)} collective-permute-done((bf16[160,512]{1,0:T(8,128)(2,1)S(1)}, bf16[160,512]{1,0:T(8,128)(2,1)S(1)}, u32[]{:S(2)}, u32[]{:S(2)}) %collective-permute-start) | collective-permute-done | bytes 163872 | tf_op jit(solution)/shard_map/ppermute | solution.py:380
  89.5 3.1 %collective-permute-done.2.refs_3_.refs_2_ = bf16[160,512]{1,0:T(8,128)(2,1)S(1)} collective-permute-done((bf16[160,512]{1,0:T(8,128)(2,1)S(1)}, bf16[160,512]{1,0:T(8,128)(2,1)S(1)}, u32[]{:S(2)}, u32[]{:S(2)}) %collective-permute-start.2) | collective-permute-done | bytes 163872 | tf_op jit(solution)/shard_map/ppermute | solution.py:380
  92.7 2.1 %collective-permute-start.12 = (bf16[160,512]{1,0:T(8,128)(2,1)S(1)}, bf16[160,512]{1,0:T(8,128)(2,1)S(1)}, u32[]{:S(2)}, u32[]{:S(2)}) collective-permute-start(bf16[160,512]{1,0:T(8,128)(2,1)S(1)} %get-tuple-element.53), channel_id=1, source_target_pairs={{0,12},{4,8},{8,4},{12,0},{16,28},{20,24},{24,20},{28,16},{1,13},{... | collective-permute-start | bytes 491528 | tf_op jit(solution)/shard_map/ppermute | solution.py:380
  94.7 0.4 spread.2
  95.1 3.7 %attend.5 = (bf16[160,256]{1,0:T(8,128)(2,1)S(1)}, bf16[160,256]{1,0:T(8,128)(2,1)S(1)}, bf16[160,256]{1,0:T(8,128)(2,1)S(1)}) custom-call(bf16[160,512]{1,0:T(8,128)(2,1)S(1)} %collective-permute-done.refs_1_.refs_0_, bf16[160,512]{1,0:T(8,128)(2,1)S(1)} %collective-permute-done.1.refs_2_.refs_1_, ...), custom_call_target="tpu_custom_call" | custom-call | flops 1258291200 | bytes 2621440 | tf_op jit(solution)/shard_map/attend/pallas_call | solution.py:297
  98.8 0.1 collective-permute-start.7
  98.9 0.0 collective-permute-done.11.refs_2_.refs_1_
  98.9 1.4 %collective-permute-start.8 = (bf16[160,256]{1,0:T(8,128)(2,1)S(1)}, bf16[160,256]{1,0:T(8,128)(2,1)S(1)}, u32[]{:S(2)}, u32[]{:S(2)}) collective-permute-start(bf16[160,256]{1,0:T(8,128)(2,1)S(1)} %get-tuple-element.48), channel_id=1, source_target_pairs={{0,8},{4,12},{8,0},{12,4},{16,24},{20,28},{24,16},{28,20},{1,9},{5... | collective-permute-start | bytes 245768 | tf_op jit(solution)/shard_map/ppermute | solution.py:380
  100.3 0.0 collective-permute-done.12.refs_3_.refs_2_
  100.3 2.1 %collective-permute-start.9 = (bf16[160,256]{1,0:T(8,128)(2,1)S(1)}, bf16[160,256]{1,0:T(8,128)(2,1)S(1)}, u32[]{:S(2)}, u32[]{:S(2)}) collective-permute-start(bf16[160,256]{1,0:T(8,128)(2,1)S(1)} %get-tuple-element.49), channel_id=1, source_target_pairs={{0,12},{4,8},{8,4},{12,0},{16,28},{20,24},{24,20},{28,16},{1,13},{... | collective-permute-start | bytes 245768 | tf_op jit(solution)/shard_map/ppermute | solution.py:380
  102.3 0.4 spread.3
  102.7 1.5 %attend.4.refs_0_ = bf16[160,256]{1,0:T(8,128)(2,1)S(1)} custom-call(bf16[160,512]{1,0:T(8,128)(2,1)S(1)} %get-tuple-element.37.refs_0_, bf16[2,2560,128]{2,1,0:T(8,128)(2,1)S(1)} %get-tuple-element.45.refs_1_.refs_3_, bf16[2,2560,128]{2,1,0:T(8,128)(2,1)S(1)} %get-tuple-element.46.refs_2_.refs_4_), custom_call_target="tpu_custom_call" | custom-call | flops 419430400 | bytes 2621440 | tf_op jit(solution)/shard_map/attend/pallas_call | solution.py:297
  104.2 3.9 %attend.7 = (bf16[160,256]{1,0:T(8,128)(2,1)S(1)}, bf16[160,256]{1,0:T(8,128)(2,1)S(1)}, bf16[160,256]{1,0:T(8,128)(2,1)S(1)}) custom-call(bf16[160,512]{1,0:T(8,128)(2,1)S(1)} %collective-permute-done.10.refs_1_.refs_0_, bf16[160,512]{1,0:T(8,128)(2,1)S(1)} %collective-permute-done.11.refs_2_.refs_1_, ...), custom_call_target="tpu_custom_call" | custom-call | flops 1258291200 | bytes 2621440 | tf_op jit(solution)/shard_map/attend/pallas_call | solution.py:297
  108.1 0.0 copy-start
  108.2 0.2 collective-permute-start.17
  108.3 0.0 collective-permute-done.8.refs_2_
  108.3 1.3 %collective-permute-start.18 = (bf16[160,256]{1,0:T(8,128)(2,1)S(1)}, bf16[160,256]{1,0:T(8,128)(2,1)S(1)}, u32[]{:S(2)}, u32[]{:S(2)}) collective-permute-start(bf16[160,256]{1,0:T(8,128)(2,1)S(1)} %get-tuple-element.61), channel_id=1, source_target_pairs={{0,8},{4,12},{8,0},{12,4},{16,24},{20,28},{24,16},{28,20},{1,9},{5... | collective-permute-start | bytes 245768 | tf_op jit(solution)/shard_map/ppermute | solution.py:380
  109.7 2.1 %collective-permute-start.19 = (bf16[160,256]{1,0:T(8,128)(2,1)S(1)}, bf16[160,256]{1,0:T(8,128)(2,1)S(1)}, u32[]{:S(2)}, u32[]{:S(2)}) collective-permute-start(bf16[160,256]{1,0:T(8,128)(2,1)S(1)} %get-tuple-element.62), channel_id=1, source_target_pairs={{0,12},{4,8},{8,4},{12,0},{16,28},{20,24},{24,20},{28,16},{1,13},{... | collective-permute-start | bytes 245768 | tf_op jit(solution)/shard_map/ppermute | solution.py:380
  111.7 1.5 %attend.6.refs_4_ = bf16[160,256]{1,0:T(8,128)(2,1)S(1)} custom-call(bf16[160,512]{1,0:T(8,128)(2,1)S(1)} %get-tuple-element.50.refs_0_, bf16[2,2560,128]{2,1,0:T(8,128)(2,1)S(1)} %get-tuple-element.58.refs_1_.refs_3_, bf16[2,2560,128]{2,1,0:T(8,128)(2,1)S(1)} %get-tuple-element.59.refs_2_.refs_4_), custom_call_target="tpu_custom_call" | custom-call | flops 419430400 | bytes 2621440 | tf_op jit(solution)/shard_map/attend/pallas_call | solution.py:297
  113.2 0.8 project.3
  114.0 0.0 collective-permute-done.17.refs_0_.refs_5_
  114.1 0.9 collective-permute-done.19.refs_2_.refs_7_
  115.0 0.6 project.4
  115.6 1.2 %project.5 = bf16[160,2048]{1,0:T(8,128)(2,1)} custom-call(bf16[160,256]{1,0:T(8,128)(2,1)S(1)} %attend.4.refs_0_, bf16[160,256]{1,0:T(8,128)(2,1)S(1)} %collective-permute-done.7.refs_1_, bf16[160,256]{1,0:T(8,128)(2,1)S(1)} %collective-permute-done.8.refs_2_, bf16[160,256]{1,0:T(8,128)(2,1)S(1)} %collective-permute-done.9.refs_3_, ...), custom_call_target="tpu_custom_call" | custom-call | flops 335544320 | bytes 4194304 | tf_op jit(solution)/shard_map/project/pallas_call | solution.py:366
  (11 shorter events, 0.0 us)
Async XLA Ops:
  0.0 48.8 %collective-permute-start.20 = (bf16[2048,512]{1,0:T(8,128)(2,1)}, bf16[2048,512]{1,0:T(8,128)(2,1)S(1)}, u32[]{:S(2)}, u32[]{:S(2)}) collective-permute-start(bf16[2048,512]{1,0:T(8,128)(2,1)} %refs_3_.1), channel_id=1, source_target_pairs={{0,2},{1,3},{2,0},{3,1},{4,6},{5,7},{6,4},{7,5},{8,10},{9,11},{10,... | collective-permute-start | bytes 6291464 | tf_op jit(solution)/shard_map/ppermute | solution.py:380
  3.0 110.2 %collective-permute-start.22 = (bf16[2048,512]{1,0:T(8,128)(2,1)}, bf16[2048,512]{1,0:T(8,128)(2,1)S(1)}, u32[]{:S(2)}, u32[]{:S(2)}) collective-permute-start(bf16[2048,512]{1,0:T(8,128)(2,1)} %refs_3_.1), channel_id=1, source_target_pairs={{0,1},{1,0},{2,3},{3,2},{4,5},{5,4},{6,7},{7,6},{8,9},{9,8},{10,11... | collective-permute-start | bytes 6291464 | tf_op jit(solution)/shard_map/ppermute | solution.py:380
  48.8 66.8 %collective-permute-start.21 = (bf16[2048,512]{1,0:T(8,128)(2,1)S(1)}, bf16[2048,512]{1,0:T(8,128)(2,1)S(1)}, u32[]{:S(2)}, u32[]{:S(2)}) collective-permute-start(bf16[2048,512]{1,0:T(8,128)(2,1)S(1)} %collective-permute-done.20.refs_7_.refs_5_), channel_id=1, source_target_pairs={{0,1},{1,0},{2,3},{3,2},{4,5},{5,4},{6,7},{7,6},{8,9},{9,8},{10,11... | collective-permute-start | bytes 6291464 | tf_op jit(solution)/shard_map/ppermute | solution.py:380
  52.3 8.0 %collective-permute-start.3 = (bf16[160,256]{1,0:T(8,128)(2,1)S(1)}, bf16[160,256]{1,0:T(8,128)(2,1)S(1)}, u32[]{:S(2)}, u32[]{:S(2)}) collective-permute-start(bf16[160,256]{1,0:T(8,128)(2,1)S(1)} %get-tuple-element.41), channel_id=1, source_target_pairs={{0,16},{4,20},{8,24},{12,28},{16,0},{20,4},{24,8},{28,12},{1,17},{... | collective-permute-start | bytes 245768 | tf_op jit(solution)/shard_map/ppermute | solution.py:380
  55.2 12.9 %collective-permute-start.4 = (bf16[160,256]{1,0:T(8,128)(2,1)S(1)}, bf16[160,256]{1,0:T(8,128)(2,1)S(1)}, u32[]{:S(2)}, u32[]{:S(2)}) collective-permute-start(bf16[160,256]{1,0:T(8,128)(2,1)S(1)} %get-tuple-element.42), channel_id=1, source_target_pairs={{0,20},{4,16},{8,28},{12,24},{16,4},{20,0},{24,12},{28,8},{1,21},{... | collective-permute-start | bytes 245768 | tf_op jit(solution)/shard_map/ppermute | solution.py:380
  56.5 11.6 %collective-permute-start.5 = (bf16[160,256]{1,0:T(8,128)(2,1)S(1)}, bf16[160,256]{1,0:T(8,128)(2,1)S(1)}, u32[]{:S(2)}, u32[]{:S(2)}) collective-permute-start(bf16[160,256]{1,0:T(8,128)(2,1)S(1)} %get-tuple-element.43), channel_id=1, source_target_pairs={{0,24},{4,28},{8,16},{12,20},{16,8},{20,12},{24,0},{28,4},{1,25},{... | collective-permute-start | bytes 245768 | tf_op jit(solution)/shard_map/ppermute | solution.py:380
  60.3 10.7 %collective-permute-start.6 = (bf16[160,256]{1,0:T(8,128)(2,1)S(1)}, bf16[160,256]{1,0:T(8,128)(2,1)S(1)}, u32[]{:S(2)}, u32[]{:S(2)}) collective-permute-start(bf16[160,256]{1,0:T(8,128)(2,1)S(1)} %get-tuple-element.44), channel_id=1, source_target_pairs={{0,28},{4,24},{8,20},{12,16},{16,12},{20,8},{24,4},{28,0},{1,29},{... | collective-permute-start | bytes 245768 | tf_op jit(solution)/shard_map/ppermute | solution.py:380
  68.1 10.3 %collective-permute-start.13 = (bf16[160,256]{1,0:T(8,128)(2,1)S(1)}, bf16[160,256]{1,0:T(8,128)(2,1)S(1)}, u32[]{:S(2)}, u32[]{:S(2)}) collective-permute-start(bf16[160,256]{1,0:T(8,128)(2,1)S(1)} %get-tuple-element.54), channel_id=1, source_target_pairs={{0,16},{4,20},{8,24},{12,28},{16,0},{20,4},{24,8},{28,12},{1,17},{... | collective-permute-start | bytes 245768 | tf_op jit(solution)/shard_map/ppermute | solution.py:380
  68.1 13.2 %collective-permute-start.14 = (bf16[160,256]{1,0:T(8,128)(2,1)S(1)}, bf16[160,256]{1,0:T(8,128)(2,1)S(1)}, u32[]{:S(2)}, u32[]{:S(2)}) collective-permute-start(bf16[160,256]{1,0:T(8,128)(2,1)S(1)} %get-tuple-element.55), channel_id=1, source_target_pairs={{0,20},{4,16},{8,28},{12,24},{16,4},{20,0},{24,12},{28,8},{1,21},{... | collective-permute-start | bytes 245768 | tf_op jit(solution)/shard_map/ppermute | solution.py:380
  71.0 11.0 %collective-permute-start.15 = (bf16[160,256]{1,0:T(8,128)(2,1)S(1)}, bf16[160,256]{1,0:T(8,128)(2,1)S(1)}, u32[]{:S(2)}, u32[]{:S(2)}) collective-permute-start(bf16[160,256]{1,0:T(8,128)(2,1)S(1)} %get-tuple-element.56), channel_id=1, source_target_pairs={{0,24},{4,28},{8,16},{12,20},{16,8},{20,12},{24,0},{28,4},{1,25},{... | collective-permute-start | bytes 245768 | tf_op jit(solution)/shard_map/ppermute | solution.py:380
  78.4 7.2 %collective-permute-start.16 = (bf16[160,256]{1,0:T(8,128)(2,1)S(1)}, bf16[160,256]{1,0:T(8,128)(2,1)S(1)}, u32[]{:S(2)}, u32[]{:S(2)}) collective-permute-start(bf16[160,256]{1,0:T(8,128)(2,1)S(1)} %get-tuple-element.57), channel_id=1, source_target_pairs={{0,28},{4,24},{8,20},{12,16},{16,12},{20,8},{24,4},{28,0},{1,29},{... | collective-permute-start | bytes 245768 | tf_op jit(solution)/shard_map/ppermute | solution.py:380
  81.3 8.2 %collective-permute-start = (bf16[160,512]{1,0:T(8,128)(2,1)S(1)}, bf16[160,512]{1,0:T(8,128)(2,1)S(1)}, u32[]{:S(2)}, u32[]{:S(2)}) collective-permute-start(bf16[160,512]{1,0:T(8,128)(2,1)S(1)} %get-tuple-element.38), channel_id=1, source_target_pairs={{0,4},{4,0},{8,12},{12,8},{16,20},{20,16},{24,28},{28,24},{1,5},{5... | collective-permute-start | bytes 491528 | tf_op jit(solution)/shard_map/ppermute | solution.py:380
  82.0 7.5 %collective-permute-start.1 = (bf16[160,512]{1,0:T(8,128)(2,1)S(1)}, bf16[160,512]{1,0:T(8,128)(2,1)S(1)}, u32[]{:S(2)}, u32[]{:S(2)}) collective-permute-start(bf16[160,512]{1,0:T(8,128)(2,1)S(1)} %get-tuple-element.39), channel_id=1, source_target_pairs={{0,8},{4,12},{8,0},{12,4},{16,24},{20,28},{24,16},{28,20},{1,9},{5... | collective-permute-start | bytes 491528 | tf_op jit(solution)/shard_map/ppermute | solution.py:380
  85.6 7.0 %collective-permute-start.2 = (bf16[160,512]{1,0:T(8,128)(2,1)S(1)}, bf16[160,512]{1,0:T(8,128)(2,1)S(1)}, u32[]{:S(2)}, u32[]{:S(2)}) collective-permute-start(bf16[160,512]{1,0:T(8,128)(2,1)S(1)} %get-tuple-element.40), channel_id=1, source_target_pairs={{0,12},{4,8},{8,4},{12,0},{16,28},{20,24},{24,20},{28,16},{1,13},{... | collective-permute-start | bytes 491528 | tf_op jit(solution)/shard_map/ppermute | solution.py:380
  89.5 9.3 %collective-permute-start.10 = (bf16[160,512]{1,0:T(8,128)(2,1)S(1)}, bf16[160,512]{1,0:T(8,128)(2,1)S(1)}, u32[]{:S(2)}, u32[]{:S(2)}) collective-permute-start(bf16[160,512]{1,0:T(8,128)(2,1)S(1)} %get-tuple-element.51), channel_id=1, source_target_pairs={{0,4},{4,0},{8,12},{12,8},{16,20},{20,16},{24,28},{28,24},{1,5},{5... | collective-permute-start | bytes 491528 | tf_op jit(solution)/shard_map/ppermute | solution.py:380
  89.5 9.3 %collective-permute-start.11 = (bf16[160,512]{1,0:T(8,128)(2,1)S(1)}, bf16[160,512]{1,0:T(8,128)(2,1)S(1)}, u32[]{:S(2)}, u32[]{:S(2)}) collective-permute-start(bf16[160,512]{1,0:T(8,128)(2,1)S(1)} %get-tuple-element.52), channel_id=1, source_target_pairs={{0,8},{4,12},{8,0},{12,4},{16,24},{20,28},{24,16},{28,20},{1,9},{5... | collective-permute-start | bytes 491528 | tf_op jit(solution)/shard_map/ppermute | solution.py:380
  92.7 7.6 %collective-permute-start.12 = (bf16[160,512]{1,0:T(8,128)(2,1)S(1)}, bf16[160,512]{1,0:T(8,128)(2,1)S(1)}, u32[]{:S(2)}, u32[]{:S(2)}) collective-permute-start(bf16[160,512]{1,0:T(8,128)(2,1)S(1)} %get-tuple-element.53), channel_id=1, source_target_pairs={{0,12},{4,8},{8,4},{12,0},{16,28},{20,24},{24,20},{28,16},{1,13},{... | collective-permute-start | bytes 491528 | tf_op jit(solution)/shard_map/ppermute | solution.py:380
  98.8 9.4 %collective-permute-start.7 = (bf16[160,256]{1,0:T(8,128)(2,1)S(1)}, bf16[160,256]{1,0:T(8,128)(2,1)S(1)}, u32[]{:S(2)}, u32[]{:S(2)}) collective-permute-start(bf16[160,256]{1,0:T(8,128)(2,1)S(1)} %get-tuple-element.47), channel_id=1, source_target_pairs={{0,4},{4,0},{8,12},{12,8},{16,20},{20,16},{24,28},{28,24},{1,5},{5... | collective-permute-start | bytes 245768 | tf_op jit(solution)/shard_map/ppermute | solution.py:380
  98.9 9.4 %collective-permute-start.8 = (bf16[160,256]{1,0:T(8,128)(2,1)S(1)}, bf16[160,256]{1,0:T(8,128)(2,1)S(1)}, u32[]{:S(2)}, u32[]{:S(2)}) collective-permute-start(bf16[160,256]{1,0:T(8,128)(2,1)S(1)} %get-tuple-element.48), channel_id=1, source_target_pairs={{0,8},{4,12},{8,0},{12,4},{16,24},{20,28},{24,16},{28,20},{1,9},{5... | collective-permute-start | bytes 245768 | tf_op jit(solution)/shard_map/ppermute | solution.py:380
  100.3 9.4 %collective-permute-start.9 = (bf16[160,256]{1,0:T(8,128)(2,1)S(1)}, bf16[160,256]{1,0:T(8,128)(2,1)S(1)}, u32[]{:S(2)}, u32[]{:S(2)}) collective-permute-start(bf16[160,256]{1,0:T(8,128)(2,1)S(1)} %get-tuple-element.49), channel_id=1, source_target_pairs={{0,12},{4,8},{8,4},{12,0},{16,28},{20,24},{24,20},{28,16},{1,13},{... | collective-permute-start | bytes 245768 | tf_op jit(solution)/shard_map/ppermute | solution.py:380
  108.1 5.1 %copy-start = (bf16[2048,512]{1,0:T(8,128)(2,1)S(1)}, bf16[2048,512]{1,0:T(8,128)(2,1)}, u32[]{:S(2)}) copy-start(bf16[2048,512]{1,0:T(8,128)(2,1)} %refs_3_.1) | copy-start | bytes 6291460
  108.2 5.9 %collective-permute-start.17 = (bf16[160,256]{1,0:T(8,128)(2,1)S(1)}, bf16[160,256]{1,0:T(8,128)(2,1)S(1)}, u32[]{:S(2)}, u32[]{:S(2)}) collective-permute-start(bf16[160,256]{1,0:T(8,128)(2,1)S(1)} %get-tuple-element.60), channel_id=1, source_target_pairs={{0,4},{4,0},{8,12},{12,8},{16,20},{20,16},{24,28},{28,24},{1,5},{5... | collective-permute-start | bytes 245768 | tf_op jit(solution)/shard_map/ppermute | solution.py:380
  108.3 5.7 %collective-permute-start.18 = (bf16[160,256]{1,0:T(8,128)(2,1)S(1)}, bf16[160,256]{1,0:T(8,128)(2,1)S(1)}, u32[]{:S(2)}, u32[]{:S(2)}) collective-permute-start(bf16[160,256]{1,0:T(8,128)(2,1)S(1)} %get-tuple-element.61), channel_id=1, source_target_pairs={{0,8},{4,12},{8,0},{12,4},{16,24},{20,28},{24,16},{28,20},{1,9},{5... | collective-permute-start | bytes 245768 | tf_op jit(solution)/shard_map/ppermute | solution.py:380
  109.7 5.3 %collective-permute-start.19 = (bf16[160,256]{1,0:T(8,128)(2,1)S(1)}, bf16[160,256]{1,0:T(8,128)(2,1)S(1)}, u32[]{:S(2)}, u32[]{:S(2)}) collective-permute-start(bf16[160,256]{1,0:T(8,128)(2,1)S(1)} %get-tuple-element.62), channel_id=1, source_target_pairs={{0,12},{4,8},{8,4},{12,0},{16,28},{20,24},{24,20},{28,16},{1,13},{... | collective-permute-start | bytes 245768 | tf_op jit(solution)/shard_map/ppermute | solution.py:380

commit v5 on v4

--- a/solution.py
+++ b/solution.py
@@ -227,88 +227,125 @@
     return both, kv
 
 
-def spread_kernel(groups, *refs):
-    near_refs, far_refs, (keys_ref, vals_ref) = refs[:groups], refs[groups : 2 * groups], refs[2 * groups :]
-    rows = near_refs[0].shape[0]
-    seq = 2 * groups * rows
+def spread_tiles(tiles, out_ref):
+    rows = tiles[0].shape[0]
+    half = len(tiles) * rows
     low = lax.broadcasted_iota(jnp.int32, (rows, TILE), 1) < HD
-    tiles = [(ref[:, 2 * TILE : 3 * TILE], ref[:, 3 * TILE :]) for ref in near_refs]
-    tiles += [(ref[:, :TILE], ref[:, TILE:]) for ref in far_refs]
-    for i, pair in enumerate(tiles):
-        for tile, out_ref in zip(pair, (keys_ref, vals_ref)):
-            tile = tile.astype(jnp.float32)
-            other = pltpu.roll(tile, HD, 1)
-            here = slice(i * rows, (i + 1) * rows)
-            there = slice(seq + i * rows, seq + (i + 1) * rows)
-            out_ref[0, here, :] = jnp.where(low, tile, 0.0).astype(jnp.bfloat16)
-            out_ref[0, there, :] = jnp.where(low, 0.0, other).astype(jnp.bfloat16)
-            out_ref[1, here, :] = jnp.where(low, other, 0.0).astype(jnp.bfloat16)
-            out_ref[1, there, :] = jnp.where(low, 0.0, tile).astype(jnp.bfloat16)
-
-
-def spread(near, far):
-    groups, rows = len(near), near[0].shape[0]
-    made = jax.ShapeDtypeStruct((2, GROUP * 2 * groups * rows, TILE), jnp.bfloat16)
+    for i, tile in enumerate(tiles):
+        tile = tile.astype(jnp.float32)
+        other = pltpu.roll(tile, HD, 1)
+        here = slice(i * rows, (i + 1) * rows)
+        there = slice(half + i * rows, half + (i + 1) * rows)
+        out_ref[0, here, :] = jnp.where(low, tile, 0.0).astype(jnp.bfloat16)
+        out_ref[0, there, :] = jnp.where(low, 0.0, other).astype(jnp.bfloat16)
+        out_ref[1, here, :] = jnp.where(low, other, 0.0).astype(jnp.bfloat16)
+        out_ref[1, there, :] = jnp.where(low, 0.0, tile).astype(jnp.bfloat16)
+
+
+def near_kernel(*refs):
+    spread_tiles([ref[:, 2 * TILE : 3 * TILE] for ref in refs[:-1]], refs[-1])
+
+
+def far_kernel(*refs):
+    groups = len(refs[:-2]) // 2
+    near_refs, far_refs, (keys_ref, vals_ref) = refs[:groups], refs[groups : 2 * groups], refs[-2:]
+    spread_tiles([ref[:, :TILE] for ref in far_refs], keys_ref)
+    spread_tiles([ref[:, 3 * TILE :] for ref in near_refs] + [ref[:, TILE:] for ref in far_refs], vals_ref)
+
+
+def spread(kernel, sources, made):
+    rows = GROUP * sources[0].shape[0]
     return pl.pallas_call(
-        functools.partial(spread_kernel, groups),
-        in_specs=in_vmem(2 * groups),
-        out_specs=in_vmem(2),
-        out_shape=[made] * 2,
+        kernel,
+        in_specs=in_vmem(len(sources)),
+        out_specs=in_vmem(len(made)),
+        out_shape=[jax.ShapeDtypeStruct((2, count * rows, TILE), jnp.bfloat16) for count in made],
         compiler_params=params(16),
-        cost_estimate=pl.CostEstimate(flops=1 << 22, bytes_accessed=1 << 22, transcendentals=0),
+        cost_estimate=pl.CostEstimate(flops=1 << 21, bytes_accessed=1 << 21, transcendentals=0),
         name="spread",
-    )(*near, *far)
+    )(*sources)
+
+
+def score(query_refs, keys_ref, p):
+    query = jnp.concatenate([ref[:, p * TILE : (p + 1) * TILE] for ref in query_refs], axis=0)
+    return lax.dot_general(query, keys_ref[p], (((1,), (1,)), ((), ())), preferred_element_type=jnp.float32)
+
+
+def score_kernel(*refs):
+    for p in range(2):
+        refs[-1][p] = score(refs[:-2], refs[-2], p)
+
+
+def early_scores(near, keys):
+    rows = len(near) * near[0].shape[0]
+    return pl.pallas_call(
+        score_kernel,
+        in_specs=in_vmem(len(near) + 1),
+        out_specs=pl.BlockSpec(memory_space=pltpu.VMEM),
+        out_shape=jax.ShapeDtypeStruct((2, rows, keys.shape[1]), jnp.float32),
+        compiler_params=params(16),
+        cost_estimate=pl.CostEstimate(
+            flops=4 * rows * keys.shape[1] * TILE, bytes_accessed=1 << 22, transcendentals=0
+        ),
+        name="score",
+    )(*near, keys)
 
 
 SOFT_ROWS = 8
 
 
-def attend_kernel(count, *refs):
-    query_refs, (keys_ref, vals_ref), out_refs = refs[:count], refs[count : count + 2], refs[count + 2 : -2]
-    s_scr, w_scr = refs[-2:]
+def attend_kernel(count, given, *refs):
+    query_refs, (near_keys, far_keys, vals), refs = refs[:count], refs[count : count + 3], refs[count + 3 :]
+    out_refs, (near_s, far_s, w_scr) = refs[given : given + count], refs[given + count :]
+    if given:
+        near_s = refs[0]
     rows = query_refs[0].shape[0]
-    seq = keys_ref.shape[1] // GROUP
+    half = near_keys.shape[1] // GROUP
+    wide = near_keys.shape[1]
     factor = HD ** (-0.5) * 1.4426950408889634
 
     def scores(p):
-        query = jnp.concatenate([ref[:, p * TILE : (p + 1) * TILE] for ref in query_refs], axis=0)
-        s_scr[p] = lax.dot_general(
-            query, keys_ref[p], (((1,), (1,)), ((), ())), preferred_element_type=jnp.float32
-        )
+        if not given:
+            near_s[p] = score(query_refs, near_keys, p)
+        far_s[p] = score(query_refs, far_keys, p)
 
     scores(0)
     for p in range(2):
         if p == 0:
             scores(1)
         for g in range(GROUP):
+            lanes = slice(g * half, (g + 1) * half)
             for r in range(0, count * rows, SOFT_ROWS):
-                s = s_scr[p, r : r + SOFT_ROWS, g * seq : (g + 1) * seq]
+                s = jnp.concatenate([part[p, r : r + SOFT_ROWS, lanes] for part in (near_s, far_s)], axis=1)
                 e = jnp.exp2((s - jnp.max(s, axis=-1, keepdims=True)) * factor)
                 w = e * (1.0 / jnp.sum(e, axis=-1, keepdims=True))
-                w_scr[p, r : r + SOFT_ROWS, g * seq : (g + 1) * seq] = w.astype(jnp.bfloat16)
-        attended = jnp.dot(w_scr[p], vals_ref[p], preferred_element_type=jnp.float32).astype(jnp.bfloat16)
+                w_scr[p, r : r + SOFT_ROWS, g * wide : (g + 1) * wide] = w.astype(jnp.bfloat16)
+        attended = jnp.dot(w_scr[p], vals[p], preferred_element_type=jnp.float32).astype(jnp.bfloat16)
         for i, out_ref in enumerate(out_refs):
             out_ref[:, p * TILE : (p + 1) * TILE] = attended[i * rows : (i + 1) * rows]
 
 
-def attend(near, keys, vals):
+def attend(near, ready, early=None):
     count, rows = len(near), near[0].shape[0]
-    wide = keys.shape[1]
+    wide = ready[0].shape[1]
+    given = [] if early is None else [early]
+    held = count * rows if early is None else SOFT_ROWS
     return pl.pallas_call(
-        functools.partial(attend_kernel, count),
-        in_specs=in_vmem(count + 2),
+        functools.partial(attend_kernel, count, len(given)),
+        in_specs=in_vmem(count + 3 + len(given)),
         out_specs=in_vmem(count),
         out_shape=[jax.ShapeDtypeStruct((rows, 2 * TILE), jnp.bfloat16)] * count,
         scratch_shapes=[
+            pltpu.VMEM((2, held, wide), jnp.float32),
             pltpu.VMEM((2, count * rows, wide), jnp.float32),
-            pltpu.VMEM((2, count * rows, wide), jnp.bfloat16),
+            pltpu.VMEM((2, count * rows, 2 * wide), jnp.bfloat16),
         ],
         compiler_params=params(32),
         cost_estimate=pl.CostEstimate(
-            flops=8 * count * rows * wide * TILE, bytes_accessed=8 * wide * TILE, transcendentals=0
+            flops=16 * count * rows * wide * TILE, bytes_accessed=8 * wide * TILE, transcendentals=0
         ),
         name="attend",
-    )(*near, keys, vals)
+    )(*near, *ready, *given)
 
 
 def home_of(groups):
@@ -396,9 +433,13 @@
         far.append([exchanged(kv[c][j], "sp", groups + j) for j in range(groups)])
     back = []
     for c in range(chunks):
-        ready = spread(near[c], far[c])
-        away = attend(near[c][1:], *ready)
-        local = attend(near[c][:1], *ready)
+        early = None
+        (near_keys,) = spread(near_kernel, near[c], [groups])
+        if c:
+            early = early_scores(near[c][1:], near_keys)
+        ready = [near_keys, *spread(far_kernel, near[c] + far[c], [groups, 2 * groups])]
+        away = attend(near[c][1:], ready, early)
+        local = attend(near[c][:1], ready)
         back.append(list(local) + [exchanged(away[j - 1], "sp", j) for j in range(1, groups)])
 
     near_blocks = [w_out, beside, across]

time: 117 us -> 118 us (level)
  waiting for transfers between devices: 58.2 us -> 61.6 us
  starting transfers between devices: 41.1 us -> 38.2 us
    ppermute x23, waiting for transfers between devices: 58.2 us -> 61.6 us  [exchanged(): return lax.ppermute(block, axis, [(i, i ^ flip) for i in range(count)])]
    ppermute x23, starting transfers between devices: 41.1 us -> 38.2 us  [exchanged(): return lax.ppermute(block, axis, [(i, i ^ flip) for i in range(count)])]
    pallas_call x6 -> x9, Pallas kernels: 11.3 us -> 12 us  [the longest x4 10.4 us: attend(): pl.pallas_call(functools.partial(attend_kernel, count, len(given)), in_sp...]
  transfers between devices with their start and end apart: 23 -> 23, of which waited for: 7 -> 10; matrix products, arithmetic and copies ran while one was open for 1% -> 1% of each run, Pallas kernels for 13% -> 14%
where the time goes in v5:
time: 118 us
  waiting for transfers between devices  61.6 us (52%)
  starting transfers between devices  38.2 us (32%)
  Pallas kernels  17.2 us (15%)
    ppermute x23, waiting for transfers between devices, exchanged(): return lax.ppermute(block, axis, [(i, i ^ flip) for i in range(count)])  61.6 us
    ppermute x23, starting transfers between devices, exchanged(): return lax.ppermute(block, axis, [(i, i ^ flip) for i in range(count)])  38.2 us
    pallas_call x4, Pallas kernels, attend(): pl.pallas_call(functools.partial(attend_kernel, count, len(given)), in_sp...  10.4 us
    pallas_call x1, Pallas kernels, turn_and_pack(): pl.pallas_call(functools.partial(turn_kernel, groups, chunks), in_specs=[...  2.68 us
    pallas_call x3, Pallas kernels, project_call(): pl.pallas_call(functools.partial(kernel, groups), in_specs=in_vmem(len(in...  2.61 us
  transfers between devices with their start and end apart: 23, of which 10 were waited for; matrix products, arithmetic and copies ran while one was open for 1% of the time, Pallas kernels for 14%

profile of v5, /device:TPU:0, one launch (start us, length us, event | category | flops | bytes accessed | tf_op | source)
XLA Modules:
  0.0 118.2 jit_solution(1438024669645201076)
XLA Ops:
  0.0 3.0 %collective-permute-start.20 = (bf16[2048,512]{1,0:T(8,128)(2,1)}, bf16[2048,512]{1,0:T(8,128)(2,1)S(1)}, u32[]{:S(2)}, u32[]{:S(2)}) collective-permute-start(bf16[2048,512]{1,0:T(8,128)(2,1)} %refs_3_.1), channel_id=1, source_target_pairs={{0,2},{1,3},{2,0},{3,1},{4,6},{5,7},{6,4},{7,5},{8,10},{9,11},{10,... | collective-permute-start | bytes 6291464 | tf_op jit(solution)/shard_map/ppermute | solution.py:417
  3.0 45.8 %collective-permute-done.20.refs_7_.refs_5_ = bf16[2048,512]{1,0:T(8,128)(2,1)S(1)} collective-permute-done((bf16[2048,512]{1,0:T(8,128)(2,1)}, bf16[2048,512]{1,0:T(8,128)(2,1)S(1)}, u32[]{:S(2)}, u32[]{:S(2)}) %collective-permute-start.20) | collective-permute-done | bytes 2097184 | tf_op jit(solution)/shard_map/ppermute | solution.py:417
  48.8 0.8 maximum_bitcast_fusion.refs_3_
  49.6 2.7 %turn.1 = (bf16[160,512]{1,0:T(8,128)(2,1)S(1)}, bf16[160,512]{1,0:T(8,128)(2,1)S(1)}, bf16[160,512]{1,0:T(8,128)(2,1)S(1)}, bf16[160,512]{1,0:T(8,128)(2,1)S(1)...) custom-call(bf16[160,2048]{1,0:T(8,128)(2,1)} %bitcast.12, ...), custom_call_target="tpu_custom_call" | custom-call | flops 19660800 | bytes 3932160 | tf_op jit(solution)/shard_map/turn/pallas_call | solution.py:214
  52.3 2.9 %collective-permute-start.3 = (bf16[160,256]{1,0:T(8,128)(2,1)S(1)}, bf16[160,256]{1,0:T(8,128)(2,1)S(1)}, u32[]{:S(2)}, u32[]{:S(2)}) collective-permute-start(bf16[160,256]{1,0:T(8,128)(2,1)S(1)} %get-tuple-element.41), channel_id=1, source_target_pairs={{0,16},{4,20},{8,24},{12,28},{16,0},{20,4},{24,8},{28,12},{1,17},{... | collective-permute-start | bytes 245768 | tf_op jit(solution)/shard_map/ppermute | solution.py:417
  55.2 1.3 %collective-permute-start.4 = (bf16[160,256]{1,0:T(8,128)(2,1)S(1)}, bf16[160,256]{1,0:T(8,128)(2,1)S(1)}, u32[]{:S(2)}, u32[]{:S(2)}) collective-permute-start(bf16[160,256]{1,0:T(8,128)(2,1)S(1)} %get-tuple-element.42), channel_id=1, source_target_pairs={{0,20},{4,16},{8,28},{12,24},{16,4},{20,0},{24,12},{28,8},{1,21},{... | collective-permute-start | bytes 245768 | tf_op jit(solution)/shard_map/ppermute | solution.py:417
  56.5 3.6 %collective-permute-start.5 = (bf16[160,256]{1,0:T(8,128)(2,1)S(1)}, bf16[160,256]{1,0:T(8,128)(2,1)S(1)}, u32[]{:S(2)}, u32[]{:S(2)}) collective-permute-start(bf16[160,256]{1,0:T(8,128)(2,1)S(1)} %get-tuple-element.43), channel_id=1, source_target_pairs={{0,24},{4,28},{8,16},{12,20},{16,8},{20,12},{24,0},{28,4},{1,25},{... | collective-permute-start | bytes 245768 | tf_op jit(solution)/shard_map/ppermute | solution.py:417
  60.1 0.2 collective-permute-done.3.refs_4_
  60.3 7.8 %collective-permute-start.6 = (bf16[160,256]{1,0:T(8,128)(2,1)S(1)}, bf16[160,256]{1,0:T(8,128)(2,1)S(1)}, u32[]{:S(2)}, u32[]{:S(2)}) collective-permute-start(bf16[160,256]{1,0:T(8,128)(2,1)S(1)} %get-tuple-element.44), channel_id=1, source_target_pairs={{0,28},{4,24},{8,20},{12,16},{16,12},{20,8},{24,4},{28,0},{1,29},{... | collective-permute-start | bytes 245768 | tf_op jit(solution)/shard_map/ppermute | solution.py:417
  68.1 0.5 collective-permute-start
  68.6 0.0 collective-permute-done.5.refs_6_
  68.6 0.0 collective-permute-start.1
  68.6 2.3 %collective-permute-done.6.refs_7_ = bf16[160,256]{1,0:T(8,128)(2,1)S(1)} collective-permute-done((bf16[160,256]{1,0:T(8,128)(2,1)S(1)}, bf16[160,256]{1,0:T(8,128)(2,1)S(1)}, u32[]{:S(2)}, u32[]{:S(2)}) %collective-permute-start.6) | collective-permute-done | bytes 81952 | tf_op jit(solution)/shard_map/ppermute | solution.py:417
  71.0 1.4 %collective-permute-start.2 = (bf16[160,512]{1,0:T(8,128)(2,1)S(1)}, bf16[160,512]{1,0:T(8,128)(2,1)S(1)}, u32[]{:S(2)}, u32[]{:S(2)}) collective-permute-start(bf16[160,512]{1,0:T(8,128)(2,1)S(1)} %get-tuple-element.40), channel_id=1, source_target_pairs={{0,12},{4,8},{8,4},{12,0},{16,28},{20,24},{24,20},{28,16},{1,13},{... | collective-permute-start | bytes 491528 | tf_op jit(solution)/shard_map/ppermute | solution.py:417
  72.3 2.7 %collective-permute-done.refs_1_.refs_0_ = bf16[160,512]{1,0:T(8,128)(2,1)S(1)} collective-permute-done((bf16[160,512]{1,0:T(8,128)(2,1)S(1)}, bf16[160,512]{1,0:T(8,128)(2,1)S(1)}, u32[]{:S(2)}, u32[]{:S(2)}) %collective-permute-start) | collective-permute-done | bytes 163872 | tf_op jit(solution)/shard_map/ppermute | solution.py:417
  75.0 0.4 collective-permute-start.10
  75.4 0.3 collective-permute-done.1.refs_2_.refs_1_
  75.7 1.2 %collective-permute-start.11 = (bf16[160,512]{1,0:T(8,128)(2,1)S(1)}, bf16[160,512]{1,0:T(8,128)(2,1)S(1)}, u32[]{:S(2)}, u32[]{:S(2)}) collective-permute-start(bf16[160,512]{1,0:T(8,128)(2,1)S(1)} %get-tuple-element.52), channel_id=1, source_target_pairs={{0,8},{4,12},{8,0},{12,4},{16,24},{20,28},{24,16},{28,20},{1,9},{5... | collective-permute-start | bytes 491528 | tf_op jit(solution)/shard_map/ppermute | solution.py:417
  77.0 3.0 %collective-permute-done.2.refs_3_.refs_2_ = bf16[160,512]{1,0:T(8,128)(2,1)S(1)} collective-permute-done((bf16[160,512]{1,0:T(8,128)(2,1)S(1)}, bf16[160,512]{1,0:T(8,128)(2,1)S(1)}, u32[]{:S(2)}, u32[]{:S(2)}) %collective-permute-start.2) | collective-permute-done | bytes 163872 | tf_op jit(solution)/shard_map/ppermute | solution.py:417
  79.9 1.5 %collective-permute-start.12 = (bf16[160,512]{1,0:T(8,128)(2,1)S(1)}, bf16[160,512]{1,0:T(8,128)(2,1)S(1)}, u32[]{:S(2)}, u32[]{:S(2)}) collective-permute-start(bf16[160,512]{1,0:T(8,128)(2,1)S(1)} %get-tuple-element.53), channel_id=1, source_target_pairs={{0,12},{4,8},{8,4},{12,0},{16,28},{20,24},{24,20},{28,16},{1,13},{... | collective-permute-start | bytes 491528 | tf_op jit(solution)/shard_map/ppermute | solution.py:417
  81.4 1.8 %collective-permute-done.10.refs_1_.refs_0_ = bf16[160,512]{1,0:T(8,128)(2,1)S(1)} collective-permute-done((bf16[160,512]{1,0:T(8,128)(2,1)S(1)}, bf16[160,512]{1,0:T(8,128)(2,1)S(1)}, u32[]{:S(2)}, u32[]{:S(2)}) %collective-permute-start.10) | collective-permute-done | bytes 163872 | tf_op jit(solution)/shard_map/ppermute | solution.py:417
  83.2 1.2 collective-permute-start.13
  84.3 0.1 spread.4.refs_1_.refs_3_
  84.5 0.3 spread.5
  84.8 2.2 %collective-permute-start.14 = (bf16[160,256]{1,0:T(8,128)(2,1)S(1)}, bf16[160,256]{1,0:T(8,128)(2,1)S(1)}, u32[]{:S(2)}, u32[]{:S(2)}) collective-permute-start(bf16[160,256]{1,0:T(8,128)(2,1)S(1)} %get-tuple-element.55), channel_id=1, source_target_pairs={{0,20},{4,16},{8,28},{12,24},{16,4},{20,0},{24,12},{28,8},{1,21},{... | collective-permute-start | bytes 245768 | tf_op jit(solution)/shard_map/ppermute | solution.py:417
  87.0 0.0 collective-permute-done.12.refs_3_.refs_2_
  87.0 3.0 %collective-permute-start.15 = (bf16[160,256]{1,0:T(8,128)(2,1)S(1)}, bf16[160,256]{1,0:T(8,128)(2,1)S(1)}, u32[]{:S(2)}, u32[]{:S(2)}) collective-permute-start(bf16[160,256]{1,0:T(8,128)(2,1)S(1)} %get-tuple-element.56), channel_id=1, source_target_pairs={{0,24},{4,28},{8,16},{12,20},{16,8},{20,12},{24,0},{28,4},{1,25},{... | collective-permute-start | bytes 245768 | tf_op jit(solution)/shard_map/ppermute | solution.py:417
  90.0 0.1 spread.6.refs_1_.refs_3_
  90.1 3.7 %collective-permute-done.13.refs_4_ = bf16[160,256]{1,0:T(8,128)(2,1)S(1)} collective-permute-done((bf16[160,256]{1,0:T(8,128)(2,1)S(1)}, bf16[160,256]{1,0:T(8,128)(2,1)S(1)}, u32[]{:S(2)}, u32[]{:S(2)}) %collective-permute-start.13) | collective-permute-done | bytes 81952 | tf_op jit(solution)/shard_map/ppermute | solution.py:417
  93.8 1.3 %collective-permute-start.16 = (bf16[160,256]{1,0:T(8,128)(2,1)S(1)}, bf16[160,256]{1,0:T(8,128)(2,1)S(1)}, u32[]{:S(2)}, u32[]{:S(2)}) collective-permute-start(bf16[160,256]{1,0:T(8,128)(2,1)S(1)} %get-tuple-element.57), channel_id=1, source_target_pairs={{0,28},{4,24},{8,20},{12,16},{16,12},{20,8},{24,4},{28,0},{1,29},{... | collective-permute-start | bytes 245768 | tf_op jit(solution)/shard_map/ppermute | solution.py:417
  95.0 3.9 %attend.5 = (bf16[160,256]{1,0:T(8,128)(2,1)S(1)}, bf16[160,256]{1,0:T(8,128)(2,1)S(1)}, bf16[160,256]{1,0:T(8,128)(2,1)S(1)}) custom-call(bf16[160,512]{1,0:T(8,128)(2,1)S(1)} %collective-permute-done.refs_1_.refs_0_, bf16[160,512]{1,0:T(8,128)(2,1)S(1)} %collective-permute-done.1.refs_2_.refs_1_, ...), custom_call_target="tpu_custom_call" | custom-call | flops 1258291200 | bytes 1310720 | tf_op jit(solution)/shard_map/attend/pallas_call | solution.py:333
  98.9 0.0 collective-permute-done.14.refs_5_
  98.9 1.6 %collective-permute-start.7 = (bf16[160,256]{1,0:T(8,128)(2,1)S(1)}, bf16[160,256]{1,0:T(8,128)(2,1)S(1)}, u32[]{:S(2)}, u32[]{:S(2)}) collective-permute-start(bf16[160,256]{1,0:T(8,128)(2,1)S(1)} %get-tuple-element.47), channel_id=1, source_target_pairs={{0,4},{4,0},{8,12},{12,8},{16,20},{20,16},{24,28},{28,24},{1,5},{5... | collective-permute-start | bytes 245768 | tf_op jit(solution)/shard_map/ppermute | solution.py:417
  100.5 0.4 collective-permute-done.16.refs_7_
  100.9 1.6 %collective-permute-start.9 = (bf16[160,256]{1,0:T(8,128)(2,1)S(1)}, bf16[160,256]{1,0:T(8,128)(2,1)S(1)}, u32[]{:S(2)}, u32[]{:S(2)}) collective-permute-start(bf16[160,256]{1,0:T(8,128)(2,1)S(1)} %get-tuple-element.49), channel_id=1, source_target_pairs={{0,12},{4,8},{8,4},{12,0},{16,28},{20,24},{24,20},{28,16},{1,13},{... | collective-permute-start | bytes 245768 | tf_op jit(solution)/shard_map/ppermute | solution.py:417
  102.5 0.3 spread.7
  102.8 0.8 score.1.refs_6_
  103.6 1.5 %attend.4.refs_0_ = bf16[160,256]{1,0:T(8,128)(2,1)S(1)} custom-call(bf16[160,512]{1,0:T(8,128)(2,1)S(1)} %get-tuple-element.37.refs_0_, bf16[2,1280,128]{2,1,0:T(8,128)(2,1)S(1)} %spread.4.refs_1_.refs_3_, bf16[2,1280,128]{2,1,0:T(8,128)(2,1)S(1)} %get-tuple-element.45.refs_2_.refs_4_, bf16[2,2560,128]{2,1,0:T(8,128)(2,1)S(1)} %get-tuple-element.46.refs_3_.refs_5_), custom_call_target="tpu_custom_call" | custom-call | flops 419430400 | bytes 1310720 | tf_op jit(solution)/shard_map/attend/pallas_call | solution.py:333
  105.1 3.4 %attend.7 = (bf16[160,256]{1,0:T(8,128)(2,1)S(1)}, bf16[160,256]{1,0:T(8,128)(2,1)S(1)}, bf16[160,256]{1,0:T(8,128)(2,1)S(1)}) custom-call(bf16[160,512]{1,0:T(8,128)(2,1)S(1)} %collective-permute-done.10.refs_1_.refs_0_, bf16[160,512]{1,0:T(8,128)(2,1)S(1)} %collective-permute-done.11.refs_2_.refs_1_, ...), custom_call_target="tpu_custom_call" | custom-call | flops 1258291200 | bytes 1310720 | tf_op jit(solution)/shard_map/attend/pallas_call | solution.py:333
  108.6 0.0 copy-start
  108.6 1.6 %collective-permute-start.17 = (bf16[160,256]{1,0:T(8,128)(2,1)S(1)}, bf16[160,256]{1,0:T(8,128)(2,1)S(1)}, u32[]{:S(2)}, u32[]{:S(2)}) collective-permute-start(bf16[160,256]{1,0:T(8,128)(2,1)S(1)} %get-tuple-element.60), channel_id=1, source_target_pairs={{0,4},{4,0},{8,12},{12,8},{16,20},{20,16},{24,28},{28,24},{1,5},{5... | collective-permute-start | bytes 245768 | tf_op jit(solution)/shard_map/ppermute | solution.py:417
  110.2 0.7 collective-permute-start.18
  110.9 1.4 %collective-permute-start.19 = (bf16[160,256]{1,0:T(8,128)(2,1)S(1)}, bf16[160,256]{1,0:T(8,128)(2,1)S(1)}, u32[]{:S(2)}, u32[]{:S(2)}) collective-permute-start(bf16[160,256]{1,0:T(8,128)(2,1)S(1)} %get-tuple-element.62), channel_id=1, source_target_pairs={{0,12},{4,8},{8,4},{12,0},{16,28},{20,24},{24,20},{28,16},{1,13},{... | collective-permute-start | bytes 245768 | tf_op jit(solution)/shard_map/ppermute | solution.py:417
  112.3 1.5 %attend.6.refs_4_ = bf16[160,256]{1,0:T(8,128)(2,1)S(1)} custom-call(bf16[160,512]{1,0:T(8,128)(2,1)S(1)} %get-tuple-element.50.refs_0_, bf16[2,1280,128]{2,1,0:T(8,128)(2,1)S(1)} %spread.6.refs_1_.refs_3_, bf16[2,1280,128]{2,1,0:T(8,128)(2,1)S(1)} %get-tuple-element.58.refs_2_.refs_4_, bf16[2,2560,128]{2,1,0:T(8,128)(2,1)S(1)} %get-tuple-element.59.refs_3_.refs_5_), custom_call_target="tpu_custom_call" | custom-call | flops 419430400 | bytes 1310720 | tf_op jit(solution)/shard_map/attend/pallas_call | solution.py:333
  113.9 0.8 project.3
  114.7 1.5 %collective-permute-done.19.refs_2_.refs_7_ = bf16[160,256]{1,0:T(8,128)(2,1)S(1)} collective-permute-done((bf16[160,256]{1,0:T(8,128)(2,1)S(1)}, bf16[160,256]{1,0:T(8,128)(2,1)S(1)}, u32[]{:S(2)}, u32[]{:S(2)}) %collective-permute-start.19) | collective-permute-done | bytes 81952 | tf_op jit(solution)/shard_map/ppermute | solution.py:417
  116.2 0.6 project.4
  116.8 1.2 %project.5 = bf16[160,2048]{1,0:T(8,128)(2,1)} custom-call(bf16[160,256]{1,0:T(8,128)(2,1)S(1)} %attend.4.refs_0_, bf16[160,256]{1,0:T(8,128)(2,1)S(1)} %collective-permute-done.7.refs_1_, bf16[160,256]{1,0:T(8,128)(2,1)S(1)} %collective-permute-done.8.refs_2_, bf16[160,256]{1,0:T(8,128)(2,1)S(1)} %collective-permute-done.9.refs_3_, ...), custom_call_target="tpu_custom_call" | custom-call | flops 335544320 | bytes 4194304 | tf_op jit(solution)/shard_map/project/pallas_call | solution.py:403
  (14 shorter events, 0.0 us)
Async XLA Ops:
  0.0 48.8 %collective-permute-start.20 = (bf16[2048,512]{1,0:T(8,128)(2,1)}, bf16[2048,512]{1,0:T(8,128)(2,1)S(1)}, u32[]{:S(2)}, u32[]{:S(2)}) collective-permute-start(bf16[2048,512]{1,0:T(8,128)(2,1)} %refs_3_.1), channel_id=1, source_target_pairs={{0,2},{1,3},{2,0},{3,1},{4,6},{5,7},{6,4},{7,5},{8,10},{9,11},{10,... | collective-permute-start | bytes 6291464 | tf_op jit(solution)/shard_map/ppermute | solution.py:417
  3.0 110.9 %collective-permute-start.22 = (bf16[2048,512]{1,0:T(8,128)(2,1)}, bf16[2048,512]{1,0:T(8,128)(2,1)S(1)}, u32[]{:S(2)}, u32[]{:S(2)}) collective-permute-start(bf16[2048,512]{1,0:T(8,128)(2,1)} %refs_3_.1), channel_id=1, source_target_pairs={{0,1},{1,0},{2,3},{3,2},{4,5},{5,4},{6,7},{7,6},{8,9},{9,8},{10,11... | collective-permute-start | bytes 6291464 | tf_op jit(solution)/shard_map/ppermute | solution.py:417
  48.8 68.0 %collective-permute-start.21 = (bf16[2048,512]{1,0:T(8,128)(2,1)S(1)}, bf16[2048,512]{1,0:T(8,128)(2,1)S(1)}, u32[]{:S(2)}, u32[]{:S(2)}) collective-permute-start(bf16[2048,512]{1,0:T(8,128)(2,1)S(1)} %collective-permute-done.20.refs_7_.refs_5_), channel_id=1, source_target_pairs={{0,1},{1,0},{2,3},{3,2},{4,5},{5,4},{6,7},{7,6},{8,9},{9,8},{10,11... | collective-permute-start | bytes 6291464 | tf_op jit(solution)/shard_map/ppermute | solution.py:417
  52.3 8.0 %collective-permute-start.3 = (bf16[160,256]{1,0:T(8,128)(2,1)S(1)}, bf16[160,256]{1,0:T(8,128)(2,1)S(1)}, u32[]{:S(2)}, u32[]{:S(2)}) collective-permute-start(bf16[160,256]{1,0:T(8,128)(2,1)S(1)} %get-tuple-element.41), channel_id=1, source_target_pairs={{0,16},{4,20},{8,24},{12,28},{16,0},{20,4},{24,8},{28,12},{1,17},{... | collective-permute-start | bytes 245768 | tf_op jit(solution)/shard_map/ppermute | solution.py:417
  55.2 12.9 %collective-permute-start.4 = (bf16[160,256]{1,0:T(8,128)(2,1)S(1)}, bf16[160,256]{1,0:T(8,128)(2,1)S(1)}, u32[]{:S(2)}, u32[]{:S(2)}) collective-permute-start(bf16[160,256]{1,0:T(8,128)(2,1)S(1)} %get-tuple-element.42), channel_id=1, source_target_pairs={{0,20},{4,16},{8,28},{12,24},{16,4},{20,0},{24,12},{28,8},{1,21},{... | collective-permute-start | bytes 245768 | tf_op jit(solution)/shard_map/ppermute | solution.py:417
  56.5 12.1 %collective-permute-start.5 = (bf16[160,256]{1,0:T(8,128)(2,1)S(1)}, bf16[160,256]{1,0:T(8,128)(2,1)S(1)}, u32[]{:S(2)}, u32[]{:S(2)}) collective-permute-start(bf16[160,256]{1,0:T(8,128)(2,1)S(1)} %get-tuple-element.43), channel_id=1, source_target_pairs={{0,24},{4,28},{8,16},{12,20},{16,8},{20,12},{24,0},{28,4},{1,25},{... | collective-permute-start | bytes 245768 | tf_op jit(solution)/shard_map/ppermute | solution.py:417
  60.3 10.7 %collective-permute-start.6 = (bf16[160,256]{1,0:T(8,128)(2,1)S(1)}, bf16[160,256]{1,0:T(8,128)(2,1)S(1)}, u32[]{:S(2)}, u32[]{:S(2)}) collective-permute-start(bf16[160,256]{1,0:T(8,128)(2,1)S(1)} %get-tuple-element.44), channel_id=1, source_target_pairs={{0,28},{4,24},{8,20},{12,16},{16,12},{20,8},{24,4},{28,0},{1,29},{... | collective-permute-start | bytes 245768 | tf_op jit(solution)/shard_map/ppermute | solution.py:417
  68.1 6.9 %collective-permute-start = (bf16[160,512]{1,0:T(8,128)(2,1)S(1)}, bf16[160,512]{1,0:T(8,128)(2,1)S(1)}, u32[]{:S(2)}, u32[]{:S(2)}) collective-permute-start(bf16[160,512]{1,0:T(8,128)(2,1)S(1)} %get-tuple-element.38), channel_id=1, source_target_pairs={{0,4},{4,0},{8,12},{12,8},{16,20},{20,16},{24,28},{28,24},{1,5},{5... | collective-permute-start | bytes 491528 | tf_op jit(solution)/shard_map/ppermute | solution.py:417
  68.6 7.1 %collective-permute-start.1 = (bf16[160,512]{1,0:T(8,128)(2,1)S(1)}, bf16[160,512]{1,0:T(8,128)(2,1)S(1)}, u32[]{:S(2)}, u32[]{:S(2)}) collective-permute-start(bf16[160,512]{1,0:T(8,128)(2,1)S(1)} %get-tuple-element.39), channel_id=1, source_target_pairs={{0,8},{4,12},{8,0},{12,4},{16,24},{20,28},{24,16},{28,20},{1,9},{5... | collective-permute-start | bytes 491528 | tf_op jit(solution)/shard_map/ppermute | solution.py:417
  71.0 9.0 %collective-permute-start.2 = (bf16[160,512]{1,0:T(8,128)(2,1)S(1)}, bf16[160,512]{1,0:T(8,128)(2,1)S(1)}, u32[]{:S(2)}, u32[]{:S(2)}) collective-permute-start(bf16[160,512]{1,0:T(8,128)(2,1)S(1)} %get-tuple-element.40), channel_id=1, source_target_pairs={{0,12},{4,8},{8,4},{12,0},{16,28},{20,24},{24,20},{28,16},{1,13},{... | collective-permute-start | bytes 491528 | tf_op jit(solution)/shard_map/ppermute | solution.py:417
  75.0 8.2 %collective-permute-start.10 = (bf16[160,512]{1,0:T(8,128)(2,1)S(1)}, bf16[160,512]{1,0:T(8,128)(2,1)S(1)}, u32[]{:S(2)}, u32[]{:S(2)}) collective-permute-start(bf16[160,512]{1,0:T(8,128)(2,1)S(1)} %get-tuple-element.51), channel_id=1, source_target_pairs={{0,4},{4,0},{8,12},{12,8},{16,20},{20,16},{24,28},{28,24},{1,5},{5... | collective-permute-start | bytes 491528 | tf_op jit(solution)/shard_map/ppermute | solution.py:417
  75.7 9.0 %collective-permute-start.11 = (bf16[160,512]{1,0:T(8,128)(2,1)S(1)}, bf16[160,512]{1,0:T(8,128)(2,1)S(1)}, u32[]{:S(2)}, u32[]{:S(2)}) collective-permute-start(bf16[160,512]{1,0:T(8,128)(2,1)S(1)} %get-tuple-element.52), channel_id=1, source_target_pairs={{0,8},{4,12},{8,0},{12,4},{16,24},{20,28},{24,16},{28,20},{1,9},{5... | collective-permute-start | bytes 491528 | tf_op jit(solution)/shard_map/ppermute | solution.py:417
  79.9 7.0 %collective-permute-start.12 = (bf16[160,512]{1,0:T(8,128)(2,1)S(1)}, bf16[160,512]{1,0:T(8,128)(2,1)S(1)}, u32[]{:S(2)}, u32[]{:S(2)}) collective-permute-start(bf16[160,512]{1,0:T(8,128)(2,1)S(1)} %get-tuple-element.53), channel_id=1, source_target_pairs={{0,12},{4,8},{8,4},{12,0},{16,28},{20,24},{24,20},{28,16},{1,13},{... | collective-permute-start | bytes 491528 | tf_op jit(solution)/shard_map/ppermute | solution.py:417
  83.2 10.6 %collective-permute-start.13 = (bf16[160,256]{1,0:T(8,128)(2,1)S(1)}, bf16[160,256]{1,0:T(8,128)(2,1)S(1)}, u32[]{:S(2)}, u32[]{:S(2)}) collective-permute-start(bf16[160,256]{1,0:T(8,128)(2,1)S(1)} %get-tuple-element.54), channel_id=1, source_target_pairs={{0,16},{4,20},{8,24},{12,28},{16,0},{20,4},{24,8},{28,12},{1,17},{... | collective-permute-start | bytes 245768 | tf_op jit(solution)/shard_map/ppermute | solution.py:417
  84.8 14.2 %collective-permute-start.14 = (bf16[160,256]{1,0:T(8,128)(2,1)S(1)}, bf16[160,256]{1,0:T(8,128)(2,1)S(1)}, u32[]{:S(2)}, u32[]{:S(2)}) collective-permute-start(bf16[160,256]{1,0:T(8,128)(2,1)S(1)} %get-tuple-element.55), channel_id=1, source_target_pairs={{0,20},{4,16},{8,28},{12,24},{16,4},{20,0},{24,12},{28,8},{1,21},{... | collective-permute-start | bytes 245768 | tf_op jit(solution)/shard_map/ppermute | solution.py:417
  87.0 13.6 %collective-permute-start.15 = (bf16[160,256]{1,0:T(8,128)(2,1)S(1)}, bf16[160,256]{1,0:T(8,128)(2,1)S(1)}, u32[]{:S(2)}, u32[]{:S(2)}) collective-permute-start(bf16[160,256]{1,0:T(8,128)(2,1)S(1)} %get-tuple-element.56), channel_id=1, source_target_pairs={{0,24},{4,28},{8,16},{12,20},{16,8},{20,12},{24,0},{28,4},{1,25},{... | collective-permute-start | bytes 245768 | tf_op jit(solution)/shard_map/ppermute | solution.py:417
  93.8 7.1 %collective-permute-start.16 = (bf16[160,256]{1,0:T(8,128)(2,1)S(1)}, bf16[160,256]{1,0:T(8,128)(2,1)S(1)}, u32[]{:S(2)}, u32[]{:S(2)}) collective-permute-start(bf16[160,256]{1,0:T(8,128)(2,1)S(1)} %get-tuple-element.57), channel_id=1, source_target_pairs={{0,28},{4,24},{8,20},{12,16},{16,12},{20,8},{24,4},{28,0},{1,29},{... | collective-permute-start | bytes 245768 | tf_op jit(solution)/shard_map/ppermute | solution.py:417
  98.9 9.6 %collective-permute-start.7 = (bf16[160,256]{1,0:T(8,128)(2,1)S(1)}, bf16[160,256]{1,0:T(8,128)(2,1)S(1)}, u32[]{:S(2)}, u32[]{:S(2)}) collective-permute-start(bf16[160,256]{1,0:T(8,128)(2,1)S(1)} %get-tuple-element.47), channel_id=1, source_target_pairs={{0,4},{4,0},{8,12},{12,8},{16,20},{20,16},{24,28},{28,24},{1,5},{5... | collective-permute-start | bytes 245768 | tf_op jit(solution)/shard_map/ppermute | solution.py:417
  100.5 9.6 %collective-permute-start.8 = (bf16[160,256]{1,0:T(8,128)(2,1)S(1)}, bf16[160,256]{1,0:T(8,128)(2,1)S(1)}, u32[]{:S(2)}, u32[]{:S(2)}) collective-permute-start(bf16[160,256]{1,0:T(8,128)(2,1)S(1)} %get-tuple-element.48), channel_id=1, source_target_pairs={{0,8},{4,12},{8,0},{12,4},{16,24},{20,28},{24,16},{28,20},{1,9},{5... | collective-permute-start | bytes 245768 | tf_op jit(solution)/shard_map/ppermute | solution.py:417
  100.9 10.0 %collective-permute-start.9 = (bf16[160,256]{1,0:T(8,128)(2,1)S(1)}, bf16[160,256]{1,0:T(8,128)(2,1)S(1)}, u32[]{:S(2)}, u32[]{:S(2)}) collective-permute-start(bf16[160,256]{1,0:T(8,128)(2,1)S(1)} %get-tuple-element.49), channel_id=1, source_target_pairs={{0,12},{4,8},{8,4},{12,0},{16,28},{20,24},{24,20},{28,16},{1,13},{... | collective-permute-start | bytes 245768 | tf_op jit(solution)/shard_map/ppermute | solution.py:417
  108.6 5.3 %copy-start = (bf16[2048,512]{1,0:T(8,128)(2,1)S(1)}, bf16[2048,512]{1,0:T(8,128)(2,1)}, u32[]{:S(2)}) copy-start(bf16[2048,512]{1,0:T(8,128)(2,1)} %refs_3_.1) | copy-start | bytes 6291460
  108.6 6.1 %collective-permute-start.17 = (bf16[160,256]{1,0:T(8,128)(2,1)S(1)}, bf16[160,256]{1,0:T(8,128)(2,1)S(1)}, u32[]{:S(2)}, u32[]{:S(2)}) collective-permute-start(bf16[160,256]{1,0:T(8,128)(2,1)S(1)} %get-tuple-element.60), channel_id=1, source_target_pairs={{0,4},{4,0},{8,12},{12,8},{16,20},{20,16},{24,28},{28,24},{1,5},{5... | collective-permute-start | bytes 245768 | tf_op jit(solution)/shard_map/ppermute | solution.py:417
  110.2 4.6 %collective-permute-start.18 = (bf16[160,256]{1,0:T(8,128)(2,1)S(1)}, bf16[160,256]{1,0:T(8,128)(2,1)S(1)}, u32[]{:S(2)}, u32[]{:S(2)}) collective-permute-start(bf16[160,256]{1,0:T(8,128)(2,1)S(1)} %get-tuple-element.61), channel_id=1, source_target_pairs={{0,8},{4,12},{8,0},{12,4},{16,24},{20,28},{24,16},{28,20},{1,9},{5... | collective-permute-start | bytes 245768 | tf_op jit(solution)/shard_map/ppermute | solution.py:417
  110.9 5.3 %collective-permute-start.19 = (bf16[160,256]{1,0:T(8,128)(2,1)S(1)}, bf16[160,256]{1,0:T(8,128)(2,1)S(1)}, u32[]{:S(2)}, u32[]{:S(2)}) collective-permute-start(bf16[160,256]{1,0:T(8,128)(2,1)S(1)} %get-tuple-element.62), channel_id=1, source_target_pairs={{0,12},{4,8},{8,4},{12,0},{16,28},{20,24},{24,20},{28,16},{1,13},{... | collective-permute-start | bytes 245768 | tf_op jit(solution)/shard_map/ppermute | solution.py:417

commit v6 on v5

--- a/solution.py
+++ b/solution.py
@@ -368,33 +368,36 @@
 
 
 def second_kernel(groups, *refs):
-    att_refs, w_refs, sums, made = refs[:-9], refs[-9:-6], refs[-6:-3], refs[-3:]
+    parts, refs = (refs[:groups], refs[groups : 2 * groups]), refs[2 * groups :]
+    w_refs, sums, made, whole_ref = refs[0:3], refs[3:6], refs[6:9], refs[9]
     for w_ref, sum_ref, made_ref in zip(w_refs, sums, made):
         total = sum_ref[...]
         for j in range(1, groups):
-            total = total + term(att_refs[j - 1], w_ref, groups, j, 1)
+            total = total + term(parts[1][j], w_ref, groups, j, 1)
         made_ref[...] = total.astype(jnp.bfloat16)
+    for c in range(2):
+        for j in range(groups):
+            start = pl.multiple_of(((home_of(groups) ^ j) * 2 + c) * 2 * TILE, 2 * TILE)
+            whole_ref[:, pl.ds(start, 2 * TILE)] = parts[c][j][...]
 
 
 def third_kernel(groups, *refs):
-    parts, refs = (refs[:groups], refs[groups : 2 * groups]), refs[2 * groups :]
-    source, made, (out_ref, last, sems) = refs[0], refs[1:4], refs[4:]
+    whole_ref, source, made, (out_ref, last, sems) = refs[0], refs[1], refs[2:5], refs[5:]
     width = source.shape[1]
-
-    def leave(i, ready):
-        column = pl.ds(pl.multiple_of((lax.axis_index("dp") ^ i) * width, width), width)
-        copy = pltpu.make_async_copy(ready, out_ref.at[:, column], sems.at[i])
+    half = width // 2
+
+    def leave(i, ready, shift, n):
+        column = pl.ds(pl.multiple_of((lax.axis_index("dp") ^ i) * width + shift, half), ready.shape[1])
+        copy = pltpu.make_async_copy(ready, out_ref.at[:, column], sems.at[n])
         copy.start()
         return copy
 
-    leaving = [leave(i, ready) for i, ready in enumerate(made)]
-    total = None
-    for c in range(2):
-        for j in range(groups):
-            part = term(parts[c][j], source, groups, j, c)
-            total = part if total is None else total + part
-    last[...] = total.astype(jnp.bfloat16)
-    for copy in leaving + [leave(3, last)]:
+    leaving = [leave(i, ready, 0, i) for i, ready in enumerate(made)]
+    for n in range(2):
+        lanes = slice(n * half, (n + 1) * half)
+        last[n] = jnp.dot(whole_ref[...], source[:, lanes], preferred_element_type=jnp.float32).astype(jnp.bfloat16)
+        leaving.append(leave(3, last.at[n], n * half, 3 + n))
+    for copy in leaving:
         copy.wait()
 
 
@@ -448,15 +451,20 @@
     sums = project_call(
         first_kernel, groups, [*back[0], back[1][0], *near_blocks], [block(jnp.float32)] * 3, [], 2 * flops
     )
-    made = project_call(
-        second_kernel, groups, [*back[1][1:], *near_blocks, *sums], [block(jnp.bfloat16)] * 3, [], flops
+    *made, whole = project_call(
+        second_kernel,
+        groups,
+        [*back[0], *back[1], *near_blocks, *sums],
+        [block(jnp.bfloat16)] * 3 + [jax.ShapeDtypeStruct((tok, w_out.shape[0]), jnp.bfloat16)],
+        [],
+        flops,
     )
     mixed = project_call(
         third_kernel,
         groups,
-        [*back[0], *back[1], corner, *made],
+        [whole, corner, *made],
         jax.ShapeDtypeStruct((tok, 4 * width), jnp.bfloat16),
-        [pltpu.VMEM((tok, width), jnp.bfloat16), pltpu.SemaphoreType.DMA((4,))],
+        [pltpu.VMEM((2, tok, width // 2), jnp.bfloat16), pltpu.SemaphoreType.DMA((5,))],
         flops,
     )
     return mixed[None]

time: 118 us -> 118 us (level)
  no operation moved by 1% of the time
where the time goes in v6:
time: 118 us
  waiting for transfers between devices  61.6 us (52%)
  starting transfers between devices  38.2 us (32%)
  Pallas kernels  17.3 us (15%)
    ppermute x23, waiting for transfers between devices, exchanged(): return lax.ppermute(block, axis, [(i, i ^ flip) for i in range(count)])  61.6 us
    ppermute x23, starting transfers between devices, exchanged(): return lax.ppermute(block, axis, [(i, i ^ flip) for i in range(count)])  38.2 us
    pallas_call x4, Pallas kernels, attend(): pl.pallas_call(functools.partial(attend_kernel, count, len(given)), in_sp...  10.4 us
    pallas_call x1, Pallas kernels, turn_and_pack(): pl.pallas_call(functools.partial(turn_kernel, groups, chunks), in_specs=[...  2.68 us
    pallas_call x3, Pallas kernels, project_call(): pl.pallas_call(functools.partial(kernel, groups), in_specs=in_vmem(len(in...  2.68 us
  transfers between devices with their start and end apart: 23, of which 10 were waited for; matrix products, arithmetic and copies ran while one was open for 1% of the time, Pallas kernels for 14%

profile of v6, /device:TPU:0, one launch (start us, length us, event | category | flops | bytes accessed | tf_op | source)
XLA Modules:
  0.0 118.3 jit_solution(13403078358194043130)
XLA Ops:
  0.0 3.0 %collective-permute-start.21 = (bf16[2048,512]{1,0:T(8,128)(2,1)}, bf16[2048,512]{1,0:T(8,128)(2,1)S(1)}, u32[]{:S(2)}, u32[]{:S(2)}) collective-permute-start(bf16[2048,512]{1,0:T(8,128)(2,1)} %refs_8_.1), channel_id=1, source_target_pairs={{0,2},{1,3},{2,0},{3,1},{4,6},{5,7},{6,4},{7,5},{8,10},{9,11},{10,... | collective-permute-start | bytes 6291464 | tf_op jit(solution)/shard_map/ppermute | solution.py:420
  3.0 45.8 %collective-permute-done.21.refs_7_.refs_10_ = bf16[2048,512]{1,0:T(8,128)(2,1)S(1)} collective-permute-done((bf16[2048,512]{1,0:T(8,128)(2,1)}, bf16[2048,512]{1,0:T(8,128)(2,1)S(1)}, u32[]{:S(2)}, u32[]{:S(2)}) %collective-permute-start.21) | collective-permute-done | bytes 2097184 | tf_op jit(solution)/shard_map/ppermute | solution.py:420
  48.8 0.8 maximum_bitcast_fusion.refs_3_
  49.6 2.7 %turn.1 = (bf16[160,512]{1,0:T(8,128)(2,1)S(1)}, bf16[160,512]{1,0:T(8,128)(2,1)S(1)}, bf16[160,512]{1,0:T(8,128)(2,1)S(1)}, bf16[160,512]{1,0:T(8,128)(2,1)S(1)...) custom-call(bf16[160,2048]{1,0:T(8,128)(2,1)} %bitcast.12, ...), custom_call_target="tpu_custom_call" | custom-call | flops 19660800 | bytes 3932160 | tf_op jit(solution)/shard_map/turn/pallas_call | solution.py:214
  52.3 2.9 %collective-permute-start.3 = (bf16[160,256]{1,0:T(8,128)(2,1)S(1)}, bf16[160,256]{1,0:T(8,128)(2,1)S(1)}, u32[]{:S(2)}, u32[]{:S(2)}) collective-permute-start(bf16[160,256]{1,0:T(8,128)(2,1)S(1)} %get-tuple-element.42), channel_id=1, source_target_pairs={{0,16},{4,20},{8,24},{12,28},{16,0},{20,4},{24,8},{28,12},{1,17},{... | collective-permute-start | bytes 245768 | tf_op jit(solution)/shard_map/ppermute | solution.py:420
  55.2 1.3 %collective-permute-start.4 = (bf16[160,256]{1,0:T(8,128)(2,1)S(1)}, bf16[160,256]{1,0:T(8,128)(2,1)S(1)}, u32[]{:S(2)}, u32[]{:S(2)}) collective-permute-start(bf16[160,256]{1,0:T(8,128)(2,1)S(1)} %get-tuple-element.43), channel_id=1, source_target_pairs={{0,20},{4,16},{8,28},{12,24},{16,4},{20,0},{24,12},{28,8},{1,21},{... | collective-permute-start | bytes 245768 | tf_op jit(solution)/shard_map/ppermute | solution.py:420
  56.5 3.6 %collective-permute-start.5 = (bf16[160,256]{1,0:T(8,128)(2,1)S(1)}, bf16[160,256]{1,0:T(8,128)(2,1)S(1)}, u32[]{:S(2)}, u32[]{:S(2)}) collective-permute-start(bf16[160,256]{1,0:T(8,128)(2,1)S(1)} %get-tuple-element.44), channel_id=1, source_target_pairs={{0,24},{4,28},{8,16},{12,20},{16,8},{20,12},{24,0},{28,4},{1,25},{... | collective-permute-start | bytes 245768 | tf_op jit(solution)/shard_map/ppermute | solution.py:420
  60.1 0.2 collective-permute-done.3.refs_4_
  60.3 7.8 %collective-permute-start.6 = (bf16[160,256]{1,0:T(8,128)(2,1)S(1)}, bf16[160,256]{1,0:T(8,128)(2,1)S(1)}, u32[]{:S(2)}, u32[]{:S(2)}) collective-permute-start(bf16[160,256]{1,0:T(8,128)(2,1)S(1)} %get-tuple-element.45), channel_id=1, source_target_pairs={{0,28},{4,24},{8,20},{12,16},{16,12},{20,8},{24,4},{28,0},{1,29},{... | collective-permute-start | bytes 245768 | tf_op jit(solution)/shard_map/ppermute | solution.py:420
  68.1 0.5 collective-permute-start
  68.6 0.0 collective-permute-done.5.refs_6_
  68.6 0.0 collective-permute-start.1
  68.6 2.3 %collective-permute-done.6.refs_7_ = bf16[160,256]{1,0:T(8,128)(2,1)S(1)} collective-permute-done((bf16[160,256]{1,0:T(8,128)(2,1)S(1)}, bf16[160,256]{1,0:T(8,128)(2,1)S(1)}, u32[]{:S(2)}, u32[]{:S(2)}) %collective-permute-start.6) | collective-permute-done | bytes 81952 | tf_op jit(solution)/shard_map/ppermute | solution.py:420
  71.0 1.4 %collective-permute-start.2 = (bf16[160,512]{1,0:T(8,128)(2,1)S(1)}, bf16[160,512]{1,0:T(8,128)(2,1)S(1)}, u32[]{:S(2)}, u32[]{:S(2)}) collective-permute-start(bf16[160,512]{1,0:T(8,128)(2,1)S(1)} %get-tuple-element.41), channel_id=1, source_target_pairs={{0,12},{4,8},{8,4},{12,0},{16,28},{20,24},{24,20},{28,16},{1,13},{... | collective-permute-start | bytes 491528 | tf_op jit(solution)/shard_map/ppermute | solution.py:420
  72.3 2.7 %collective-permute-done.refs_1_.refs_0_ = bf16[160,512]{1,0:T(8,128)(2,1)S(1)} collective-permute-done((bf16[160,512]{1,0:T(8,128)(2,1)S(1)}, bf16[160,512]{1,0:T(8,128)(2,1)S(1)}, u32[]{:S(2)}, u32[]{:S(2)}) %collective-permute-start) | collective-permute-done | bytes 163872 | tf_op jit(solution)/shard_map/ppermute | solution.py:420
  75.0 0.4 collective-permute-start.10
  75.4 0.3 collective-permute-done.1.refs_2_.refs_1_
  75.7 1.2 %collective-permute-start.11 = (bf16[160,512]{1,0:T(8,128)(2,1)S(1)}, bf16[160,512]{1,0:T(8,128)(2,1)S(1)}, u32[]{:S(2)}, u32[]{:S(2)}) collective-permute-start(bf16[160,512]{1,0:T(8,128)(2,1)S(1)} %get-tuple-element.53), channel_id=1, source_target_pairs={{0,8},{4,12},{8,0},{12,4},{16,24},{20,28},{24,16},{28,20},{1,9},{5... | collective-permute-start | bytes 491528 | tf_op jit(solution)/shard_map/ppermute | solution.py:420
  77.0 3.0 %collective-permute-done.2.refs_3_.refs_2_ = bf16[160,512]{1,0:T(8,128)(2,1)S(1)} collective-permute-done((bf16[160,512]{1,0:T(8,128)(2,1)S(1)}, bf16[160,512]{1,0:T(8,128)(2,1)S(1)}, u32[]{:S(2)}, u32[]{:S(2)}) %collective-permute-start.2) | collective-permute-done | bytes 163872 | tf_op jit(solution)/shard_map/ppermute | solution.py:420
  79.9 1.5 %collective-permute-start.12 = (bf16[160,512]{1,0:T(8,128)(2,1)S(1)}, bf16[160,512]{1,0:T(8,128)(2,1)S(1)}, u32[]{:S(2)}, u32[]{:S(2)}) collective-permute-start(bf16[160,512]{1,0:T(8,128)(2,1)S(1)} %get-tuple-element.54), channel_id=1, source_target_pairs={{0,12},{4,8},{8,4},{12,0},{16,28},{20,24},{24,20},{28,16},{1,13},{... | collective-permute-start | bytes 491528 | tf_op jit(solution)/shard_map/ppermute | solution.py:420
  81.4 1.8 %collective-permute-done.10.refs_1_.refs_0_ = bf16[160,512]{1,0:T(8,128)(2,1)S(1)} collective-permute-done((bf16[160,512]{1,0:T(8,128)(2,1)S(1)}, bf16[160,512]{1,0:T(8,128)(2,1)S(1)}, u32[]{:S(2)}, u32[]{:S(2)}) %collective-permute-start.10) | collective-permute-done | bytes 163872 | tf_op jit(solution)/shard_map/ppermute | solution.py:420
  83.2 1.2 collective-permute-start.13
  84.3 0.1 spread.4.refs_1_.refs_3_
  84.5 0.3 spread.5
  84.8 2.2 %collective-permute-start.14 = (bf16[160,256]{1,0:T(8,128)(2,1)S(1)}, bf16[160,256]{1,0:T(8,128)(2,1)S(1)}, u32[]{:S(2)}, u32[]{:S(2)}) collective-permute-start(bf16[160,256]{1,0:T(8,128)(2,1)S(1)} %get-tuple-element.56), channel_id=1, source_target_pairs={{0,20},{4,16},{8,28},{12,24},{16,4},{20,0},{24,12},{28,8},{1,21},{... | collective-permute-start | bytes 245768 | tf_op jit(solution)/shard_map/ppermute | solution.py:420
  87.0 0.0 collective-permute-done.12.refs_3_.refs_2_
  87.0 3.0 %collective-permute-start.15 = (bf16[160,256]{1,0:T(8,128)(2,1)S(1)}, bf16[160,256]{1,0:T(8,128)(2,1)S(1)}, u32[]{:S(2)}, u32[]{:S(2)}) collective-permute-start(bf16[160,256]{1,0:T(8,128)(2,1)S(1)} %get-tuple-element.57), channel_id=1, source_target_pairs={{0,24},{4,28},{8,16},{12,20},{16,8},{20,12},{24,0},{28,4},{1,25},{... | collective-permute-start | bytes 245768 | tf_op jit(solution)/shard_map/ppermute | solution.py:420
  90.0 0.1 spread.6.refs_1_.refs_3_
  90.1 3.7 %collective-permute-done.13.refs_4_ = bf16[160,256]{1,0:T(8,128)(2,1)S(1)} collective-permute-done((bf16[160,256]{1,0:T(8,128)(2,1)S(1)}, bf16[160,256]{1,0:T(8,128)(2,1)S(1)}, u32[]{:S(2)}, u32[]{:S(2)}) %collective-permute-start.13) | collective-permute-done | bytes 81952 | tf_op jit(solution)/shard_map/ppermute | solution.py:420
  93.8 1.3 %collective-permute-start.16 = (bf16[160,256]{1,0:T(8,128)(2,1)S(1)}, bf16[160,256]{1,0:T(8,128)(2,1)S(1)}, u32[]{:S(2)}, u32[]{:S(2)}) collective-permute-start(bf16[160,256]{1,0:T(8,128)(2,1)S(1)} %get-tuple-element.58), channel_id=1, source_target_pairs={{0,28},{4,24},{8,20},{12,16},{16,12},{20,8},{24,4},{28,0},{1,29},{... | collective-permute-start | bytes 245768 | tf_op jit(solution)/shard_map/ppermute | solution.py:420
  95.0 3.9 %attend.5 = (bf16[160,256]{1,0:T(8,128)(2,1)S(1)}, bf16[160,256]{1,0:T(8,128)(2,1)S(1)}, bf16[160,256]{1,0:T(8,128)(2,1)S(1)}) custom-call(bf16[160,512]{1,0:T(8,128)(2,1)S(1)} %collective-permute-done.refs_1_.refs_0_, bf16[160,512]{1,0:T(8,128)(2,1)S(1)} %collective-permute-done.1.refs_2_.refs_1_, ...), custom_call_target="tpu_custom_call" | custom-call | flops 1258291200 | bytes 1310720 | tf_op jit(solution)/shard_map/attend/pallas_call | solution.py:333
  98.9 0.0 collective-permute-done.14.refs_5_
  98.9 1.6 %collective-permute-start.7 = (bf16[160,256]{1,0:T(8,128)(2,1)S(1)}, bf16[160,256]{1,0:T(8,128)(2,1)S(1)}, u32[]{:S(2)}, u32[]{:S(2)}) collective-permute-start(bf16[160,256]{1,0:T(8,128)(2,1)S(1)} %get-tuple-element.48), channel_id=1, source_target_pairs={{0,4},{4,0},{8,12},{12,8},{16,20},{20,16},{24,28},{28,24},{1,5},{5... | collective-permute-start | bytes 245768 | tf_op jit(solution)/shard_map/ppermute | solution.py:420
  100.5 0.4 collective-permute-done.16.refs_7_
  100.9 1.6 %collective-permute-start.9 = (bf16[160,256]{1,0:T(8,128)(2,1)S(1)}, bf16[160,256]{1,0:T(8,128)(2,1)S(1)}, u32[]{:S(2)}, u32[]{:S(2)}) collective-permute-start(bf16[160,256]{1,0:T(8,128)(2,1)S(1)} %get-tuple-element.50), channel_id=1, source_target_pairs={{0,12},{4,8},{8,4},{12,0},{16,28},{20,24},{24,20},{28,16},{1,13},{... | collective-permute-start | bytes 245768 | tf_op jit(solution)/shard_map/ppermute | solution.py:420
  102.5 0.3 spread.7
  102.8 0.8 score.1.refs_6_
  103.6 1.5 %attend.4.refs_0_ = bf16[160,256]{1,0:T(8,128)(2,1)S(1)} custom-call(bf16[160,512]{1,0:T(8,128)(2,1)S(1)} %get-tuple-element.38.refs_0_, bf16[2,1280,128]{2,1,0:T(8,128)(2,1)S(1)} %spread.4.refs_1_.refs_3_, bf16[2,1280,128]{2,1,0:T(8,128)(2,1)S(1)} %get-tuple-element.46.refs_2_.refs_4_, bf16[2,2560,128]{2,1,0:T(8,128)(2,1)S(1)} %get-tuple-element.47.refs_3_.refs_5_), custom_call_target="tpu_custom_call" | custom-call | flops 419430400 | bytes 1310720 | tf_op jit(solution)/shard_map/attend/pallas_call | solution.py:333
  105.1 3.4 %attend.7 = (bf16[160,256]{1,0:T(8,128)(2,1)S(1)}, bf16[160,256]{1,0:T(8,128)(2,1)S(1)}, bf16[160,256]{1,0:T(8,128)(2,1)S(1)}) custom-call(bf16[160,512]{1,0:T(8,128)(2,1)S(1)} %collective-permute-done.10.refs_1_.refs_0_, bf16[160,512]{1,0:T(8,128)(2,1)S(1)} %collective-permute-done.11.refs_2_.refs_1_, ...), custom_call_target="tpu_custom_call" | custom-call | flops 1258291200 | bytes 1310720 | tf_op jit(solution)/shard_map/attend/pallas_call | solution.py:333
  108.6 0.0 copy-start
  108.6 1.6 %collective-permute-start.17 = (bf16[160,256]{1,0:T(8,128)(2,1)S(1)}, bf16[160,256]{1,0:T(8,128)(2,1)S(1)}, u32[]{:S(2)}, u32[]{:S(2)}) collective-permute-start(bf16[160,256]{1,0:T(8,128)(2,1)S(1)} %get-tuple-element.61), channel_id=1, source_target_pairs={{0,4},{4,0},{8,12},{12,8},{16,20},{20,16},{24,28},{28,24},{1,5},{5... | collective-permute-start | bytes 245768 | tf_op jit(solution)/shard_map/ppermute | solution.py:420
  110.2 0.7 collective-permute-start.18
  110.9 1.4 %collective-permute-start.19 = (bf16[160,256]{1,0:T(8,128)(2,1)S(1)}, bf16[160,256]{1,0:T(8,128)(2,1)S(1)}, u32[]{:S(2)}, u32[]{:S(2)}) collective-permute-start(bf16[160,256]{1,0:T(8,128)(2,1)S(1)} %get-tuple-element.63), channel_id=1, source_target_pairs={{0,12},{4,8},{8,4},{12,0},{16,28},{20,24},{24,20},{28,16},{1,13},{... | collective-permute-start | bytes 245768 | tf_op jit(solution)/shard_map/ppermute | solution.py:420
  112.3 1.5 %attend.6.refs_4_ = bf16[160,256]{1,0:T(8,128)(2,1)S(1)} custom-call(bf16[160,512]{1,0:T(8,128)(2,1)S(1)} %get-tuple-element.51.refs_0_, bf16[2,1280,128]{2,1,0:T(8,128)(2,1)S(1)} %spread.6.refs_1_.refs_3_, bf16[2,1280,128]{2,1,0:T(8,128)(2,1)S(1)} %get-tuple-element.59.refs_2_.refs_4_, bf16[2,2560,128]{2,1,0:T(8,128)(2,1)S(1)} %get-tuple-element.60.refs_3_.refs_5_), custom_call_target="tpu_custom_call" | custom-call | flops 419430400 | bytes 1310720 | tf_op jit(solution)/shard_map/attend/pallas_call | solution.py:333
  113.9 0.8 project.3
  114.7 1.5 %collective-permute-done.19.refs_7_ = bf16[160,256]{1,0:T(8,128)(2,1)S(1)} collective-permute-done((bf16[160,256]{1,0:T(8,128)(2,1)S(1)}, bf16[160,256]{1,0:T(8,128)(2,1)S(1)}, u32[]{:S(2)}, u32[]{:S(2)}) %collective-permute-start.19) | collective-permute-done | bytes 81952 | tf_op jit(solution)/shard_map/ppermute | solution.py:420
  116.2 0.6 project.4
  116.9 1.2 %project.5 = bf16[160,2048]{1,0:T(8,128)(2,1)} custom-call(bf16[160,2048]{1,0:T(8,128)(2,1)S(1)} %get-tuple-element.67.refs_0_, bf16[2048,512]{1,0:T(8,128)(2,1)S(1)} %collective-permute-done.22.refs_1_, bf16[160,512]{1,0:T(8,128)(2,1)S(1)} %get-tuple-element.68.refs_2_, bf16[160,512]{1,0:T(8,128)(2,1)S(1)} %get-tuple-element.69.refs_3_, ...), custom_call_target="tpu_custom_call" | custom-call | flops 335544320 | bytes 4194304 | tf_op jit(solution)/shard_map/project/pallas_call | solution.py:406
  (14 shorter events, 0.0 us)
Async XLA Ops:
  0.0 48.8 %collective-permute-start.21 = (bf16[2048,512]{1,0:T(8,128)(2,1)}, bf16[2048,512]{1,0:T(8,128)(2,1)S(1)}, u32[]{:S(2)}, u32[]{:S(2)}) collective-permute-start(bf16[2048,512]{1,0:T(8,128)(2,1)} %refs_8_.1), channel_id=1, source_target_pairs={{0,2},{1,3},{2,0},{3,1},{4,6},{5,7},{6,4},{7,5},{8,10},{9,11},{10,... | collective-permute-start | bytes 6291464 | tf_op jit(solution)/shard_map/ppermute | solution.py:420
  3.0 110.9 %collective-permute-start.20 = (bf16[2048,512]{1,0:T(8,128)(2,1)}, bf16[2048,512]{1,0:T(8,128)(2,1)S(1)}, u32[]{:S(2)}, u32[]{:S(2)}) collective-permute-start(bf16[2048,512]{1,0:T(8,128)(2,1)} %refs_8_.1), channel_id=1, source_target_pairs={{0,1},{1,0},{2,3},{3,2},{4,5},{5,4},{6,7},{7,6},{8,9},{9,8},{10,11... | collective-permute-start | bytes 6291464 | tf_op jit(solution)/shard_map/ppermute | solution.py:420
  48.8 68.0 %collective-permute-start.22 = (bf16[2048,512]{1,0:T(8,128)(2,1)S(1)}, bf16[2048,512]{1,0:T(8,128)(2,1)S(1)}, u32[]{:S(2)}, u32[]{:S(2)}) collective-permute-start(bf16[2048,512]{1,0:T(8,128)(2,1)S(1)} %collective-permute-done.21.refs_7_.refs_10_), channel_id=1, source_target_pairs={{0,1},{1,0},{2,3},{3,2},{4,5},{5,4},{6,7},{7,6},{8,9},{9,8},{10,11... | collective-permute-start | bytes 6291464 | tf_op jit(solution)/shard_map/ppermute | solution.py:420
  52.3 8.0 %collective-permute-start.3 = (bf16[160,256]{1,0:T(8,128)(2,1)S(1)}, bf16[160,256]{1,0:T(8,128)(2,1)S(1)}, u32[]{:S(2)}, u32[]{:S(2)}) collective-permute-start(bf16[160,256]{1,0:T(8,128)(2,1)S(1)} %get-tuple-element.42), channel_id=1, source_target_pairs={{0,16},{4,20},{8,24},{12,28},{16,0},{20,4},{24,8},{28,12},{1,17},{... | collective-permute-start | bytes 245768 | tf_op jit(solution)/shard_map/ppermute | solution.py:420
  55.2 12.9 %collective-permute-start.4 = (bf16[160,256]{1,0:T(8,128)(2,1)S(1)}, bf16[160,256]{1,0:T(8,128)(2,1)S(1)}, u32[]{:S(2)}, u32[]{:S(2)}) collective-permute-start(bf16[160,256]{1,0:T(8,128)(2,1)S(1)} %get-tuple-element.43), channel_id=1, source_target_pairs={{0,20},{4,16},{8,28},{12,24},{16,4},{20,0},{24,12},{28,8},{1,21},{... | collective-permute-start | bytes 245768 | tf_op jit(solution)/shard_map/ppermute | solution.py:420
  56.5 12.1 %collective-permute-start.5 = (bf16[160,256]{1,0:T(8,128)(2,1)S(1)}, bf16[160,256]{1,0:T(8,128)(2,1)S(1)}, u32[]{:S(2)}, u32[]{:S(2)}) collective-permute-start(bf16[160,256]{1,0:T(8,128)(2,1)S(1)} %get-tuple-element.44), channel_id=1, source_target_pairs={{0,24},{4,28},{8,16},{12,20},{16,8},{20,12},{24,0},{28,4},{1,25},{... | collective-permute-start | bytes 245768 | tf_op jit(solution)/shard_map/ppermute | solution.py:420
  60.3 10.7 %collective-permute-start.6 = (bf16[160,256]{1,0:T(8,128)(2,1)S(1)}, bf16[160,256]{1,0:T(8,128)(2,1)S(1)}, u32[]{:S(2)}, u32[]{:S(2)}) collective-permute-start(bf16[160,256]{1,0:T(8,128)(2,1)S(1)} %get-tuple-element.45), channel_id=1, source_target_pairs={{0,28},{4,24},{8,20},{12,16},{16,12},{20,8},{24,4},{28,0},{1,29},{... | collective-permute-start | bytes 245768 | tf_op jit(solution)/shard_map/ppermute | solution.py:420
  68.1 6.9 %collective-permute-start = (bf16[160,512]{1,0:T(8,128)(2,1)S(1)}, bf16[160,512]{1,0:T(8,128)(2,1)S(1)}, u32[]{:S(2)}, u32[]{:S(2)}) collective-permute-start(bf16[160,512]{1,0:T(8,128)(2,1)S(1)} %get-tuple-element.39), channel_id=1, source_target_pairs={{0,4},{4,0},{8,12},{12,8},{16,20},{20,16},{24,28},{28,24},{1,5},{5... | collective-permute-start | bytes 491528 | tf_op jit(solution)/shard_map/ppermute | solution.py:420
  68.6 7.1 %collective-permute-start.1 = (bf16[160,512]{1,0:T(8,128)(2,1)S(1)}, bf16[160,512]{1,0:T(8,128)(2,1)S(1)}, u32[]{:S(2)}, u32[]{:S(2)}) collective-permute-start(bf16[160,512]{1,0:T(8,128)(2,1)S(1)} %get-tuple-element.40), channel_id=1, source_target_pairs={{0,8},{4,12},{8,0},{12,4},{16,24},{20,28},{24,16},{28,20},{1,9},{5... | collective-permute-start | bytes 491528 | tf_op jit(solution)/shard_map/ppermute | solution.py:420
  71.0 9.0 %collective-permute-start.2 = (bf16[160,512]{1,0:T(8,128)(2,1)S(1)}, bf16[160,512]{1,0:T(8,128)(2,1)S(1)}, u32[]{:S(2)}, u32[]{:S(2)}) collective-permute-start(bf16[160,512]{1,0:T(8,128)(2,1)S(1)} %get-tuple-element.41), channel_id=1, source_target_pairs={{0,12},{4,8},{8,4},{12,0},{16,28},{20,24},{24,20},{28,16},{1,13},{... | collective-permute-start | bytes 491528 | tf_op jit(solution)/shard_map/ppermute | solution.py:420
  75.0 8.2 %collective-permute-start.10 = (bf16[160,512]{1,0:T(8,128)(2,1)S(1)}, bf16[160,512]{1,0:T(8,128)(2,1)S(1)}, u32[]{:S(2)}, u32[]{:S(2)}) collective-permute-start(bf16[160,512]{1,0:T(8,128)(2,1)S(1)} %get-tuple-element.52), channel_id=1, source_target_pairs={{0,4},{4,0},{8,12},{12,8},{16,20},{20,16},{24,28},{28,24},{1,5},{5... | collective-permute-start | bytes 491528 | tf_op jit(solution)/shard_map/ppermute | solution.py:420
  75.7 9.0 %collective-permute-start.11 = (bf16[160,512]{1,0:T(8,128)(2,1)S(1)}, bf16[160,512]{1,0:T(8,128)(2,1)S(1)}, u32[]{:S(2)}, u32[]{:S(2)}) collective-permute-start(bf16[160,512]{1,0:T(8,128)(2,1)S(1)} %get-tuple-element.53), channel_id=1, source_target_pairs={{0,8},{4,12},{8,0},{12,4},{16,24},{20,28},{24,16},{28,20},{1,9},{5... | collective-permute-start | bytes 491528 | tf_op jit(solution)/shard_map/ppermute | solution.py:420
  79.9 7.0 %collective-permute-start.12 = (bf16[160,512]{1,0:T(8,128)(2,1)S(1)}, bf16[160,512]{1,0:T(8,128)(2,1)S(1)}, u32[]{:S(2)}, u32[]{:S(2)}) collective-permute-start(bf16[160,512]{1,0:T(8,128)(2,1)S(1)} %get-tuple-element.54), channel_id=1, source_target_pairs={{0,12},{4,8},{8,4},{12,0},{16,28},{20,24},{24,20},{28,16},{1,13},{... | collective-permute-start | bytes 491528 | tf_op jit(solution)/shard_map/ppermute | solution.py:420
  83.2 10.6 %collective-permute-start.13 = (bf16[160,256]{1,0:T(8,128)(2,1)S(1)}, bf16[160,256]{1,0:T(8,128)(2,1)S(1)}, u32[]{:S(2)}, u32[]{:S(2)}) collective-permute-start(bf16[160,256]{1,0:T(8,128)(2,1)S(1)} %get-tuple-element.55), channel_id=1, source_target_pairs={{0,16},{4,20},{8,24},{12,28},{16,0},{20,4},{24,8},{28,12},{1,17},{... | collective-permute-start | bytes 245768 | tf_op jit(solution)/shard_map/ppermute | solution.py:420
  84.8 14.2 %collective-permute-start.14 = (bf16[160,256]{1,0:T(8,128)(2,1)S(1)}, bf16[160,256]{1,0:T(8,128)(2,1)S(1)}, u32[]{:S(2)}, u32[]{:S(2)}) collective-permute-start(bf16[160,256]{1,0:T(8,128)(2,1)S(1)} %get-tuple-element.56), channel_id=1, source_target_pairs={{0,20},{4,16},{8,28},{12,24},{16,4},{20,0},{24,12},{28,8},{1,21},{... | collective-permute-start | bytes 245768 | tf_op jit(solution)/shard_map/ppermute | solution.py:420
  87.0 13.6 %collective-permute-start.15 = (bf16[160,256]{1,0:T(8,128)(2,1)S(1)}, bf16[160,256]{1,0:T(8,128)(2,1)S(1)}, u32[]{:S(2)}, u32[]{:S(2)}) collective-permute-start(bf16[160,256]{1,0:T(8,128)(2,1)S(1)} %get-tuple-element.57), channel_id=1, source_target_pairs={{0,24},{4,28},{8,16},{12,20},{16,8},{20,12},{24,0},{28,4},{1,25},{... | collective-permute-start | bytes 245768 | tf_op jit(solution)/shard_map/ppermute | solution.py:420
  93.8 7.1 %collective-permute-start.16 = (bf16[160,256]{1,0:T(8,128)(2,1)S(1)}, bf16[160,256]{1,0:T(8,128)(2,1)S(1)}, u32[]{:S(2)}, u32[]{:S(2)}) collective-permute-start(bf16[160,256]{1,0:T(8,128)(2,1)S(1)} %get-tuple-element.58), channel_id=1, source_target_pairs={{0,28},{4,24},{8,20},{12,16},{16,12},{20,8},{24,4},{28,0},{1,29},{... | collective-permute-start | bytes 245768 | tf_op jit(solution)/shard_map/ppermute | solution.py:420
  98.9 9.6 %collective-permute-start.7 = (bf16[160,256]{1,0:T(8,128)(2,1)S(1)}, bf16[160,256]{1,0:T(8,128)(2,1)S(1)}, u32[]{:S(2)}, u32[]{:S(2)}) collective-permute-start(bf16[160,256]{1,0:T(8,128)(2,1)S(1)} %get-tuple-element.48), channel_id=1, source_target_pairs={{0,4},{4,0},{8,12},{12,8},{16,20},{20,16},{24,28},{28,24},{1,5},{5... | collective-permute-start | bytes 245768 | tf_op jit(solution)/shard_map/ppermute | solution.py:420
  100.5 9.6 %collective-permute-start.8 = (bf16[160,256]{1,0:T(8,128)(2,1)S(1)}, bf16[160,256]{1,0:T(8,128)(2,1)S(1)}, u32[]{:S(2)}, u32[]{:S(2)}) collective-permute-start(bf16[160,256]{1,0:T(8,128)(2,1)S(1)} %get-tuple-element.49), channel_id=1, source_target_pairs={{0,8},{4,12},{8,0},{12,4},{16,24},{20,28},{24,16},{28,20},{1,9},{5... | collective-permute-start | bytes 245768 | tf_op jit(solution)/shard_map/ppermute | solution.py:420
  100.9 10.0 %collective-permute-start.9 = (bf16[160,256]{1,0:T(8,128)(2,1)S(1)}, bf16[160,256]{1,0:T(8,128)(2,1)S(1)}, u32[]{:S(2)}, u32[]{:S(2)}) collective-permute-start(bf16[160,256]{1,0:T(8,128)(2,1)S(1)} %get-tuple-element.50), channel_id=1, source_target_pairs={{0,12},{4,8},{8,4},{12,0},{16,28},{20,24},{24,20},{28,16},{1,13},{... | collective-permute-start | bytes 245768 | tf_op jit(solution)/shard_map/ppermute | solution.py:420
  108.6 5.3 %copy-start = (bf16[2048,512]{1,0:T(8,128)(2,1)S(1)}, bf16[2048,512]{1,0:T(8,128)(2,1)}, u32[]{:S(2)}) copy-start(bf16[2048,512]{1,0:T(8,128)(2,1)} %refs_8_.1) | copy-start | bytes 6291460
  108.6 6.1 %collective-permute-start.17 = (bf16[160,256]{1,0:T(8,128)(2,1)S(1)}, bf16[160,256]{1,0:T(8,128)(2,1)S(1)}, u32[]{:S(2)}, u32[]{:S(2)}) collective-permute-start(bf16[160,256]{1,0:T(8,128)(2,1)S(1)} %get-tuple-element.61), channel_id=1, source_target_pairs={{0,4},{4,0},{8,12},{12,8},{16,20},{20,16},{24,28},{28,24},{1,5},{5... | collective-permute-start | bytes 245768 | tf_op jit(solution)/shard_map/ppermute | solution.py:420
  110.2 4.6 %collective-permute-start.18 = (bf16[160,256]{1,0:T(8,128)(2,1)S(1)}, bf16[160,256]{1,0:T(8,128)(2,1)S(1)}, u32[]{:S(2)}, u32[]{:S(2)}) collective-permute-start(bf16[160,256]{1,0:T(8,128)(2,1)S(1)} %get-tuple-element.62), channel_id=1, source_target_pairs={{0,8},{4,12},{8,0},{12,4},{16,24},{20,28},{24,16},{28,20},{1,9},{5... | collective-permute-start | bytes 245768 | tf_op jit(solution)/shard_map/ppermute | solution.py:420
  110.9 5.3 %collective-permute-start.19 = (bf16[160,256]{1,0:T(8,128)(2,1)S(1)}, bf16[160,256]{1,0:T(8,128)(2,1)S(1)}, u32[]{:S(2)}, u32[]{:S(2)}) collective-permute-start(bf16[160,256]{1,0:T(8,128)(2,1)S(1)} %get-tuple-element.63), channel_id=1, source_target_pairs={{0,12},{4,8},{8,4},{12,0},{16,28},{20,24},{24,20},{28,16},{1,13},{... | collective-permute-start | bytes 245768 | tf_op jit(solution)/shard_map/ppermute | solution.py:420

commit v7 on v6

--- a/solution.py
+++ b/solution.py
@@ -383,20 +383,20 @@
 
 def third_kernel(groups, *refs):
     whole_ref, source, made, (out_ref, last, sems) = refs[0], refs[1], refs[2:5], refs[5:]
-    width = source.shape[1]
-    half = width // 2
-
-    def leave(i, ready, shift, n):
-        column = pl.ds(pl.multiple_of((lax.axis_index("dp") ^ i) * width + shift, half), ready.shape[1])
-        copy = pltpu.make_async_copy(ready, out_ref.at[:, column], sems.at[n])
+    width, tok = source.shape[1], whole_ref.shape[0]
+    half = tok // 2
+    column = lambda i: pl.ds(pl.multiple_of((lax.axis_index("dp") ^ i) * width, width), width)
+
+    def leave(ready, rows, lanes, n):
+        copy = pltpu.make_async_copy(ready, out_ref.at[rows, lanes], sems.at[n])
         copy.start()
         return copy
 
-    leaving = [leave(i, ready, 0, i) for i, ready in enumerate(made)]
+    leaving = [leave(ready, slice(0, tok), column(i), i) for i, ready in enumerate(made)]
+    total = jnp.dot(whole_ref[...], source[...], preferred_element_type=jnp.float32).astype(jnp.bfloat16)
     for n in range(2):
-        lanes = slice(n * half, (n + 1) * half)
-        last[n] = jnp.dot(whole_ref[...], source[:, lanes], preferred_element_type=jnp.float32).astype(jnp.bfloat16)
-        leaving.append(leave(3, last.at[n], n * half, 3 + n))
+        last[n] = total[n * half : (n + 1) * half]
+        leaving.append(leave(last.at[n], slice(n * half, (n + 1) * half), column(3), 3 + n))
     for copy in leaving:
         copy.wait()
 
@@ -464,7 +464,7 @@
         groups,
         [whole, corner, *made],
         jax.ShapeDtypeStruct((tok, 4 * width), jnp.bfloat16),
-        [pltpu.VMEM((2, tok, width // 2), jnp.bfloat16), pltpu.SemaphoreType.DMA((5,))],
+        [pltpu.VMEM((2, tok // 2, width), jnp.bfloat16), pltpu.SemaphoreType.DMA((5,))],
         flops,
     )
     return mixed[None]

time: 118 us -> 118 us (level)
  no operation moved by 1% of the time
where the time goes in v7:
time: 118 us
  waiting for transfers between devices  61.6 us (52%)
  starting transfers between devices  38.2 us (32%)
  Pallas kernels  17.3 us (15%)
    ppermute x23, waiting for transfers between devices, exchanged(): return lax.ppermute(block, axis, [(i, i ^ flip) for i in range(count)])  61.6 us
    ppermute x23, starting transfers between devices, exchanged(): return lax.ppermute(block, axis, [(i, i ^ flip) for i in range(count)])  38.2 us
    pallas_call x4, Pallas kernels, attend(): pl.pallas_call(functools.partial(attend_kernel, count, len(given)), in_sp...  10.4 us
    pallas_call x1, Pallas kernels, turn_and_pack(): pl.pallas_call(functools.partial(turn_kernel, groups, chunks), in_specs=[...  2.68 us
    pallas_call x3, Pallas kernels, project_call(): pl.pallas_call(functools.partial(kernel, groups), in_specs=in_vmem(len(in...  2.68 us
  transfers between devices with their start and end apart: 23, of which 10 were waited for; matrix products, arithmetic and copies ran while one was open for 1% of the time, Pallas kernels for 14%

profile of v7, /device:TPU:0, one launch (start us, length us, event | category | flops | bytes accessed | tf_op | source)
XLA Modules:
  0.0 118.3 jit_solution(4314625089539022036)
XLA Ops:
  0.0 3.0 %collective-permute-start.21 = (bf16[2048,512]{1,0:T(8,128)(2,1)}, bf16[2048,512]{1,0:T(8,128)(2,1)S(1)}, u32[]{:S(2)}, u32[]{:S(2)}) collective-permute-start(bf16[2048,512]{1,0:T(8,128)(2,1)} %refs_8_.1), channel_id=1, source_target_pairs={{0,2},{1,3},{2,0},{3,1},{4,6},{5,7},{6,4},{7,5},{8,10},{9,11},{10,... | collective-permute-start | bytes 6291464 | tf_op jit(solution)/shard_map/ppermute | solution.py:420
  3.0 45.8 %collective-permute-done.21.refs_7_.refs_10_ = bf16[2048,512]{1,0:T(8,128)(2,1)S(1)} collective-permute-done((bf16[2048,512]{1,0:T(8,128)(2,1)}, bf16[2048,512]{1,0:T(8,128)(2,1)S(1)}, u32[]{:S(2)}, u32[]{:S(2)}) %collective-permute-start.21) | collective-permute-done | bytes 2097184 | tf_op jit(solution)/shard_map/ppermute | solution.py:420
  48.8 0.8 maximum_bitcast_fusion.refs_3_
  49.6 2.7 %turn.1 = (bf16[160,512]{1,0:T(8,128)(2,1)S(1)}, bf16[160,512]{1,0:T(8,128)(2,1)S(1)}, bf16[160,512]{1,0:T(8,128)(2,1)S(1)}, bf16[160,512]{1,0:T(8,128)(2,1)S(1)...) custom-call(bf16[160,2048]{1,0:T(8,128)(2,1)} %bitcast.12, ...), custom_call_target="tpu_custom_call" | custom-call | flops 19660800 | bytes 3932160 | tf_op jit(solution)/shard_map/turn/pallas_call | solution.py:214
  52.3 2.9 %collective-permute-start.3 = (bf16[160,256]{1,0:T(8,128)(2,1)S(1)}, bf16[160,256]{1,0:T(8,128)(2,1)S(1)}, u32[]{:S(2)}, u32[]{:S(2)}) collective-permute-start(bf16[160,256]{1,0:T(8,128)(2,1)S(1)} %get-tuple-element.42), channel_id=1, source_target_pairs={{0,16},{4,20},{8,24},{12,28},{16,0},{20,4},{24,8},{28,12},{1,17},{... | collective-permute-start | bytes 245768 | tf_op jit(solution)/shard_map/ppermute | solution.py:420
  55.2 1.3 %collective-permute-start.4 = (bf16[160,256]{1,0:T(8,128)(2,1)S(1)}, bf16[160,256]{1,0:T(8,128)(2,1)S(1)}, u32[]{:S(2)}, u32[]{:S(2)}) collective-permute-start(bf16[160,256]{1,0:T(8,128)(2,1)S(1)} %get-tuple-element.43), channel_id=1, source_target_pairs={{0,20},{4,16},{8,28},{12,24},{16,4},{20,0},{24,12},{28,8},{1,21},{... | collective-permute-start | bytes 245768 | tf_op jit(solution)/shard_map/ppermute | solution.py:420
  56.5 3.6 %collective-permute-start.5 = (bf16[160,256]{1,0:T(8,128)(2,1)S(1)}, bf16[160,256]{1,0:T(8,128)(2,1)S(1)}, u32[]{:S(2)}, u32[]{:S(2)}) collective-permute-start(bf16[160,256]{1,0:T(8,128)(2,1)S(1)} %get-tuple-element.44), channel_id=1, source_target_pairs={{0,24},{4,28},{8,16},{12,20},{16,8},{20,12},{24,0},{28,4},{1,25},{... | collective-permute-start | bytes 245768 | tf_op jit(solution)/shard_map/ppermute | solution.py:420
  60.1 0.2 collective-permute-done.3.refs_4_
  60.3 7.8 %collective-permute-start.6 = (bf16[160,256]{1,0:T(8,128)(2,1)S(1)}, bf16[160,256]{1,0:T(8,128)(2,1)S(1)}, u32[]{:S(2)}, u32[]{:S(2)}) collective-permute-start(bf16[160,256]{1,0:T(8,128)(2,1)S(1)} %get-tuple-element.45), channel_id=1, source_target_pairs={{0,28},{4,24},{8,20},{12,16},{16,12},{20,8},{24,4},{28,0},{1,29},{... | collective-permute-start | bytes 245768 | tf_op jit(solution)/shard_map/ppermute | solution.py:420
  68.1 0.5 collective-permute-start
  68.6 0.0 collective-permute-done.5.refs_6_
  68.6 0.0 collective-permute-start.1
  68.6 2.3 %collective-permute-done.6.refs_7_ = bf16[160,256]{1,0:T(8,128)(2,1)S(1)} collective-permute-done((bf16[160,256]{1,0:T(8,128)(2,1)S(1)}, bf16[160,256]{1,0:T(8,128)(2,1)S(1)}, u32[]{:S(2)}, u32[]{:S(2)}) %collective-permute-start.6) | collective-permute-done | bytes 81952 | tf_op jit(solution)/shard_map/ppermute | solution.py:420
  71.0 1.4 %collective-permute-start.2 = (bf16[160,512]{1,0:T(8,128)(2,1)S(1)}, bf16[160,512]{1,0:T(8,128)(2,1)S(1)}, u32[]{:S(2)}, u32[]{:S(2)}) collective-permute-start(bf16[160,512]{1,0:T(8,128)(2,1)S(1)} %get-tuple-element.41), channel_id=1, source_target_pairs={{0,12},{4,8},{8,4},{12,0},{16,28},{20,24},{24,20},{28,16},{1,13},{... | collective-permute-start | bytes 491528 | tf_op jit(solution)/shard_map/ppermute | solution.py:420
  72.3 2.7 %collective-permute-done.refs_1_.refs_0_ = bf16[160,512]{1,0:T(8,128)(2,1)S(1)} collective-permute-done((bf16[160,512]{1,0:T(8,128)(2,1)S(1)}, bf16[160,512]{1,0:T(8,128)(2,1)S(1)}, u32[]{:S(2)}, u32[]{:S(2)}) %collective-permute-start) | collective-permute-done | bytes 163872 | tf_op jit(solution)/shard_map/ppermute | solution.py:420
  75.0 0.4 collective-permute-start.10
  75.4 0.3 collective-permute-done.1.refs_2_.refs_1_
  75.7 1.2 %collective-permute-start.11 = (bf16[160,512]{1,0:T(8,128)(2,1)S(1)}, bf16[160,512]{1,0:T(8,128)(2,1)S(1)}, u32[]{:S(2)}, u32[]{:S(2)}) collective-permute-start(bf16[160,512]{1,0:T(8,128)(2,1)S(1)} %get-tuple-element.53), channel_id=1, source_target_pairs={{0,8},{4,12},{8,0},{12,4},{16,24},{20,28},{24,16},{28,20},{1,9},{5... | collective-permute-start | bytes 491528 | tf_op jit(solution)/shard_map/ppermute | solution.py:420
  77.0 3.0 %collective-permute-done.2.refs_3_.refs_2_ = bf16[160,512]{1,0:T(8,128)(2,1)S(1)} collective-permute-done((bf16[160,512]{1,0:T(8,128)(2,1)S(1)}, bf16[160,512]{1,0:T(8,128)(2,1)S(1)}, u32[]{:S(2)}, u32[]{:S(2)}) %collective-permute-start.2) | collective-permute-done | bytes 163872 | tf_op jit(solution)/shard_map/ppermute | solution.py:420
  79.9 1.5 %collective-permute-start.12 = (bf16[160,512]{1,0:T(8,128)(2,1)S(1)}, bf16[160,512]{1,0:T(8,128)(2,1)S(1)}, u32[]{:S(2)}, u32[]{:S(2)}) collective-permute-start(bf16[160,512]{1,0:T(8,128)(2,1)S(1)} %get-tuple-element.54), channel_id=1, source_target_pairs={{0,12},{4,8},{8,4},{12,0},{16,28},{20,24},{24,20},{28,16},{1,13},{... | collective-permute-start | bytes 491528 | tf_op jit(solution)/shard_map/ppermute | solution.py:420
  81.4 1.8 %collective-permute-done.10.refs_1_.refs_0_ = bf16[160,512]{1,0:T(8,128)(2,1)S(1)} collective-permute-done((bf16[160,512]{1,0:T(8,128)(2,1)S(1)}, bf16[160,512]{1,0:T(8,128)(2,1)S(1)}, u32[]{:S(2)}, u32[]{:S(2)}) %collective-permute-start.10) | collective-permute-done | bytes 163872 | tf_op jit(solution)/shard_map/ppermute | solution.py:420
  83.2 1.2 collective-permute-start.13
  84.3 0.1 spread.4.refs_1_.refs_3_
  84.5 0.3 spread.5
  84.8 2.2 %collective-permute-start.14 = (bf16[160,256]{1,0:T(8,128)(2,1)S(1)}, bf16[160,256]{1,0:T(8,128)(2,1)S(1)}, u32[]{:S(2)}, u32[]{:S(2)}) collective-permute-start(bf16[160,256]{1,0:T(8,128)(2,1)S(1)} %get-tuple-element.56), channel_id=1, source_target_pairs={{0,20},{4,16},{8,28},{12,24},{16,4},{20,0},{24,12},{28,8},{1,21},{... | collective-permute-start | bytes 245768 | tf_op jit(solution)/shard_map/ppermute | solution.py:420
  87.0 0.0 collective-permute-done.12.refs_3_.refs_2_
  87.0 3.0 %collective-permute-start.15 = (bf16[160,256]{1,0:T(8,128)(2,1)S(1)}, bf16[160,256]{1,0:T(8,128)(2,1)S(1)}, u32[]{:S(2)}, u32[]{:S(2)}) collective-permute-start(bf16[160,256]{1,0:T(8,128)(2,1)S(1)} %get-tuple-element.57), channel_id=1, source_target_pairs={{0,24},{4,28},{8,16},{12,20},{16,8},{20,12},{24,0},{28,4},{1,25},{... | collective-permute-start | bytes 245768 | tf_op jit(solution)/shard_map/ppermute | solution.py:420
  90.0 0.1 spread.6.refs_1_.refs_3_
  90.1 3.7 %collective-permute-done.13.refs_4_ = bf16[160,256]{1,0:T(8,128)(2,1)S(1)} collective-permute-done((bf16[160,256]{1,0:T(8,128)(2,1)S(1)}, bf16[160,256]{1,0:T(8,128)(2,1)S(1)}, u32[]{:S(2)}, u32[]{:S(2)}) %collective-permute-start.13) | collective-permute-done | bytes 81952 | tf_op jit(solution)/shard_map/ppermute | solution.py:420
  93.8 1.3 %collective-permute-start.16 = (bf16[160,256]{1,0:T(8,128)(2,1)S(1)}, bf16[160,256]{1,0:T(8,128)(2,1)S(1)}, u32[]{:S(2)}, u32[]{:S(2)}) collective-permute-start(bf16[160,256]{1,0:T(8,128)(2,1)S(1)} %get-tuple-element.58), channel_id=1, source_target_pairs={{0,28},{4,24},{8,20},{12,16},{16,12},{20,8},{24,4},{28,0},{1,29},{... | collective-permute-start | bytes 245768 | tf_op jit(solution)/shard_map/ppermute | solution.py:420
  95.0 3.9 %attend.5 = (bf16[160,256]{1,0:T(8,128)(2,1)S(1)}, bf16[160,256]{1,0:T(8,128)(2,1)S(1)}, bf16[160,256]{1,0:T(8,128)(2,1)S(1)}) custom-call(bf16[160,512]{1,0:T(8,128)(2,1)S(1)} %collective-permute-done.refs_1_.refs_0_, bf16[160,512]{1,0:T(8,128)(2,1)S(1)} %collective-permute-done.1.refs_2_.refs_1_, ...), custom_call_target="tpu_custom_call" | custom-call | flops 1258291200 | bytes 1310720 | tf_op jit(solution)/shard_map/attend/pallas_call | solution.py:333
  98.9 0.0 collective-permute-done.14.refs_5_
  98.9 1.6 %collective-permute-start.7 = (bf16[160,256]{1,0:T(8,128)(2,1)S(1)}, bf16[160,256]{1,0:T(8,128)(2,1)S(1)}, u32[]{:S(2)}, u32[]{:S(2)}) collective-permute-start(bf16[160,256]{1,0:T(8,128)(2,1)S(1)} %get-tuple-element.48), channel_id=1, source_target_pairs={{0,4},{4,0},{8,12},{12,8},{16,20},{20,16},{24,28},{28,24},{1,5},{5... | collective-permute-start | bytes 245768 | tf_op jit(solution)/shard_map/ppermute | solution.py:420
  100.5 0.4 collective-permute-done.16.refs_7_
  100.9 1.6 %collective-permute-start.9 = (bf16[160,256]{1,0:T(8,128)(2,1)S(1)}, bf16[160,256]{1,0:T(8,128)(2,1)S(1)}, u32[]{:S(2)}, u32[]{:S(2)}) collective-permute-start(bf16[160,256]{1,0:T(8,128)(2,1)S(1)} %get-tuple-element.50), channel_id=1, source_target_pairs={{0,12},{4,8},{8,4},{12,0},{16,28},{20,24},{24,20},{28,16},{1,13},{... | collective-permute-start | bytes 245768 | tf_op jit(solution)/shard_map/ppermute | solution.py:420
  102.5 0.3 spread.7
  102.8 0.8 score.1.refs_6_
  103.6 1.5 %attend.4.refs_0_ = bf16[160,256]{1,0:T(8,128)(2,1)S(1)} custom-call(bf16[160,512]{1,0:T(8,128)(2,1)S(1)} %get-tuple-element.38.refs_0_, bf16[2,1280,128]{2,1,0:T(8,128)(2,1)S(1)} %spread.4.refs_1_.refs_3_, bf16[2,1280,128]{2,1,0:T(8,128)(2,1)S(1)} %get-tuple-element.46.refs_2_.refs_4_, bf16[2,2560,128]{2,1,0:T(8,128)(2,1)S(1)} %get-tuple-element.47.refs_3_.refs_5_), custom_call_target="tpu_custom_call" | custom-call | flops 419430400 | bytes 1310720 | tf_op jit(solution)/shard_map/attend/pallas_call | solution.py:333
  105.1 3.4 %attend.7 = (bf16[160,256]{1,0:T(8,128)(2,1)S(1)}, bf16[160,256]{1,0:T(8,128)(2,1)S(1)}, bf16[160,256]{1,0:T(8,128)(2,1)S(1)}) custom-call(bf16[160,512]{1,0:T(8,128)(2,1)S(1)} %collective-permute-done.10.refs_1_.refs_0_, bf16[160,512]{1,0:T(8,128)(2,1)S(1)} %collective-permute-done.11.refs_2_.refs_1_, ...), custom_call_target="tpu_custom_call" | custom-call | flops 1258291200 | bytes 1310720 | tf_op jit(solution)/shard_map/attend/pallas_call | solution.py:333
  108.6 0.0 copy-start
  108.6 1.6 %collective-permute-start.17 = (bf16[160,256]{1,0:T(8,128)(2,1)S(1)}, bf16[160,256]{1,0:T(8,128)(2,1)S(1)}, u32[]{:S(2)}, u32[]{:S(2)}) collective-permute-start(bf16[160,256]{1,0:T(8,128)(2,1)S(1)} %get-tuple-element.61), channel_id=1, source_target_pairs={{0,4},{4,0},{8,12},{12,8},{16,20},{20,16},{24,28},{28,24},{1,5},{5... | collective-permute-start | bytes 245768 | tf_op jit(solution)/shard_map/ppermute | solution.py:420
  110.2 0.7 collective-permute-start.18
  110.9 1.4 %collective-permute-start.19 = (bf16[160,256]{1,0:T(8,128)(2,1)S(1)}, bf16[160,256]{1,0:T(8,128)(2,1)S(1)}, u32[]{:S(2)}, u32[]{:S(2)}) collective-permute-start(bf16[160,256]{1,0:T(8,128)(2,1)S(1)} %get-tuple-element.63), channel_id=1, source_target_pairs={{0,12},{4,8},{8,4},{12,0},{16,28},{20,24},{24,20},{28,16},{1,13},{... | collective-permute-start | bytes 245768 | tf_op jit(solution)/shard_map/ppermute | solution.py:420
  112.3 1.5 %attend.6.refs_4_ = bf16[160,256]{1,0:T(8,128)(2,1)S(1)} custom-call(bf16[160,512]{1,0:T(8,128)(2,1)S(1)} %get-tuple-element.51.refs_0_, bf16[2,1280,128]{2,1,0:T(8,128)(2,1)S(1)} %spread.6.refs_1_.refs_3_, bf16[2,1280,128]{2,1,0:T(8,128)(2,1)S(1)} %get-tuple-element.59.refs_2_.refs_4_, bf16[2,2560,128]{2,1,0:T(8,128)(2,1)S(1)} %get-tuple-element.60.refs_3_.refs_5_), custom_call_target="tpu_custom_call" | custom-call | flops 419430400 | bytes 1310720 | tf_op jit(solution)/shard_map/attend/pallas_call | solution.py:333
  113.9 0.8 project.3
  114.7 1.5 %collective-permute-done.19.refs_7_ = bf16[160,256]{1,0:T(8,128)(2,1)S(1)} collective-permute-done((bf16[160,256]{1,0:T(8,128)(2,1)S(1)}, bf16[160,256]{1,0:T(8,128)(2,1)S(1)}, u32[]{:S(2)}, u32[]{:S(2)}) %collective-permute-start.19) | collective-permute-done | bytes 81952 | tf_op jit(solution)/shard_map/ppermute | solution.py:420
  116.2 0.6 project.4
  116.9 1.2 %project.5 = bf16[160,2048]{1,0:T(8,128)(2,1)} custom-call(bf16[160,2048]{1,0:T(8,128)(2,1)S(1)} %get-tuple-element.67.refs_0_, bf16[2048,512]{1,0:T(8,128)(2,1)S(1)} %collective-permute-done.22.refs_1_, bf16[160,512]{1,0:T(8,128)(2,1)S(1)} %get-tuple-element.68.refs_2_, bf16[160,512]{1,0:T(8,128)(2,1)S(1)} %get-tuple-element.69.refs_3_, ...), custom_call_target="tpu_custom_call" | custom-call | flops 335544320 | bytes 4194304 | tf_op jit(solution)/shard_map/project/pallas_call | solution.py:406
  (14 shorter events, 0.0 us)
Async XLA Ops:
  0.0 48.8 %collective-permute-start.21 = (bf16[2048,512]{1,0:T(8,128)(2,1)}, bf16[2048,512]{1,0:T(8,128)(2,1)S(1)}, u32[]{:S(2)}, u32[]{:S(2)}) collective-permute-start(bf16[2048,512]{1,0:T(8,128)(2,1)} %refs_8_.1), channel_id=1, source_target_pairs={{0,2},{1,3},{2,0},{3,1},{4,6},{5,7},{6,4},{7,5},{8,10},{9,11},{10,... | collective-permute-start | bytes 6291464 | tf_op jit(solution)/shard_map/ppermute | solution.py:420
  3.0 110.9 %collective-permute-start.20 = (bf16[2048,512]{1,0:T(8,128)(2,1)}, bf16[2048,512]{1,0:T(8,128)(2,1)S(1)}, u32[]{:S(2)}, u32[]{:S(2)}) collective-permute-start(bf16[2048,512]{1,0:T(8,128)(2,1)} %refs_8_.1), channel_id=1, source_target_pairs={{0,1},{1,0},{2,3},{3,2},{4,5},{5,4},{6,7},{7,6},{8,9},{9,8},{10,11... | collective-permute-start | bytes 6291464 | tf_op jit(solution)/shard_map/ppermute | solution.py:420
  48.8 68.0 %collective-permute-start.22 = (bf16[2048,512]{1,0:T(8,128)(2,1)S(1)}, bf16[2048,512]{1,0:T(8,128)(2,1)S(1)}, u32[]{:S(2)}, u32[]{:S(2)}) collective-permute-start(bf16[2048,512]{1,0:T(8,128)(2,1)S(1)} %collective-permute-done.21.refs_7_.refs_10_), channel_id=1, source_target_pairs={{0,1},{1,0},{2,3},{3,2},{4,5},{5,4},{6,7},{7,6},{8,9},{9,8},{10,11... | collective-permute-start | bytes 6291464 | tf_op jit(solution)/shard_map/ppermute | solution.py:420
  52.3 8.0 %collective-permute-start.3 = (bf16[160,256]{1,0:T(8,128)(2,1)S(1)}, bf16[160,256]{1,0:T(8,128)(2,1)S(1)}, u32[]{:S(2)}, u32[]{:S(2)}) collective-permute-start(bf16[160,256]{1,0:T(8,128)(2,1)S(1)} %get-tuple-element.42), channel_id=1, source_target_pairs={{0,16},{4,20},{8,24},{12,28},{16,0},{20,4},{24,8},{28,12},{1,17},{... | collective-permute-start | bytes 245768 | tf_op jit(solution)/shard_map/ppermute | solution.py:420
  55.2 12.9 %collective-permute-start.4 = (bf16[160,256]{1,0:T(8,128)(2,1)S(1)}, bf16[160,256]{1,0:T(8,128)(2,1)S(1)}, u32[]{:S(2)}, u32[]{:S(2)}) collective-permute-start(bf16[160,256]{1,0:T(8,128)(2,1)S(1)} %get-tuple-element.43), channel_id=1, source_target_pairs={{0,20},{4,16},{8,28},{12,24},{16,4},{20,0},{24,12},{28,8},{1,21},{... | collective-permute-start | bytes 245768 | tf_op jit(solution)/shard_map/ppermute | solution.py:420
  56.5 12.1 %collective-permute-start.5 = (bf16[160,256]{1,0:T(8,128)(2,1)S(1)}, bf16[160,256]{1,0:T(8,128)(2,1)S(1)}, u32[]{:S(2)}, u32[]{:S(2)}) collective-permute-start(bf16[160,256]{1,0:T(8,128)(2,1)S(1)} %get-tuple-element.44), channel_id=1, source_target_pairs={{0,24},{4,28},{8,16},{12,20},{16,8},{20,12},{24,0},{28,4},{1,25},{... | collective-permute-start | bytes 245768 | tf_op jit(solution)/shard_map/ppermute | solution.py:420
  60.3 10.7 %collective-permute-start.6 = (bf16[160,256]{1,0:T(8,128)(2,1)S(1)}, bf16[160,256]{1,0:T(8,128)(2,1)S(1)}, u32[]{:S(2)}, u32[]{:S(2)}) collective-permute-start(bf16[160,256]{1,0:T(8,128)(2,1)S(1)} %get-tuple-element.45), channel_id=1, source_target_pairs={{0,28},{4,24},{8,20},{12,16},{16,12},{20,8},{24,4},{28,0},{1,29},{... | collective-permute-start | bytes 245768 | tf_op jit(solution)/shard_map/ppermute | solution.py:420
  68.1 6.9 %collective-permute-start = (bf16[160,512]{1,0:T(8,128)(2,1)S(1)}, bf16[160,512]{1,0:T(8,128)(2,1)S(1)}, u32[]{:S(2)}, u32[]{:S(2)}) collective-permute-start(bf16[160,512]{1,0:T(8,128)(2,1)S(1)} %get-tuple-element.39), channel_id=1, source_target_pairs={{0,4},{4,0},{8,12},{12,8},{16,20},{20,16},{24,28},{28,24},{1,5},{5... | collective-permute-start | bytes 491528 | tf_op jit(solution)/shard_map/ppermute | solution.py:420
  68.6 7.1 %collective-permute-start.1 = (bf16[160,512]{1,0:T(8,128)(2,1)S(1)}, bf16[160,512]{1,0:T(8,128)(2,1)S(1)}, u32[]{:S(2)}, u32[]{:S(2)}) collective-permute-start(bf16[160,512]{1,0:T(8,128)(2,1)S(1)} %get-tuple-element.40), channel_id=1, source_target_pairs={{0,8},{4,12},{8,0},{12,4},{16,24},{20,28},{24,16},{28,20},{1,9},{5... | collective-permute-start | bytes 491528 | tf_op jit(solution)/shard_map/ppermute | solution.py:420
  71.0 9.0 %collective-permute-start.2 = (bf16[160,512]{1,0:T(8,128)(2,1)S(1)}, bf16[160,512]{1,0:T(8,128)(2,1)S(1)}, u32[]{:S(2)}, u32[]{:S(2)}) collective-permute-start(bf16[160,512]{1,0:T(8,128)(2,1)S(1)} %get-tuple-element.41), channel_id=1, source_target_pairs={{0,12},{4,8},{8,4},{12,0},{16,28},{20,24},{24,20},{28,16},{1,13},{... | collective-permute-start | bytes 491528 | tf_op jit(solution)/shard_map/ppermute | solution.py:420
  75.0 8.2 %collective-permute-start.10 = (bf16[160,512]{1,0:T(8,128)(2,1)S(1)}, bf16[160,512]{1,0:T(8,128)(2,1)S(1)}, u32[]{:S(2)}, u32[]{:S(2)}) collective-permute-start(bf16[160,512]{1,0:T(8,128)(2,1)S(1)} %get-tuple-element.52), channel_id=1, source_target_pairs={{0,4},{4,0},{8,12},{12,8},{16,20},{20,16},{24,28},{28,24},{1,5},{5... | collective-permute-start | bytes 491528 | tf_op jit(solution)/shard_map/ppermute | solution.py:420
  75.7 9.0 %collective-permute-start.11 = (bf16[160,512]{1,0:T(8,128)(2,1)S(1)}, bf16[160,512]{1,0:T(8,128)(2,1)S(1)}, u32[]{:S(2)}, u32[]{:S(2)}) collective-permute-start(bf16[160,512]{1,0:T(8,128)(2,1)S(1)} %get-tuple-element.53), channel_id=1, source_target_pairs={{0,8},{4,12},{8,0},{12,4},{16,24},{20,28},{24,16},{28,20},{1,9},{5... | collective-permute-start | bytes 491528 | tf_op jit(solution)/shard_map/ppermute | solution.py:420
  79.9 7.0 %collective-permute-start.12 = (bf16[160,512]{1,0:T(8,128)(2,1)S(1)}, bf16[160,512]{1,0:T(8,128)(2,1)S(1)}, u32[]{:S(2)}, u32[]{:S(2)}) collective-permute-start(bf16[160,512]{1,0:T(8,128)(2,1)S(1)} %get-tuple-element.54), channel_id=1, source_target_pairs={{0,12},{4,8},{8,4},{12,0},{16,28},{20,24},{24,20},{28,16},{1,13},{... | collective-permute-start | bytes 491528 | tf_op jit(solution)/shard_map/ppermute | solution.py:420
  83.2 10.6 %collective-permute-start.13 = (bf16[160,256]{1,0:T(8,128)(2,1)S(1)}, bf16[160,256]{1,0:T(8,128)(2,1)S(1)}, u32[]{:S(2)}, u32[]{:S(2)}) collective-permute-start(bf16[160,256]{1,0:T(8,128)(2,1)S(1)} %get-tuple-element.55), channel_id=1, source_target_pairs={{0,16},{4,20},{8,24},{12,28},{16,0},{20,4},{24,8},{28,12},{1,17},{... | collective-permute-start | bytes 245768 | tf_op jit(solution)/shard_map/ppermute | solution.py:420
  84.8 14.2 %collective-permute-start.14 = (bf16[160,256]{1,0:T(8,128)(2,1)S(1)}, bf16[160,256]{1,0:T(8,128)(2,1)S(1)}, u32[]{:S(2)}, u32[]{:S(2)}) collective-permute-start(bf16[160,256]{1,0:T(8,128)(2,1)S(1)} %get-tuple-element.56), channel_id=1, source_target_pairs={{0,20},{4,16},{8,28},{12,24},{16,4},{20,0},{24,12},{28,8},{1,21},{... | collective-permute-start | bytes 245768 | tf_op jit(solution)/shard_map/ppermute | solution.py:420
  87.0 13.6 %collective-permute-start.15 = (bf16[160,256]{1,0:T(8,128)(2,1)S(1)}, bf16[160,256]{1,0:T(8,128)(2,1)S(1)}, u32[]{:S(2)}, u32[]{:S(2)}) collective-permute-start(bf16[160,256]{1,0:T(8,128)(2,1)S(1)} %get-tuple-element.57), channel_id=1, source_target_pairs={{0,24},{4,28},{8,16},{12,20},{16,8},{20,12},{24,0},{28,4},{1,25},{... | collective-permute-start | bytes 245768 | tf_op jit(solution)/shard_map/ppermute | solution.py:420
  93.8 7.1 %collective-permute-start.16 = (bf16[160,256]{1,0:T(8,128)(2,1)S(1)}, bf16[160,256]{1,0:T(8,128)(2,1)S(1)}, u32[]{:S(2)}, u32[]{:S(2)}) collective-permute-start(bf16[160,256]{1,0:T(8,128)(2,1)S(1)} %get-tuple-element.58), channel_id=1, source_target_pairs={{0,28},{4,24},{8,20},{12,16},{16,12},{20,8},{24,4},{28,0},{1,29},{... | collective-permute-start | bytes 245768 | tf_op jit(solution)/shard_map/ppermute | solution.py:420
  98.9 9.6 %collective-permute-start.7 = (bf16[160,256]{1,0:T(8,128)(2,1)S(1)}, bf16[160,256]{1,0:T(8,128)(2,1)S(1)}, u32[]{:S(2)}, u32[]{:S(2)}) collective-permute-start(bf16[160,256]{1,0:T(8,128)(2,1)S(1)} %get-tuple-element.48), channel_id=1, source_target_pairs={{0,4},{4,0},{8,12},{12,8},{16,20},{20,16},{24,28},{28,24},{1,5},{5... | collective-permute-start | bytes 245768 | tf_op jit(solution)/shard_map/ppermute | solution.py:420
  100.5 9.6 %collective-permute-start.8 = (bf16[160,256]{1,0:T(8,128)(2,1)S(1)}, bf16[160,256]{1,0:T(8,128)(2,1)S(1)}, u32[]{:S(2)}, u32[]{:S(2)}) collective-permute-start(bf16[160,256]{1,0:T(8,128)(2,1)S(1)} %get-tuple-element.49), channel_id=1, source_target_pairs={{0,8},{4,12},{8,0},{12,4},{16,24},{20,28},{24,16},{28,20},{1,9},{5... | collective-permute-start | bytes 245768 | tf_op jit(solution)/shard_map/ppermute | solution.py:420
  100.9 10.0 %collective-permute-start.9 = (bf16[160,256]{1,0:T(8,128)(2,1)S(1)}, bf16[160,256]{1,0:T(8,128)(2,1)S(1)}, u32[]{:S(2)}, u32[]{:S(2)}) collective-permute-start(bf16[160,256]{1,0:T(8,128)(2,1)S(1)} %get-tuple-element.50), channel_id=1, source_target_pairs={{0,12},{4,8},{8,4},{12,0},{16,28},{20,24},{24,20},{28,16},{1,13},{... | collective-permute-start | bytes 245768 | tf_op jit(solution)/shard_map/ppermute | solution.py:420
  108.6 5.3 %copy-start = (bf16[2048,512]{1,0:T(8,128)(2,1)S(1)}, bf16[2048,512]{1,0:T(8,128)(2,1)}, u32[]{:S(2)}) copy-start(bf16[2048,512]{1,0:T(8,128)(2,1)} %refs_8_.1) | copy-start | bytes 6291460
  108.6 6.1 %collective-permute-start.17 = (bf16[160,256]{1,0:T(8,128)(2,1)S(1)}, bf16[160,256]{1,0:T(8,128)(2,1)S(1)}, u32[]{:S(2)}, u32[]{:S(2)}) collective-permute-start(bf16[160,256]{1,0:T(8,128)(2,1)S(1)} %get-tuple-element.61), channel_id=1, source_target_pairs={{0,4},{4,0},{8,12},{12,8},{16,20},{20,16},{24,28},{28,24},{1,5},{5... | collective-permute-start | bytes 245768 | tf_op jit(solution)/shard_map/ppermute | solution.py:420
  110.2 4.6 %collective-permute-start.18 = (bf16[160,256]{1,0:T(8,128)(2,1)S(1)}, bf16[160,256]{1,0:T(8,128)(2,1)S(1)}, u32[]{:S(2)}, u32[]{:S(2)}) collective-permute-start(bf16[160,256]{1,0:T(8,128)(2,1)S(1)} %get-tuple-element.62), channel_id=1, source_target_pairs={{0,8},{4,12},{8,0},{12,4},{16,24},{20,28},{24,16},{28,20},{1,9},{5... | collective-permute-start | bytes 245768 | tf_op jit(solution)/shard_map/ppermute | solution.py:420
  110.9 5.3 %collective-permute-start.19 = (bf16[160,256]{1,0:T(8,128)(2,1)S(1)}, bf16[160,256]{1,0:T(8,128)(2,1)S(1)}, u32[]{:S(2)}, u32[]{:S(2)}) collective-permute-start(bf16[160,256]{1,0:T(8,128)(2,1)S(1)} %get-tuple-element.63), channel_id=1, source_target_pairs={{0,12},{4,8},{8,4},{12,0},{16,28},{20,24},{24,20},{28,16},{1,13},{... | collective-permute-start | bytes 245768 | tf_op jit(solution)/shard_map/ppermute | solution.py:420
